TPU v7x, 32 devices: a whole 2x2x4 slice. The times are simulated.
32 devices in a mesh: sp: 16 (over z, y, core), tp: 2 (over x).
Axes of the slice: x: 2, y: 2, z: 4, core: 2. Of those that a mesh axis runs over, the one named last changes fastest.
Arguments:
- asking_matrix: bfloat16 [2048, 2048], P('sp', 'tp'), may hold values from -30 to 30
- matching_key_matrix: bfloat16 [2048, 1024], P('sp', 'tp'), may hold values from -30 to 30
- carried_value_matrix: bfloat16 [2048, 1024], P('sp', 'tp'), may hold values from -48 to 48
- silu_switch_argument: bfloat16 [2048, 2048], P('sp', 'tp'), may hold values from -6 to 6
- duality_source_matrix: bfloat16 [2048, 2048], P('sp', 'tp'), may hold values from -6 to 6
- storing_direction_matrix: bfloat16 [2048, 1024], P('sp', 'tp'), may hold values from -6 to 6
- fetching_direction_matrix: bfloat16 [2048, 1024], P('sp', 'tp'), may hold values from -6 to 6
- duality_kernel_coefficients: bfloat16 [5, 2048], P(None, 'tp'), may hold values from -2.5 to 2.5
- storing_kernel_coefficients: bfloat16 [5, 1024], P(None, 'tp'), may hold values from -2.5 to 2.5
- fetching_kernel_coefficients: bfloat16 [5, 1024], P(None, 'tp'), may hold values from -2.5 to 2.5
- raw_increment_lengths: float32 [2, 32, 2048], P(None, 'tp', 'sp'), may hold values from -5.5 to 5.5
- logarithmic_fading_speeds: float32 [2, 32], P(None, 'tp'), may hold values from -16 to -2.9
- token_fading_spikes: float32 [2, 32, 2048], P(None, 'tp', 'sp'), may hold values from -2.1 to 0
- absorber_score_vector: float32 [16], P('tp'), may hold values from 4 to 8
- cluster_scaling_factor: float32 [2048], P('tp'), may hold values from 0.1 to 1.9
- final_mapping_matrix: bfloat16 [2, 2048, 4096], P(None, 'tp', 'sp'), may hold values from -0.09375 to 0.09375
Outputs:
- mixed_out: bfloat16 [2048, 4096], P(('sp', 'tp'))
All inputs are finite; a program needn't handle non-finite values.
Results may differ from a plain program's by a relative error of at most 0.014.
Values may be sent and summed in bfloat16 or wider, within the bound.
No kernel may reach another device: no remote copies, remote signals or barrier semaphores. Data moves between devices by JAX's collectives and lax.ppermute only.
A program may use at most 128 MiB of HBM per device.

v0:
```python
import jax
import jax.numpy as jnp
from jax import lax
from jax.sharding import PartitionSpec as P

HEAD = 128
SSD_HEAD = 64
STATE = 128
CONV = 5
WINDOW = 128
SPAN = 128


ROTARY_BASE = 500000.0
EPSILON = 1e-06


def padded_2(cells, sides, width):
    for axis, dim in sides:
        count = lax.axis_size(axis)
        ends = count - 1
        head = lax.slice_in_dim(cells, 0, width, axis=dim)
        tail = lax.slice_in_dim(cells, cells.shape[dim] - width, cells.shape[dim], axis=dim)
        cells = jnp.concatenate(
            [
                lax.ppermute(tail, axis, [(i, (i + 1) % count) for i in range(ends)]),
                cells,
                lax.ppermute(head, axis, [((i + 1) % count, i) for i in range(ends)]),
            ],
            axis=dim,
        )
    return cells


def entering_2(part, axis, combine, identity, reverse):
    count = lax.axis_size(axis)
    place = lax.axis_index(axis)
    ahead = count - 1 - place if reverse else place
    gathered = jax.tree.map(lambda a: lax.all_gather(a, axis), part)
    state = jax.tree.map(lambda a, e: jnp.zeros_like(a) + jnp.asarray(e, a.dtype), part, identity)

    def one(turn, state):
        source = count - 1 - turn if reverse else turn
        return combine(
            state, jax.tree.map(lambda a: lax.dynamic_index_in_dim(a, source, 0, False), gathered)
        )

    return lax.fori_loop(0, ahead, one, state)


def rotate(matrix, offset):
    row_count = matrix.shape[0]
    halfway = HEAD // 2
    heads_here = matrix.shape[1] // HEAD
    spacing = ROTARY_BASE ** (-jnp.arange(halfway, dtype=jnp.float32) * 2.0 / HEAD)
    places = (offset + jnp.arange(row_count, dtype=jnp.int32)).astype(jnp.float32)
    angles = places[:, None] * spacing[None, :]
    cosine = jnp.cos(angles)[:, None, :]
    sine_table = jnp.sin(angles)[:, None, :]
    halves = matrix.astype(jnp.float32).reshape(row_count, heads_here, 2, halfway)
    former = halves[:, :, 0]
    latter = halves[:, :, 1]
    turned = jnp.stack(
        [former * cosine - latter * sine_table, latter * cosine + former * sine_table], axis=2
    )
    return turned.reshape(row_count, heads_here * HEAD).astype(jnp.bfloat16)


def banded(matrix, block_count, kv_here):
    stacked = matrix.reshape(block_count + 2, SPAN, kv_here, HEAD)
    return jnp.concatenate([stacked[:-2], stacked[1:-1], stacked[2:]], axis=1)


def attend(turned_queries, key_band, value_band, absorber_score_vector, offset, seq_total):
    row_count = turned_queries.shape[0]
    block_count = row_count // SPAN
    kv_here = key_band.shape[1] // HEAD
    sharing = turned_queries.shape[1] // HEAD // kv_here
    key_tiles = banded(key_band, block_count, kv_here)
    value_tiles = banded(value_band, block_count, kv_here)
    query_tiles = turned_queries.reshape(block_count, SPAN, kv_here, sharing, HEAD)
    scores = jnp.einsum(
        "bqkgd,bskd->bkgqs", query_tiles, key_tiles, preferred_element_type=jnp.float32
    ) * HEAD ** (-0.5)
    within = jnp.arange(SPAN, dtype=jnp.int32)[:, None]
    across = jnp.arange(3 * SPAN, dtype=jnp.int32)[None, :]
    inside = jnp.abs(across - SPAN - within) <= WINDOW
    places = offset - SPAN + jnp.arange(block_count, dtype=jnp.int32)[:, None] * SPAN + across
    present = (places >= 0) & (places < seq_total)
    allowed = inside[None, :, :] & present[:, None, :]
    scores = jnp.where(allowed[:, None, None, :, :], scores, -jnp.inf)
    sink_rows = absorber_score_vector.reshape(kv_here, sharing)[None, :, :, None, None]
    ceiling = jnp.maximum(jnp.max(scores, axis=-1, keepdims=True), sink_rows)
    weights = jnp.exp(scores - ceiling)
    denominator = jnp.sum(weights, axis=-1, keepdims=True) + jnp.exp(sink_rows - ceiling)
    probabilities = (weights / denominator).astype(jnp.bfloat16)
    attended = jnp.einsum(
        "bkgqs,bskd->bqkgd", probabilities, value_tiles, preferred_element_type=jnp.float32
    )
    return attended.reshape(row_count, turned_queries.shape[1]).astype(jnp.bfloat16)


def convolve(padded, taps_all, row_count):
    summed = jnp.zeros((row_count, padded.shape[1]), jnp.float32)
    for tap_index in range(CONV):
        summed = summed + padded[tap_index : tap_index + row_count].astype(jnp.float32) * taps_all[
            tap_index
        ].astype(jnp.float32)
    return jax.nn.silu(summed).astype(jnp.bfloat16)


def prepare(scan_rows, step_rows, decay_rows, write_rows, read_rows):
    row_count = scan_rows.shape[0]
    block_count = row_count // SPAN
    groups_here = write_rows.shape[1]
    per_group = scan_rows.shape[2]
    highest = lax.Precision.HIGHEST
    step_tiles = step_rows.reshape(block_count, SPAN, groups_here, per_group)
    scaled = (
        scan_rows.astype(jnp.float32).reshape(block_count, SPAN, groups_here, per_group, SSD_HEAD)
        * step_tiles[..., None]
    )
    running = jnp.cumsum(decay_rows.reshape(block_count, SPAN, groups_here, per_group), axis=1)
    write_tiles = write_rows.reshape(block_count, SPAN, groups_here, STATE)
    read_tiles = read_rows.reshape(block_count, SPAN, groups_here, STATE)
    earlier_mask = jnp.arange(SPAN)[:, None] >= jnp.arange(SPAN)[None, :]
    spread = running[:, :, None] - running[:, None, :]
    fading = jnp.exp(jnp.where(earlier_mask[None, :, :, None, None], spread, -jnp.inf))
    affinity = jnp.einsum(
        "blgn,bsgn->blsg", read_tiles, write_tiles, preferred_element_type=jnp.float32
    )
    within_block = jnp.einsum(
        "blsgr,bsgrp->blgrp", affinity[..., None] * fading, scaled, precision=highest
    )
    to_end = jnp.exp(running[:, -1:] - running)
    block_states = jnp.einsum(
        "blgn,blgrp->bgrpn",
        write_tiles.astype(jnp.float32),
        scaled * to_end[..., None],
        precision=highest,
    )
    totals = running[:, -1]

    def advance(carried, block_item):
        fresh_state, block_total = block_item
        return (carried * jnp.exp(block_total)[..., None, None] + fresh_state, carried)

    final_state, entering = lax.scan(
        advance, jnp.zeros(block_states.shape[1:], jnp.float32), (block_states, totals)
    )
    summary = (jnp.exp(jnp.sum(totals, axis=0)), final_state)
    return ((within_block, entering, running, totals, read_tiles), summary)


def finish(pieces, incoming):
    within_block, entering, running, totals, read_tiles = pieces
    before = jnp.cumsum(totals, axis=0) - totals
    starting = entering + incoming[None] * jnp.exp(before)[..., None, None]
    carried = (
        jnp.einsum(
            "blgn,bgrpn->blgrp",
            read_tiles.astype(jnp.float32),
            starting,
            precision=lax.Precision.HIGHEST,
        )
        * jnp.exp(running)[..., None]
    )
    joined = within_block + carried
    return joined.reshape(joined.shape[0] * SPAN, -1)


def linked(earlier, later):
    return (earlier[0] * later[0], earlier[1] * later[0][..., None, None] + later[1])


def local(
    asking_matrix,
    matching_key_matrix,
    carried_value_matrix,
    silu_switch_argument,
    duality_source_matrix,
    storing_direction_matrix,
    fetching_direction_matrix,
    duality_kernel_coefficients,
    storing_kernel_coefficients,
    fetching_kernel_coefficients,
    raw_increment_lengths,
    logarithmic_fading_speeds,
    token_fading_spikes,
    absorber_score_vector,
    cluster_scaling_factor,
    final_mapping_matrix,
):
    row_count = asking_matrix.shape[0]
    offset = lax.axis_index("sp") * row_count
    seq_total = lax.axis_size("sp") * row_count
    turned_queries = rotate(asking_matrix, offset)
    key_value = jnp.concatenate([rotate(matching_key_matrix, offset), carried_value_matrix], axis=1)
    raw_rows = jnp.concatenate(
        [duality_source_matrix, storing_direction_matrix, fetching_direction_matrix], axis=1
    )
    margin = CONV // 2
    pair_rims = padded_2(key_value, (("sp", 0),), WINDOW)
    raw_rims = padded_2(raw_rows, (("sp", 0),), margin)
    filler = jnp.zeros((SPAN - WINDOW, key_value.shape[1]), jnp.bfloat16)
    pair_band = jnp.concatenate([filler, pair_rims, filler], axis=0)
    kv_width = matching_key_matrix.shape[1]
    attended = attend(
        turned_queries,
        pair_band[:, :kv_width],
        pair_band[:, kv_width:],
        absorber_score_vector,
        offset,
        seq_total,
    )
    conved = convolve(
        raw_rims,
        jnp.concatenate(
            [
                duality_kernel_coefficients,
                storing_kernel_coefficients,
                fetching_kernel_coefficients,
            ],
            axis=1,
        ),
        row_count,
    )
    scan_width = duality_source_matrix.shape[1]
    write_width = storing_direction_matrix.shape[1]
    groups_here = write_width // STATE
    per_group = scan_width // SSD_HEAD // groups_here
    scan_rows = conved[:, :scan_width].reshape(row_count, groups_here, per_group, SSD_HEAD)
    write_rows = conved[:, scan_width : scan_width + write_width].reshape(
        row_count, groups_here, STATE
    )
    read_rows = conved[:, scan_width + write_width :].reshape(row_count, groups_here, STATE)
    joint_increment_lengths = jax.nn.softplus(raw_increment_lengths)
    joint_fading_amounts = (
        -jnp.exp(logarithmic_fading_speeds)[:, :, None] * joint_increment_lengths
        + token_fading_spikes
    )
    steps_rows = jnp.transpose(joint_increment_lengths, (0, 2, 1)).reshape(
        2, row_count, groups_here, per_group
    )
    decay_rows = jnp.transpose(joint_fading_amounts, (0, 2, 1)).reshape(
        2, row_count, groups_here, per_group
    )
    ahead_pieces, ahead_summary = prepare(
        scan_rows, steps_rows[0], decay_rows[0], write_rows, read_rows
    )
    back_pieces, back_summary = prepare(
        scan_rows[::-1], steps_rows[1][::-1], decay_rows[1][::-1], write_rows[::-1], read_rows[::-1]
    )
    identity = (
        jnp.ones((groups_here, per_group), jnp.float32),
        jnp.zeros((groups_here, per_group, SSD_HEAD, STATE), jnp.float32),
    )
    ahead_in = entering_2(ahead_summary, "sp", linked, identity, False)
    back_in = entering_2(back_summary, "sp", linked, identity, True)
    both_ways = finish(ahead_pieces, ahead_in[1]) + finish(back_pieces, back_in[1])[::-1]
    gated_rows = both_ways * jax.nn.silu(silu_switch_argument.astype(jnp.float32))
    grouped = gated_rows.reshape(row_count, groups_here, -1)
    grouped = grouped * lax.rsqrt(jnp.mean(grouped * grouped, axis=-1, keepdims=True) + EPSILON)
    normed = (grouped.reshape(row_count, scan_width) * cluster_scaling_factor).astype(jnp.bfloat16)
    mixed_rows = jnp.concatenate([attended, normed], axis=1)
    whole_weight = lax.all_gather(final_mapping_matrix, "sp", axis=2, tiled=True)
    stacked = whole_weight.reshape(-1, whole_weight.shape[2])
    return lax.psum_scatter(
        jnp.dot(mixed_rows, stacked, preferred_element_type=jnp.float32).astype(jnp.bfloat16),
        "tp",
        scatter_dimension=0,
        tiled=True,
    )


def solution(mesh):
    in_specs = (
        P("sp", "tp"),
        P("sp", "tp"),
        P("sp", "tp"),
        P("sp", "tp"),
        P("sp", "tp"),
        P("sp", "tp"),
        P("sp", "tp"),
        P(None, "tp"),
        P(None, "tp"),
        P(None, "tp"),
        P(None, "tp", "sp"),
        P(None, "tp"),
        P(None, "tp", "sp"),
        P("tp"),
        P("tp"),
        P(None, "tp", "sp"),
    )
    out_specs = P(("sp", "tp"), None)
    return jax.shard_map(local, mesh=mesh, in_specs=in_specs, out_specs=out_specs, check_vma=False)
```

profile of v0, /device:TPU:0, one launch (start us, length us, event | category | flops | bytes accessed | tf_op | source)
XLA Modules:
  0.0 351.5 jit_solution(15018297728650527483)
XLA Ops:
  10.1 2.4 collective-permute-start.2
  12.5 1.3 collective-permute-start.3
  16.6 1.8 collective-permute-done.3
  19.1 4.5 %multiply_convert_fusion = bf16[128,2048]{0,1:T(8,128)(2,1)S(1)} fusion(bf16[130,2048]{0,1:T(8,128)(2,1)S(1)} %get-tuple-element.190, bf16[130,2048]{0,1:T(8,128)(2,1)S(1)} %get-tuple-element.189, f32[2048]{0:T(1024)S(1)} %bitcast.195, f32[2048]{0:T(1024)S(1)} %bitcast.196, f32[2048]{0:T(1024)S(1)} %bitcast.197, f32[2048]{0:T(1024)S(1)} %bitcast.198, ...), kind=kLoop, calls=%fused_computation.32 | loop fusion | flops 6291456 | bytes 3186688 | tf_op jit(solution)/shard_map/convert_element_type | solution.py:109
  24.2 1.2 convolution_add_fusion
  26.2 1.2 convolution_add_fusion.1
  28.9 11.0 %collective-permute-start = (bf16[128,1024]{0,1:T(8,128)(2,1)S(1)}, bf16[128,1024]{0,1:T(8,128)(2,1)}, u32[]{:S(2)}, u32[]{:S(2)}) collective-permute-start(bf16[128,1024]{0,1:T(8,128)(2,1)S(1)} %pad_maximum_fusion.2), channel_id=1, source_target_pairs={{0,2},{2,4},{4,6},{6,8},{8,10},{10,12},{12,14},{14,16},{16,18},{18... | collective-permute-start | bytes 786440 | tf_op jit(solution)/shard_map/ppermute | solution.py:26
  39.9 1.3 collective-permute-start.1
  43.3 24.6 %all-gather.2 = f32[16,1,4,4]{3,2,1,0:T(4,128)S(1)} all-gather(f32[1,1,4,4]{3,2,1,0:T(4,128)S(1)} %copy-done.13), channel_id=4, replica_groups=mesh['sp'=16,'tp'=2] {'sp'}, dimensions={0}, use_global_device_ids=true | all-gather | bytes 1088 | tf_op jit(solution)/shard_map/all_gather | solution.py:39
  68.0 18.2 %all-gather = f32[16,1,4,4]{3,2,1,0:T(4,128)S(1)} all-gather(f32[1,1,4,4]{3,2,1,0:T(4,128)S(1)} %get-tuple-element.210), channel_id=2, replica_groups=mesh['sp'=16,'tp'=2] {'sp'}, dimensions={0}, use_global_device_ids=true | all-gather | bytes 1088 | tf_op jit(solution)/shard_map/all_gather | solution.py:39
  91.3 20.1 %all-gather.12.cloned.1.call-done = f32[64,4,64,128]{3,2,1,0:T(8,128)} async-done(((f32[4,4,64,128]{3,2,1,0:T(8,128)}), f32[64,4,64,128]{3,2,1,0:T(8,128)}) %all-gather.12.cloned.1.call-update) | async-done | bytes 8388624 | tf_op jit(solution)/shard_map/all_gather | solution.py:39
  111.5 18.6 %while.17 = (s32[]{:T(128)}, f32[4,4,64,128]{3,2,1,0:T(8,128)S(1)}, s32[]{:T(128)}, f32[16,4,4]{2,1,0:T(4,128)S(1)}, f32[16,4,4,64,128]{4,3,2,1,0:T(8,128)}, /*index=5*/s32[]{:T(128)}, s32[]{:T(128)}, s32[]{:T(128)}, s32[]{:T(128)}) while((s32[]{:T(128)}, f32[4,4,64,128]{3,2,1,0:T(8,128)S(1)}, s32[]{:T(128)}, f32[16,4,4]{2,1,0:T(4,128)S(1)}, ...), condition=%wide.region_7.8_spmd, body=%wide.region_6.7_spmd.sunk | while | flops 262150 | bytes 1573203 | solution.py:48
  115.2 1.2 bitcast_add_fusion.5
  118.9 1.2 bitcast_add_fusion.5
  120.2 1.2 bitcast_add_fusion.5
  125.2 1.2 bitcast_add_fusion.5
  126.4 1.2 bitcast_add_fusion.5
  127.6 1.2 bitcast_add_fusion.5
  130.6 2.2 fusion.1
  133.2 53.3 %all-gather.10.cloned.1.call-done = f32[64,4,64,128]{3,2,1,0:T(8,128)} async-done(((f32[4,4,64,128]{3,2,1,0:T(8,128)}), f32[64,4,64,128]{3,2,1,0:T(8,128)}) %all-gather.10.cloned.1.call-update) | async-done | bytes 8388624 | tf_op jit(solution)/shard_map/all_gather | solution.py:39
  187.2 2.2 fusion.2
  190.9 126.3 %all-gather.8.cloned.1.call-done = bf16[2,1024,4096]{2,1,0:T(8,128)(2,1)} async-done(((bf16[2,1024,256]{2,1,0:T(8,128)(2,1)}), bf16[2,1024,4096]{2,1,0:T(8,128)(2,1)}) %all-gather.8.cloned.1.call-update) | async-done | bytes 16777232 | tf_op jit(solution)/shard_map/all_gather | solution.py:266
  317.2 9.1 %convolution_convert_fusion = bf16[128,4096]{1,0:T(8,128)(2,1)} fusion(bf16[2048,4096]{1,0:T(8,128)(2,1)} %bitcast.163, bf16[128,1024]{1,0:T(8,128)(2,1)S(1)} %multiply_convert_fusion.1, bf16[128,1024]{1,0:T(8,128)(2,1)S(1)} %copy.185), kind=kOutput, calls=%fused_computation.4 | convolution fusion | flops 2149056512 | bytes 18350080 | tf_op jit(solution)/shard_map/dot_general | solution.py:269
  326.3 18.7 %reduce-scatter.2.cloned.1.call-done = bf16[64,4096]{1,0:T(8,128)(2,1)} async-done(((bf16[128,4096]{1,0:T(8,128)(2,1)}), bf16[64,4096]{1,0:T(8,128)(2,1)}) %reduce-scatter.2.cloned.1.call-update) | async-done | bytes 524304 | tf_op jit(solution)/shard_map/reduce_scatter | solution.py:268
  (157 shorter events, 30.3 us)
Async XLA Ops:
  6.5 7.3 %copy-start.7 = (bf16[5,1024]{1,0:T(8,128)(2,1)S(1)}, bf16[5,1024]{1,0:T(8,128)(2,1)}, u32[]{:S(2)}) copy-start(bf16[5,1024]{1,0:T(8,128)(2,1)} %param.27) | copy-start | bytes 30724
  6.5 7.3 %copy-start.14 = (bf16[5,512]{1,0:T(8,128)(2,1)S(1)}, bf16[5,512]{1,0:T(8,128)(2,1)}, u32[]{:S(2)}) copy-start(bf16[5,512]{1,0:T(8,128)(2,1)} %param.28) | copy-start | bytes 15364
  6.5 7.3 %copy-start.15 = (bf16[5,512]{1,0:T(8,128)(2,1)S(1)}, bf16[5,512]{1,0:T(8,128)(2,1)}, u32[]{:S(2)}) copy-start(bf16[5,512]{1,0:T(8,128)(2,1)} %param.29) | copy-start | bytes 15364
  6.5 7.4 %copy-start.17 = (f32[2,16]{1,0:T(2,128)S(1)}, f32[2,16]{1,0:T(2,128)}, u32[]{:S(2)}) copy-start(f32[2,16]{1,0:T(2,128)} %param.31) | copy-start | bytes 388
  6.5 7.4 %copy-start.8 = (f32[2,16,128]{2,1,0:T(8,128)S(1)}, f32[2,16,128]{2,1,0:T(8,128)}, u32[]{:S(2)}) copy-start(f32[2,16,128]{2,1,0:T(8,128)} %param.30) | copy-start | bytes 49156
  6.5 7.4 %copy-start.9 = (f32[2,16,128]{2,1,0:T(8,128)S(1)}, f32[2,16,128]{2,1,0:T(8,128)}, u32[]{:S(2)}) copy-start(f32[2,16,128]{2,1,0:T(8,128)} %param.32) | copy-start | bytes 49156
  6.6 104.9 %all-gather.12.cloned.1.call-start = ((), (), s32[]{:S(2)}) async-start(), calls=%async_computation.4 | async-start | bytes 8912896 | tf_op jit(solution)/shard_map/all_gather | solution.py:39
  10.1 6.5 %collective-permute-start.2 = (bf16[2,2048]{0,1:T(8,128)(2,1)S(1)}, bf16[2,2048]{0,1:T(8,128)(2,1)S(1)}, u32[]{:S(2)}, u32[]{:S(2)}) collective-permute-start(bf16[2,2048]{0,1:T(8,128)(2,1)S(1)} %get-tuple-element.191), channel_id=1, source_target_pairs={{0,2},{2,4},{4,6},{6,8},{8,10},{10,12},{12,14},{14,16},{16,18},{18... | collective-permute-start | bytes 24584 | tf_op jit(solution)/shard_map/ppermute | solution.py:26
  12.5 5.9 %collective-permute-start.3 = (bf16[2,2048]{0,1:T(8,128)(2,1)S(1)}, bf16[2,2048]{0,1:T(8,128)(2,1)S(1)}, u32[]{:S(2)}, u32[]{:S(2)}) collective-permute-start(bf16[2,2048]{0,1:T(8,128)(2,1)S(1)} %get-tuple-element.192), channel_id=1, source_target_pairs={{2,0},{4,2},{6,4},{8,6},{10,8},{12,10},{14,12},{16,14},{18,16},{20... | collective-permute-start | bytes 24584 | tf_op jit(solution)/shard_map/ppermute | solution.py:28
  19.1 5.2 %copy-start.11 = (f32[4,4]{1,0:T(4,128)S(1)}, f32[4,4]{1,0:T(4,128)}, u32[]{:S(2)}) copy-start(f32[4,4]{1,0:T(4,128)} %get-tuple-element.200) | copy-start | bytes 196
  23.6 2.5 copy-start.5
  25.5 161.0 %all-gather.10.cloned.1.call-start = ((), (), s32[]{:S(2)}) async-start(), calls=%async_computation.3 | async-start | bytes 8912896 | tf_op jit(solution)/shard_map/all_gather | solution.py:39
  25.9 2.5 copy-start.3
  27.4 14.5 %copy-start.1 = (bf16[128,1024]{1,0:T(8,128)(2,1)S(1)}, bf16[128,1024]{1,0:T(8,128)(2,1)}, u32[]{:S(2)}) copy-start(bf16[128,1024]{1,0:T(8,128)(2,1)} %param.20) | copy-start | bytes 786436
  27.4 289.8 %all-gather.8.cloned.1.call-start = ((), (), s32[]{:S(2)}) async-start(), calls=%async_computation.1 | async-start | bytes 17825792 | tf_op jit(solution)/shard_map/all_gather | solution.py:266
  28.2 14.0 %copy-start.18 = (f32[8]{0:T(128)S(1)}, f32[8]{0:T(128)}, u32[]{:S(2)}) copy-start(f32[8]{0:T(128)} %param.33) | copy-start | bytes 100
  28.2 316.8 %reduce-scatter.2.cloned.1.call-start = ((), (), s32[]{:S(2)}) async-start(), calls=%async_computation.2 | async-start | bytes 1572864 | tf_op jit(solution)/shard_map/reduce_scatter | solution.py:268
  28.4 14.9 %copy-start.13 = (f32[1,1,4,4]{3,2,1,0:T(4,128)S(1)}, f32[1,1,4,4]{3,2,1,0:T(4,128)}, u32[]{:S(2)}) copy-start(f32[1,1,4,4]{3,2,1,0:T(4,128)} %get-tuple-element.204) | copy-start | bytes 196
  28.9 58.8 %collective-permute-start = (bf16[128,1024]{0,1:T(8,128)(2,1)S(1)}, bf16[128,1024]{0,1:T(8,128)(2,1)}, u32[]{:S(2)}, u32[]{:S(2)}) collective-permute-start(bf16[128,1024]{0,1:T(8,128)(2,1)S(1)} %pad_maximum_fusion.2), channel_id=1, source_target_pairs={{0,2},{2,4},{4,6},{6,8},{8,10},{10,12},{12,14},{14,16},{16,18},{18... | collective-permute-start | bytes 786440 | tf_op jit(solution)/shard_map/ppermute | solution.py:26
  39.9 48.9 %collective-permute-start.1 = (bf16[128,1024]{0,1:T(8,128)(2,1)S(1)}, bf16[128,1024]{0,1:T(8,128)(2,1)}, u32[]{:S(2)}, u32[]{:S(2)}) collective-permute-start(bf16[128,1024]{0,1:T(8,128)(2,1)S(1)} %pad_maximum_fusion.2), channel_id=1, source_target_pairs={{2,0},{4,2},{6,4},{8,6},{10,8},{12,10},{14,12},{16,14},{18,16},{20... | collective-permute-start | bytes 786440 | tf_op jit(solution)/shard_map/ppermute | solution.py:28
  86.4 3.6 %copy-start.4 = (bf16[1,128,4,128]{3,1,2,0:T(8,128)(2,1)S(1)}, bf16[1,128,4,128]{3,1,2,0:T(8,128)(2,1)}, u32[]{:S(2)}) copy-start(bf16[1,128,4,128]{3,1,2,0:T(8,128)(2,1)} %copy.153) | copy-start | bytes 393220
  111.5 18.6 %copy-start.10 = (f32[4,4]{1,0:T(4,128)S(1)}, f32[4,4]{1,0:T(4,128)}, u32[]{:S(2)}) copy-start(f32[4,4]{1,0:T(4,128)} %get-tuple-element.199) | copy-start | bytes 196
  111.5 19.1 %copy-start.12 = (f32[128,4,4]{0,2,1:T(4,128)S(1)}, f32[128,4,4]{0,2,1:T(4,128)}, u32[]{:S(2)}) copy-start(f32[128,4,4]{0,2,1:T(4,128)} %copy.175) | copy-start | bytes 24580
  186.8 2.9 copy-start
  (3 other events, 5.3 us)
Sparse Core Ops, SparseCore 0:
  25.6 85.7 all-gather.11
  113.6 72.8 all-gather.9
  188.7 128.4 all-gather.7
  326.4 18.5 reduce-scatter.1
where the time goes:
time: 353 us; the launch traced here: 352 us
  waiting for transfers between devices  221 us (63%)
  blocking collectives  42.9 us (12%)
  other arithmetic  26 us (7%)
  matrix products  18.1 us (5%)
  starting transfers between devices  16.2 us (5%)
  between operations  13.9 us (4%)
  local copies, waits for them, and re-layouts  12.8 us (4%)
    all_gather x1, waiting for transfers between devices, local(): lax.all_gather(final_mapping_matrix, 'sp', axis=2, tiled=True)  126 us
    all_gather x2, waiting for transfers between devices, entering_2(): gathered = jax.tree.map(lambda a: lax.all_gather(a, axis), part)  73.4 us
    all_gather x2, blocking collectives, entering_2(): gathered = jax.tree.map(lambda a: lax.all_gather(a, axis), part)  42.9 us
    reduce_scatter x1, waiting for transfers between devices, local(): lax.psum_scatter(jnp.dot(mixed_rows, stacked, preferred_element_type=jnp....  18.7 us
    add x15, other arithmetic, linked(): earlier[1] * later[0][..., None, None] + later[1]  17.9 us
    ppermute x2, starting transfers between devices, padded_2(): lax.ppermute(tail, axis, [(i, (i + 1) % count) for i in range(ends)])  13.5 us
    dot_general x1, matrix products, local(): jnp.dot(mixed_rows, stacked, preferred_element_type=jnp.float32)  9.08 us
  transfers between devices with their start and end apart: 8, of which 5 were waited for; matrix products, arithmetic and copies ran while one was open for 11% of the time, Pallas kernels for 0%

commit v1 on v0

v1 whole, which is shorter than its diff:
```python
import functools

import jax
import jax.numpy as jnp
from jax import lax
from jax.experimental import pallas as pl
from jax.experimental.pallas import tpu as pltpu
from jax.sharding import PartitionSpec as P

HEAD = 128
SSD_HEAD = 64
STATE = 128
CONV = 5
WINDOW = 128
EDGE = 16

ROTARY_BASE = 500000.0
EPSILON = 1e-06
HIGHEST = lax.Precision.HIGHEST
F32 = jnp.float32
BF16 = jnp.bfloat16
VMEM = pl.BlockSpec(memory_space=pltpu.VMEM)
SMEM = pl.BlockSpec(memory_space=pltpu.SMEM)


def call(kernel, outs, ins, flops, scratch=(), scalars=1, name=None):
    moved = sum(a.size * a.dtype.itemsize for a in list(ins) + list(outs))
    return pl.pallas_call(
        kernel,
        out_shape=outs,
        in_specs=[SMEM] * scalars + [VMEM] * (len(ins) - scalars),
        out_specs=[VMEM] * len(outs),
        scratch_shapes=list(scratch),
        cost_estimate=pl.CostEstimate(flops=flops, bytes_accessed=moved, transcendentals=0),
        name=name,
    )(*ins)


def nn(a, b, precision=None):
    return lax.dot_general(
        a, b, (((1,), (0,)), ((), ())), precision=precision, preferred_element_type=F32
    )


def nt(a, b, precision=None):
    return lax.dot_general(
        a, b, (((1,), (1,)), ((), ())), precision=precision, preferred_element_type=F32
    )


def silu(v):
    return v / (1.0 + jnp.exp(-v))


def head_spread(heads, cols):
    head = lax.broadcasted_iota(jnp.int32, (heads, cols), 0)
    col = lax.broadcasted_iota(jnp.int32, (heads, cols), 1)
    return jnp.where(col // SSD_HEAD == head, 1.0, 0.0).astype(F32)


def block_kernel(
    place,
    x_ref,
    w_ref,
    r_ref,
    prev_ref,
    next_ref,
    tx_ref,
    tw_ref,
    tr_ref,
    inc_ref,
    fade_ref,
    spike_ref,
    keep_ref,
    send_ref,
    read_ref,
    y_ref,
    expl_ref,
    line,
    xs,
    ws,
):
    rows, cols = x_ref.shape
    wide = w_ref.shape[1]
    heads = cols // SSD_HEAD
    groups = wide // STATE
    per = heads // groups
    margin = CONV // 2
    start = 0
    for src, taps, dst in ((x_ref, tx_ref, xs), (w_ref, tw_ref, ws), (r_ref, tr_ref, read_ref)):
        span = src.shape[1]
        line[0:EDGE, 0:span] = prev_ref[:, start : start + span].astype(F32)
        line[EDGE : EDGE + rows, 0:span] = src[...].astype(F32)
        line[EDGE + rows : 2 * EDGE + rows, 0:span] = next_ref[:, start : start + span].astype(F32)
        step = min(span, 256)
        for at in range(0, span, step):
            total = jnp.zeros((rows, step), F32)
            for k in range(CONV):
                low = EDGE - margin + k
                total = total + line[low : low + rows, at : at + step] * taps[
                    k : k + 1, at : at + step
                ].astype(F32)
            dst[:, at : at + step] = silu(total).astype(BF16)
        start += span

    steps = jax.nn.softplus(inc_ref[...])
    logs = -jnp.exp(fade_ref[...]) * steps + spike_ref[...]
    first = lax.broadcasted_iota(jnp.int32, (rows, rows), 0)
    second = lax.broadcasted_iota(jnp.int32, (rows, rows), 1)
    lower = first >= second
    upper = first <= second
    run_f = nn(logs[0:heads], jnp.where(upper, 1.0, 0.0), HIGHEST)
    run_b = nn(logs[heads : 2 * heads], jnp.where(lower, 1.0, 0.0), HIGHEST)
    tall = jnp.concatenate([run_f, run_b], axis=0).T
    expl_ref[...] = jnp.exp(tall)
    tot_f = run_f[:, rows - 1 : rows]
    tot_b = run_b[:, 0:1]
    end_f = jnp.exp(tot_f - run_f) * steps[0:heads]
    end_b = jnp.exp(tot_b - run_b) * steps[heads : 2 * heads]

    spread = head_spread(heads, cols)
    tot = jnp.exp(jnp.concatenate([tall[rows - 1 : rows, 0:heads], tall[0:1, heads:]], axis=0))
    tot = nn(tot, spread, HIGHEST)
    high = tot.astype(BF16)
    low = (tot - high.astype(F32)).astype(BF16)
    half = cols // 2
    tail = jnp.concatenate(
        [high.astype(F32), low.astype(F32), jnp.zeros((EDGE - 4, cols), F32)], axis=0
    ).astype(BF16)
    for side in range(2):
        part = tail[:, side * half : (side + 1) * half]

        @pl.when(place[0] == side)
        def _():
            keep_ref[2 * STATE : 2 * STATE + EDGE, :] = part

        @pl.when(place[0] != side)
        def _():
            send_ref[2 * STATE : 2 * STATE + EDGE, :] = part

    for g in range(groups):
        wg = ws[:, g * STATE : (g + 1) * STATE]
        rg = read_ref[:, g * STATE : (g + 1) * STATE]
        affinity = nt(rg, wg)
        turned = wg.astype(F32).T
        fresh = []
        for j in range(per):
            h = g * per + j
            at = h * SSD_HEAD
            ahead = jnp.exp(
                jnp.where(lower, tall[:, h : h + 1] - run_f[h : h + 1, :], -jnp.inf)
            ) * steps[h : h + 1, :]
            back = jnp.exp(
                jnp.where(
                    upper, tall[:, heads + h : heads + h + 1] - run_b[h : h + 1, :], -jnp.inf
                )
            ) * steps[heads + h : heads + h + 1, :]
            mixed = (affinity * (ahead + back)).astype(BF16)
            grow_f = (turned * end_f[h : h + 1, :]).astype(BF16)
            grow_b = (turned * end_b[h : h + 1, :]).astype(BF16)
            got = nn(jnp.concatenate([mixed, grow_f, grow_b], axis=0), xs[:, at : at + SSD_HEAD])
            y_ref[:, at : at + SSD_HEAD] = got[0:rows]
            fresh.append(got[rows : rows + 2 * STATE].astype(BF16))
        whole = jnp.concatenate(fresh, axis=1)
        size = per * SSD_HEAD
        base = g * size
        for side in range(2):
            a = max(base, side * half)
            b = min(base + size, (side + 1) * half)
            if a >= b:
                continue
            part = whole[:, a - base : b - base]

            @pl.when(place[0] == side)
            def _():
                keep_ref[0 : 2 * STATE, a - side * half : b - side * half] = part

            @pl.when(place[0] != side)
            def _():
                send_ref[0 : 2 * STATE, a - side * half : b - side * half] = part


def attend_kernel(
    place, sink, q_ref, k_ref, v_ref, prev_ref, next_ref, cos_ref, sin_ref, out_ref
):
    rows = q_ref.shape[0]
    kv = k_ref.shape[1] // HEAD
    sharing = q_ref.shape[1] // k_ref.shape[1]
    wide = k_ref.shape[1]

    def turn(m, low):
        m = m.astype(F32)
        half = HEAD // 2
        other = jnp.concatenate([m[:, half:], m[:, :half]], axis=1)
        high = low + m.shape[0]
        return (m * cos_ref[low:high, :] + other * sin_ref[low:high, :]).astype(BF16)

    within = lax.broadcasted_iota(jnp.int32, (rows, 3 * rows), 0)
    across = lax.broadcasted_iota(jnp.int32, (rows, 3 * rows), 1)
    far = across - rows - within
    allowed = (far <= WINDOW) & (far >= -WINDOW)
    allowed = allowed & ((across >= rows) | (place[0] > 0))
    allowed = allowed & ((across < 2 * rows) | (place[0] < place[1] - 1))
    for g in range(kv):
        at = g * HEAD
        keys = jnp.concatenate(
            [
                turn(prev_ref[:, at : at + HEAD], 0),
                turn(k_ref[:, at : at + HEAD], rows),
                turn(next_ref[:, at : at + HEAD], 2 * rows),
            ],
            axis=0,
        )
        values = jnp.concatenate(
            [
                prev_ref[:, wide + at : wide + at + HEAD],
                v_ref[:, at : at + HEAD],
                next_ref[:, wide + at : wide + at + HEAD],
            ],
            axis=0,
        )
        for j in range(sharing):
            h = g * sharing + j
            query = turn(q_ref[:, h * HEAD : (h + 1) * HEAD], rows)
            scores = nt(query, keys) * HEAD ** (-0.5)
            scores = jnp.where(allowed, scores, -jnp.inf)
            top = jnp.maximum(jnp.max(scores, axis=1, keepdims=True), sink[h])
            weights = jnp.exp(scores - top)
            total = jnp.sum(weights, axis=1, keepdims=True) + jnp.exp(sink[h] - top)
            chance = (weights / total).astype(BF16)
            out_ref[:, h * HEAD : (h + 1) * HEAD] = nn(chance, values).astype(BF16)


def finish_kernel(place, y_ref, read_ref, expl_ref, own_ref, got_ref, gate_ref, gain_ref, out_ref):
    rows, cols = y_ref.shape
    wide = read_ref.shape[1]
    heads = cols // SSD_HEAD
    groups = wide // STATE
    size = cols // groups
    half = cols // 2
    spread = head_spread(heads, cols)
    for g in range(groups):
        at = g * size
        rg = read_ref[:, g * STATE : (g + 1) * STATE]
        pieces = []
        for low in range(at, at + size, min(size, half)):
            span = min(size, half)
            side = low // half
            off = low - side * half
            mine = place[0] == side
            pieces.append(
                jnp.where(
                    mine,
                    own_ref[:, off : off + span].astype(F32),
                    got_ref[:, off : off + span].astype(F32),
                ).astype(BF16)
            )
        states = pieces[0] if len(pieces) == 1 else jnp.concatenate(pieces, axis=1)
        local = spread[:, at : at + size]
        fade_f = nn(expl_ref[:, 0:heads], local, HIGHEST)
        fade_b = nn(expl_ref[:, heads : 2 * heads], local, HIGHEST)
        both = (
            y_ref[:, at : at + size]
            + fade_f * nn(rg, states[0:STATE])
            + fade_b * nn(rg, states[STATE : 2 * STATE])
        )
        gated = both * silu(gate_ref[:, at : at + size].astype(F32))
        mean = jnp.sum(gated * gated, axis=1, keepdims=True) * (1.0 / size)
        out_ref[:, at : at + size] = (
            gated * lax.rsqrt(mean + EPSILON) * gain_ref[:, at : at + size]
        ).astype(BF16)


def project_kernel(count, place, a_ref, ap_ref, n_ref, np_ref, *refs):
    shards = refs[:count]
    own_ref, x_ref, c_ref, cx_ref = refs[count:]
    rows = a_ref.shape[0]
    half = rows // 2
    left = jnp.concatenate([a_ref[...], ap_ref[...]], axis=0)
    right = jnp.concatenate([n_ref[...], np_ref[...]], axis=0)
    for j in range(count):
        span = shards[j].shape[2]
        at = j * span
        total = (nn(left, shards[j][0]) + nn(right, shards[j][1])).astype(BF16)
        for side in range(2):

            @pl.when(place[0] == side)
            def _():
                a, b = side * half, (1 - side) * half
                own_ref[:, at : at + span] = total[a : a + half]
                x_ref[:, at : at + span] = total[b : b + half]
                c_ref[:, at : at + span] = total[rows + a : rows + a + half]
                cx_ref[:, at : at + span] = total[rows + b : rows + b + half]


def place_kernel(masks, spans, place, *refs):
    out_ref = refs[-1]
    for i, group in enumerate(masks):
        own, x, c, cx = refs[4 * i : 4 * i + 4]
        span = spans
        for j, _ in enumerate(group):
            index = sum(len(m) for m in masks[:i]) + j
            at = j * span
            mine = pl.multiple_of(place[2 * index] * span, span)
            theirs = pl.multiple_of(place[2 * index + 1] * span, span)
            out_ref[:, pl.ds(mine, span)] = (
                own[:, at : at + span].astype(F32) + x[:, at : at + span].astype(F32)
            ).astype(BF16)
            out_ref[:, pl.ds(theirs, span)] = (
                c[:, at : at + span].astype(F32) + cx[:, at : at + span].astype(F32)
            ).astype(BF16)


def flip(a, count, mask):
    return lax.ppermute(a, "sp", [(i, i ^ mask) for i in range(count)])


def shift(a, count, by):
    return lax.ppermute(
        a, "sp", [(i, i + by) for i in range(count) if 0 <= i + by < count]
    )


def exchange_states(keep, send, count, me):
    half = keep.shape[1]
    core = me & 1
    got = flip(send, count, 1)

    def split(a):
        tail = a[2 * STATE :].astype(F32)
        return (
            a[:STATE].astype(F32),
            a[STATE : 2 * STATE].astype(F32),
            tail[0:1] + tail[2:3],
            tail[1:2] + tail[3:4],
        )

    mine = split(keep)
    theirs = split(got)
    pick = lambda flag, a, b: jax.tree.map(lambda u, v: jnp.where(flag, u, v), a, b)
    low = pick(core == 0, mine, theirs)
    high = pick(core == 0, theirs, mine)
    join = lambda low, high: (
        low[0] * high[2] + high[0],
        high[1] * low[3] + low[1],
        low[2] * high[2],
        low[3] * high[3],
    )
    pair = (low, high)
    total = join(low, high)
    into_f = jnp.zeros((STATE, half), F32)
    into_b = jnp.zeros((STATE, half), F32)
    gap_f = jnp.ones((1, half), F32)
    gap_b = jnp.ones((1, half), F32)
    bit = 2
    while bit < count:
        upper = (me & bit) != 0
        last = bit * 2 >= count
        if last:
            payload = jnp.where(upper, total[1], total[0]).astype(BF16)
            other = flip(payload, count, bit).astype(F32)
            into_f = jnp.where(upper, other * gap_f + into_f, into_f)
            into_b = jnp.where(upper, into_b, other * gap_b + into_b)
        else:
            fades = jnp.concatenate([total[2], total[3]], axis=0)
            top = fades.astype(BF16)
            rest = (fades - top.astype(F32)).astype(BF16)
            payload = jnp.concatenate(
                [
                    total[0].astype(BF16),
                    total[1].astype(BF16),
                    top,
                    rest,
                    jnp.zeros((EDGE - 4, half), BF16),
                ],
                axis=0,
            )
            other = split(flip(payload, count, bit))
            low = pick(upper, other, total)
            high = pick(upper, total, other)
            into_f = jnp.where(upper, other[0] * gap_f + into_f, into_f)
            into_b = jnp.where(upper, into_b, other[1] * gap_b + into_b)
            gap_f = jnp.where(upper, gap_f * other[2], gap_f)
            gap_b = jnp.where(upper, gap_b, gap_b * other[3])
            total = join(low, high)
        bit *= 2
    low, high = pair
    first = jnp.concatenate([into_f, into_b * high[3] + high[1]], axis=0).astype(BF16)
    second = jnp.concatenate([into_f * low[2] + low[0], into_b], axis=0).astype(BF16)
    own = jnp.where(core == 0, first, second)
    away = jnp.where(core == 0, second, first)
    return own, flip(away, count, 1)


def local(
    asking_matrix,
    matching_key_matrix,
    carried_value_matrix,
    silu_switch_argument,
    duality_source_matrix,
    storing_direction_matrix,
    fetching_direction_matrix,
    duality_kernel_coefficients,
    storing_kernel_coefficients,
    fetching_kernel_coefficients,
    raw_increment_lengths,
    logarithmic_fading_speeds,
    token_fading_spikes,
    absorber_score_vector,
    cluster_scaling_factor,
    final_mapping_matrix,
):
    rows = asking_matrix.shape[0]
    me = lax.axis_index("sp")
    side = lax.axis_index("tp")
    count = lax.axis_size("sp")
    tps = lax.axis_size("tp")
    cols = duality_source_matrix.shape[1]
    wide = storing_direction_matrix.shape[1]
    heads = cols // SSD_HEAD
    core = (me & 1).astype(jnp.int32).reshape(1)
    sds = jax.ShapeDtypeStruct

    raw = (duality_source_matrix, storing_direction_matrix, fetching_direction_matrix)
    tail = jnp.concatenate([a[rows - EDGE :] for a in raw], axis=1)
    lead = jnp.concatenate([a[:EDGE] for a in raw], axis=1)
    prev_edge = shift(tail, count, 1)
    next_edge = shift(lead, count, -1)
    pairs = jnp.concatenate([matching_key_matrix, carried_value_matrix], axis=1)
    prev_pair = shift(pairs, count, 1)
    next_pair = shift(pairs, count, -1)

    shards = {0: final_mapping_matrix}
    bits = []
    bit = count // 2
    while bit >= 2:
        bits.append(bit)
        bit //= 2
    for bit in bits:
        for mask in list(shards):
            shards[mask ^ bit] = flip(shards[mask], count, bit)

    keep, send, read, inner, expl = call(
        block_kernel,
        [
            sds((2 * STATE + EDGE, cols // 2), BF16),
            sds((2 * STATE + EDGE, cols // 2), BF16),
            sds((rows, wide), BF16),
            sds((rows, cols), F32),
            sds((rows, 2 * heads), F32),
        ],
        [
            core,
            *raw,
            prev_edge,
            next_edge,
            duality_kernel_coefficients,
            storing_kernel_coefficients,
            fetching_kernel_coefficients,
            raw_increment_lengths.reshape(2 * heads, rows),
            logarithmic_fading_speeds.reshape(2 * heads, 1),
            token_fading_spikes.reshape(2 * heads, rows),
        ],
        flops=4 * 10**9,
        scratch=[
            pltpu.VMEM((rows + 2 * EDGE, max(cols, wide)), F32),
            pltpu.VMEM((rows, cols), BF16),
            pltpu.VMEM((rows, wide), BF16),
        ],
        name="block",
    )
    own_state, got_state = exchange_states(keep, send, count, me)

    halfway = HEAD // 2
    spacing = ROTARY_BASE ** (-jnp.arange(halfway, dtype=F32) * 2.0 / HEAD)
    places = ((me - 1) * rows + jnp.arange(3 * rows, dtype=jnp.int32)).astype(F32)
    angles = places[:, None] * spacing[None, :]
    cosine = jnp.cos(angles)
    sine = jnp.sin(angles)
    cosine = jnp.concatenate([cosine, cosine], axis=1)
    sine = jnp.concatenate([-sine, sine], axis=1)
    where = jnp.stack([me, jnp.int32(count)]).astype(jnp.int32)
    (attended,) = call(
        attend_kernel,
        [sds(asking_matrix.shape, BF16)],
        [
            where,
            absorber_score_vector,
            asking_matrix,
            matching_key_matrix,
            carried_value_matrix,
            prev_pair,
            next_pair,
            cosine,
            sine,
        ],
        flops=3 * 10**9,
        scalars=2,
        name="attend",
    )
    attended_pair = flip(attended, count, 1)

    (normed,) = call(
        finish_kernel,
        [sds((rows, cols), BF16)],
        [
            core,
            inner,
            read,
            expl,
            own_state,
            got_state,
            silu_switch_argument,
            cluster_scaling_factor.reshape(1, cols),
        ],
        flops=3 * 10**9,
        name="finish",
    )
    normed_pair = flip(normed, count, 1)

    masks = list(shards)
    span = final_mapping_matrix.shape[2]
    if tps == 2 and span % 128 == 0:
        cut = len(masks) - max(1, len(masks) // 4)
        groups = [masks[:cut], masks[cut:]]
        pieces = []
        diag = [(2 * i + j, 2 * (i ^ 1) + 1 - j) for i in range(count) for j in range(2)]
        for group in groups:
            width = span * len(group)
            outs = call(
                functools.partial(project_kernel, len(group)),
                [sds((rows // 2, width), BF16)] * 4,
                [
                    side.astype(jnp.int32).reshape(1),
                    attended,
                    attended_pair,
                    normed,
                    normed_pair,
                    *[shards[m] for m in group],
                ],
                flops=4 * 10**8 * len(group),
                name="project",
            )
            pieces += [
                outs[0],
                lax.ppermute(outs[1], "tp", [(0, 1), (1, 0)]),
                flip(outs[2], count, 1),
                lax.ppermute(outs[3], ("sp", "tp"), diag),
            ]
        order = []
        for m in masks:
            order += [me ^ m, me ^ 1 ^ m]
        (out,) = call(
            functools.partial(place_kernel, groups, span),
            [sds((rows // 2, span * count), BF16)],
            [jnp.stack(order).astype(jnp.int32), *pieces],
            flops=10**6,
            name="place",
        )
        return out

    left = jnp.concatenate(
        [
            jnp.concatenate([attended, normed], axis=1),
            jnp.concatenate([attended_pair, normed_pair], axis=1),
        ],
        axis=0,
    )
    stacked = jnp.concatenate([shards[m] for m in masks], axis=2).reshape(
        -1, span * len(masks)
    )
    partial = jnp.dot(left, stacked, preferred_element_type=F32).astype(BF16)
    partial = partial.reshape(2, tps, rows // tps, -1)
    summed = lax.psum_scatter(partial, "tp", scatter_dimension=1, tiled=True)
    summed = summed.reshape(2, rows // tps, len(masks), span)
    own, away = summed[0], flip(summed[1], count, 1)
    full = [None] * count
    for j, m in enumerate(masks):
        full[m] = own[:, j]
        full[m ^ 1] = away[:, j]
    full = jnp.stack(full, axis=0)
    bit = 1
    while bit < count:
        seen = full.reshape(count // (2 * bit), 2, bit, rows // tps, span)
        full = jnp.where((me & bit) != 0, seen[:, ::-1], seen).reshape(full.shape)
        bit *= 2
    return jnp.moveaxis(full, 0, 1).reshape(rows // tps, count * span)


def solution(mesh):
    in_specs = (
        P("sp", "tp"),
        P("sp", "tp"),
        P("sp", "tp"),
        P("sp", "tp"),
        P("sp", "tp"),
        P("sp", "tp"),
        P("sp", "tp"),
        P(None, "tp"),
        P(None, "tp"),
        P(None, "tp"),
        P(None, "tp", "sp"),
        P(None, "tp"),
        P(None, "tp", "sp"),
        P("tp"),
        P("tp"),
        P(None, "tp", "sp"),
    )
    out_specs = P(("sp", "tp"), None)
    return jax.shard_map(local, mesh=mesh, in_specs=in_specs, out_specs=out_specs, check_vma=False)
```

time: 353 us -> 217 us (0.61)
  waiting for transfers between devices: 221 us -> 140 us
  blocking collectives: 42.9 us -> 0 us
  Pallas kernels: 0 us -> 28.6 us
  other arithmetic: 26 us -> 6.01 us
  matrix products: 18.1 us -> 0 us
  starting transfers between devices: 16.2 us -> 31 us
  between operations: 13.9 us -> 0.35 us
  local copies, waits for them, and re-layouts: 12.8 us -> 6.84 us
    all_gather x3 -> x0, waiting for transfers between devices: 200 us -> none  [the longest x1 126 us: local(): lax.all_gather(final_mapping_matrix, 'sp', axis=2, tiled=True)]
    ppermute x4 -> x24, waiting for transfers between devices: 1.84 us -> 140 us  [the longest x16 135 us: flip(): return lax.ppermute(a, 'sp', [(i, i ^ mask) for i in range(count)])]
    all_gather x2 -> x0, blocking collectives: 42.9 us -> none  [entering_2(): gathered = jax.tree.map(lambda a: lax.all_gather(a, axis), part)]
    pallas_call x0 -> x6, Pallas kernels: none -> 28.6 us  [call(): pl.pallas_call(kernel, out_shape=outs, in_specs=[SMEM] * scalars + [VMEM]...]
    reduce_scatter x1 -> x0, waiting for transfers between devices: 18.7 us -> none  [local(): lax.psum_scatter(jnp.dot(mixed_rows, stacked, preferred_element_type=jnp....]
    dot_general x11 -> x0, matrix products: 18.1 us -> none  [the longest x1 9.08 us: local(): jnp.dot(mixed_rows, stacked, preferred_element_type=jnp.float32)]
    add x16 -> x0, other arithmetic: 18 us -> none  [the longest x15 17.9 us: linked(): earlier[1] * later[0][..., None, None] + later[1]]
    ppermute x4 -> x24, starting transfers between devices: 16 us -> 31 us  [the longest x16 19.7 us: flip(): return lax.ppermute(a, 'sp', [(i, i ^ mask) for i in range(count)])]
  transfers between devices with their start and end apart: 8 -> 24, of which waited for: 5 -> 10; matrix products, arithmetic and copies ran while one was open for 11% -> 3% of each run, Pallas kernels for 0% -> 10%
where the time goes in v1:
time: 217 us; the launch traced here: 213 us
  waiting for transfers between devices  140 us (65%)
  starting transfers between devices  31 us (14%)
  Pallas kernels  28.6 us (13%)
  local copies, waits for them, and re-layouts  6.84 us (3%)
  other arithmetic  6.01 us (3%)
    ppermute x16, waiting for transfers between devices, flip(): return lax.ppermute(a, 'sp', [(i, i ^ mask) for i in range(count)])  135 us
    pallas_call x6, Pallas kernels, call(): pl.pallas_call(kernel, out_shape=outs, in_specs=[SMEM] * scalars + [VMEM]...  28.6 us
    ppermute x16, starting transfers between devices, flip(): return lax.ppermute(a, 'sp', [(i, i ^ mask) for i in range(count)])  19.7 us
    ppermute x4, starting transfers between devices, shift(): lax.ppermute(a, 'sp', [(i, i + by) for i in range(count) if 0 <= i + by <...  7 us
  transfers between devices with their start and end apart: 24, of which 10 were waited for; matrix products, arithmetic and copies ran while one was open for 3% of the time, Pallas kernels for 10%

profile of v1, /device:TPU:0, one launch (start us, length us, event | category | flops | bytes accessed | tf_op | source)
XLA Modules:
  0.0 212.9 jit_solution(6758468210278541754)
XLA Ops:
  1.6 2.4 %collective-permute-start.3 = (bf16[16,2048]{1,0:T(8,128)(2,1)S(1)}, bf16[16,2048]{1,0:T(8,128)(2,1)S(1)}, u32[]{:S(2)}, u32[]{:S(2)}) collective-permute-start(bf16[16,2048]{1,0:T(8,128)(2,1)S(1)} %pad_maximum_fusion.4), channel_id=1, source_target_pairs={{0,2},{2,4},{4,6},{6,8},{8,10},{10,12},{12,14},{14,16},{16,18},{18... | collective-permute-start | bytes 196616 | tf_op jit(solution)/shard_map/ppermute | solution.py:319
  4.0 1.3 collective-permute-start.4
  6.7 2.6 %collective-permute-done.4.next_ref = bf16[16,2048]{1,0:T(8,128)(2,1)S(1)} collective-permute-done((bf16[16,2048]{1,0:T(8,128)(2,1)S(1)}, bf16[16,2048]{1,0:T(8,128)(2,1)S(1)}, u32[]{:S(2)}, u32[]{:S(2)}) %collective-permute-start.4) | collective-permute-done | bytes 65568 | tf_op jit(solution)/shard_map/ppermute | solution.py:319
  9.9 5.9 %block.1 = (bf16[272,512]{1,0:T(8,128)(2,1)}, bf16[272,512]{1,0:T(8,128)(2,1)}, bf16[128,512]{1,0:T(8,128)(2,1)}, f32[128,1024]{1,0:T(8,128)}, f32[128,32]{1,0:T(8,128)}) custom-call(s32[1]{0:T(128)} %bitcast.17.place, bf16[128,1024]{1,0:T(8,128)(2,1)} %x_ref.1, bf16[128,512]{1,0:T(8,128)(2,1)} %w_ref.1, bf16[128,512]{1,0:T(8,128)(2,1)} %r_ref.1, ...), custom_call_target="tpu_custom_call" | custom-call | flops 4000000000 | bytes 1937540 | tf_op jit(solution)/shard_map/block/pallas_call | solution.py:28
  15.7 2.9 %collective-permute-start.5 = (bf16[272,512]{1,0:T(8,128)(2,1)}, bf16[272,512]{1,0:T(8,128)(2,1)S(1)}, u32[]{:S(2)}, u32[]{:S(2)}) collective-permute-start(bf16[272,512]{1,0:T(8,128)(2,1)} %get-tuple-element.21), channel_id=1, source_target_pairs={{0,2},{2,0},{4,6},{6,4},{8,10},{10,8},{12,14},{14,12},{16,18},{18,... | collective-permute-start | bytes 835592 | tf_op jit(solution)/shard_map/ppermute | solution.py:315
  21.5 2.5 %collective-permute-start.6 = (bf16[272,512]{1,0:T(8,128)(2,1)S(1)}, bf16[272,512]{1,0:T(8,128)(2,1)S(1)}, u32[]{:S(2)}, u32[]{:S(2)}) collective-permute-start(bf16[272,512]{1,0:T(8,128)(2,1)S(1)} %concatenate.41), channel_id=1, source_target_pairs={{0,4},{2,6},{4,0},{6,2},{8,12},{10,14},{12,8},{14,10},{16,20},{18,... | collective-permute-start | bytes 835592 | tf_op jit(solution)/shard_map/ppermute | solution.py:315
  24.0 2.0 collective-permute-start
  27.3 5.8 %collective-permute-start.11 = (bf16[2,1024,256]{2,1,0:T(8,128)(2,1)}, bf16[2,1024,256]{2,1,0:T(8,128)(2,1)}, u32[]{:S(2)}, u32[]{:S(2)}) collective-permute-start(bf16[2,1024,256]{2,1,0:T(8,128)(2,1)} %refs_0_.1), channel_id=1, source_target_pairs={{0,16},{2,18},{4,20},{6,22},{8,24},{10,26},{12,28},{14,30},{16,0},... | collective-permute-start | bytes 3145736 | tf_op jit(solution)/shard_map/ppermute | solution.py:315
  33.6 2.4 %collective-permute-start.7 = (bf16[272,512]{1,0:T(8,128)(2,1)S(1)}, bf16[272,512]{1,0:T(8,128)(2,1)S(1)}, u32[]{:S(2)}, u32[]{:S(2)}) collective-permute-start(bf16[272,512]{1,0:T(8,128)(2,1)S(1)} %concatenate.43), channel_id=1, source_target_pairs={{0,8},{2,10},{4,12},{6,14},{8,0},{10,2},{12,4},{14,6},{16,24},{18,... | collective-permute-start | bytes 835592 | tf_op jit(solution)/shard_map/ppermute | solution.py:315
  36.8 49.3 %collective-permute-done.7 = bf16[272,512]{1,0:T(8,128)(2,1)S(1)} collective-permute-done((bf16[272,512]{1,0:T(8,128)(2,1)S(1)}, bf16[272,512]{1,0:T(8,128)(2,1)S(1)}, u32[]{:S(2)}, u32[]{:S(2)}) %collective-permute-start.7) | collective-permute-done | bytes 278560 | tf_op jit(solution)/shard_map/ppermute | solution.py:315
  86.6 1.7 collective-permute-start.8
  89.8 19.9 %collective-permute-done.8 = bf16[128,512]{1,0:T(8,128)(2,1)S(1)} collective-permute-done((bf16[128,512]{1,0:T(8,128)(2,1)S(1)}, bf16[128,512]{1,0:T(8,128)(2,1)S(1)}, u32[]{:S(2)}, u32[]{:S(2)}) %collective-permute-start.8) | collective-permute-done | bytes 131104 | tf_op jit(solution)/shard_map/ppermute | solution.py:315
  115.2 5.1 %attend.1.a_ref = bf16[128,1024]{1,0:T(8,128)(2,1)} custom-call(s32[2]{0:T(128)} %pad_add_fusion.place, f32[8]{0:T(128)} %sink.1, bf16[128,1024]{1,0:T(8,128)(2,1)} %q_ref.1, bf16[128,512]{1,0:T(8,128)(2,1)} %k_ref.1, bf16[128,512]{1,0:T(8,128)(2,1)} %v_ref.1, bf16[128,1024]{1,0:T(8,128)(2,1)} %copy-done.14, bf16[128,1024]{1,0:T(8,128)(2,1)} %copy-done.15, ...), custom_call_target="tpu_custom_call" | custom-call | flops 3000000000 | bytes 1703976 | tf_op jit(solution)/shard_map/attend/pallas_call | solution.py:28
  121.0 3.3 %finish.1.n_ref = bf16[128,1024]{1,0:T(8,128)(2,1)} custom-call(s32[1]{0:T(128)} %bitcast.17.place, f32[128,1024]{1,0:T(8,128)} %get-tuple-element.18.y_ref, bf16[128,512]{1,0:T(8,128)(2,1)} %get-tuple-element.19.read_ref, f32[128,32]{1,0:T(8,128)} %get-tuple-element.20.expl_ref, bf16[256,512]{1,0:T(8,128)(2,1)} %get-tuple-element.56.own_ref, ...), custom_call_target="tpu_custom_call" | custom-call | flops 3000000000 | bytes 1724420 | tf_op jit(solution)/shard_map/finish/pallas_call | solution.py:28
  124.3 11.7 %collective-permute-done.14.refs_4_ = bf16[2,1024,256]{2,1,0:T(8,128)(2,1)} collective-permute-done((bf16[2,1024,256]{2,1,0:T(8,128)(2,1)}, bf16[2,1024,256]{2,1,0:T(8,128)(2,1)}, u32[]{:S(2)}, u32[]{:S(2)}) %collective-permute-start.14) | collective-permute-done | bytes 1048608 | tf_op jit(solution)/shard_map/ppermute | solution.py:315
  136.0 22.5 %collective-permute-done.15.refs_5_ = bf16[2,1024,256]{2,1,0:T(8,128)(2,1)} collective-permute-done((bf16[2,1024,256]{2,1,0:T(8,128)(2,1)}, bf16[2,1024,256]{2,1,0:T(8,128)(2,1)}, u32[]{:S(2)}, u32[]{:S(2)}) %collective-permute-start.15) | collective-permute-done | bytes 1048608 | tf_op jit(solution)/shard_map/ppermute | solution.py:315
  158.5 8.2 %project.2 = (bf16[64,1536]{1,0:T(8,128)(2,1)}, bf16[64,1536]{1,0:T(8,128)(2,1)}, bf16[64,1536]{1,0:T(8,128)(2,1)}, bf16[64,1536]{1,0:T(8,128)(2,1)}) custom-call(s32[1]{0:T(128)} %bitcast.16.place, bf16[128,1024]{1,0:T(8,128)(2,1)} %attend.1.a_ref, bf16[128,1024]{1,0:T(8,128)(2,1)} %copy-done.3, bf16[128,1024]{1,0:T(8,128)(2,1)} %finish.1.n_ref, ...), custom_call_target="tpu_custom_call" | custom-call | flops 2400000000 | bytes 8126468 | tf_op jit(solution)/shard_map/project/pallas_call | solution.py:28
  166.7 1.5 collective-permute-start.16
  168.8 12.0 %collective-permute-done.19.refs_0_ = bf16[2,1024,256]{2,1,0:T(8,128)(2,1)S(1)} collective-permute-done((bf16[2,1024,256]{2,1,0:T(8,128)(2,1)}, bf16[2,1024,256]{2,1,0:T(8,128)(2,1)S(1)}, u32[]{:S(2)}, u32[]{:S(2)}) %collective-permute-start.19) | collective-permute-done | bytes 1048608 | tf_op jit(solution)/shard_map/ppermute | solution.py:315
  180.9 18.8 %collective-permute-done.20.refs_1_ = bf16[2,1024,256]{2,1,0:T(8,128)(2,1)S(1)} collective-permute-done((bf16[2,1024,256]{2,1,0:T(8,128)(2,1)}, bf16[2,1024,256]{2,1,0:T(8,128)(2,1)S(1)}, u32[]{:S(2)}, u32[]{:S(2)}) %collective-permute-start.20) | collective-permute-done | bytes 1048608 | tf_op jit(solution)/shard_map/ppermute | solution.py:315
  200.6 4.0 %project.3 = (bf16[64,512]{1,0:T(8,128)(2,1)}, bf16[64,512]{1,0:T(8,128)(2,1)}, bf16[64,512]{1,0:T(8,128)(2,1)}, bf16[64,512]{1,0:T(8,128)(2,1)}) custom-call(s32[1]{0:T(128)} %bitcast.16.place, bf16[128,1024]{1,0:T(8,128)(2,1)} %attend.1.a_ref, bf16[128,1024]{1,0:T(8,128)(2,1)} %copy-done.3, bf16[128,1024]{1,0:T(8,128)(2,1)} %finish.1.n_ref, ...), custom_call_target="tpu_custom_call" | custom-call | flops 800000000 | bytes 3407876 | tf_op jit(solution)/shard_map/project/pallas_call | solution.py:28
  204.6 1.5 collective-permute-start.21
  207.4 1.6 collective-permute-done.21.refs_5_
  210.8 2.2 %place.1 = bf16[64,4096]{1,0:T(8,128)(2,1)} custom-call(s32[16]{0:T(128)} %stack.71.place, bf16[64,1536]{1,0:T(8,128)(2,1)} %get-tuple-element.23.refs_0_, bf16[64,1536]{1,0:T(8,128)(2,1)} %copy-done.5, bf16[64,1536]{1,0:T(8,128)(2,1)} %copy-done.6, bf16[64,1536]{1,0:T(8,128)(2,1)} %copy-done.7, bf16[64,512]{1,0:T(8,128)(2,1)} %get-tuple-element.27.refs_4_, ...), custom_call_target="tpu_custom_call" | custom-call | flops 1000000 | bytes 1572928 | tf_op jit(solution)/shard_map/place/pallas_call | solution.py:28
  (101 shorter events, 21.5 us)
Async XLA Ops:
  1.6 5.1 %collective-permute-start.3 = (bf16[16,2048]{1,0:T(8,128)(2,1)S(1)}, bf16[16,2048]{1,0:T(8,128)(2,1)S(1)}, u32[]{:S(2)}, u32[]{:S(2)}) collective-permute-start(bf16[16,2048]{1,0:T(8,128)(2,1)S(1)} %pad_maximum_fusion.4), channel_id=1, source_target_pairs={{0,2},{2,4},{4,6},{6,8},{8,10},{10,12},{12,14},{14,16},{16,18},{18... | collective-permute-start | bytes 196616 | tf_op jit(solution)/shard_map/ppermute | solution.py:319
  4.0 5.3 %collective-permute-start.4 = (bf16[16,2048]{1,0:T(8,128)(2,1)S(1)}, bf16[16,2048]{1,0:T(8,128)(2,1)S(1)}, u32[]{:S(2)}, u32[]{:S(2)}) collective-permute-start(bf16[16,2048]{1,0:T(8,128)(2,1)S(1)} %pad_maximum_fusion.5), channel_id=1, source_target_pairs={{2,0},{4,2},{6,4},{8,6},{10,8},{12,10},{14,12},{16,14},{18,16},{20... | collective-permute-start | bytes 196616 | tf_op jit(solution)/shard_map/ppermute | solution.py:319
  15.7 4.3 %collective-permute-start.5 = (bf16[272,512]{1,0:T(8,128)(2,1)}, bf16[272,512]{1,0:T(8,128)(2,1)S(1)}, u32[]{:S(2)}, u32[]{:S(2)}) collective-permute-start(bf16[272,512]{1,0:T(8,128)(2,1)} %get-tuple-element.21), channel_id=1, source_target_pairs={{0,2},{2,0},{4,6},{6,4},{8,10},{10,8},{12,14},{14,12},{16,18},{18,... | collective-permute-start | bytes 835592 | tf_op jit(solution)/shard_map/ppermute | solution.py:315
  21.5 11.7 %collective-permute-start.6 = (bf16[272,512]{1,0:T(8,128)(2,1)S(1)}, bf16[272,512]{1,0:T(8,128)(2,1)S(1)}, u32[]{:S(2)}, u32[]{:S(2)}) collective-permute-start(bf16[272,512]{1,0:T(8,128)(2,1)S(1)} %concatenate.41), channel_id=1, source_target_pairs={{0,4},{2,6},{4,0},{6,2},{8,12},{10,14},{12,8},{14,10},{16,20},{18,... | collective-permute-start | bytes 835592 | tf_op jit(solution)/shard_map/ppermute | solution.py:315
  24.0 86.8 %collective-permute-start = (bf16[128,1024]{1,0:T(8,128)(2,1)S(1)}, bf16[128,1024]{1,0:T(8,128)(2,1)S(1)}, u32[]{:S(2)}, u32[]{:S(2)}) collective-permute-start(bf16[128,1024]{1,0:T(8,128)(2,1)S(1)} %constant_dynamic-update-slice_fusion), channel_id=1, source_target_pairs={{0,2},{2,4},{4,6},{6,8},{8,10},{10,12},{12,14},{14,16},{16,18},{18... | collective-permute-start | bytes 786440 | tf_op jit(solution)/shard_map/ppermute | solution.py:319
  26.0 87.1 %collective-permute-start.1 = (bf16[128,1024]{1,0:T(8,128)(2,1)S(1)}, bf16[128,1024]{1,0:T(8,128)(2,1)S(1)}, u32[]{:S(2)}, u32[]{:S(2)}) collective-permute-start(bf16[128,1024]{1,0:T(8,128)(2,1)S(1)} %constant_dynamic-update-slice_fusion), channel_id=1, source_target_pairs={{2,0},{4,2},{6,4},{8,6},{10,8},{12,10},{14,12},{16,14},{18,16},{20... | collective-permute-start | bytes 786440 | tf_op jit(solution)/shard_map/ppermute | solution.py:319
  27.3 58.9 %collective-permute-start.11 = (bf16[2,1024,256]{2,1,0:T(8,128)(2,1)}, bf16[2,1024,256]{2,1,0:T(8,128)(2,1)}, u32[]{:S(2)}, u32[]{:S(2)}) collective-permute-start(bf16[2,1024,256]{2,1,0:T(8,128)(2,1)} %refs_0_.1), channel_id=1, source_target_pairs={{0,16},{2,18},{4,20},{6,22},{8,24},{10,26},{12,28},{14,30},{16,0},... | collective-permute-start | bytes 3145736 | tf_op jit(solution)/shard_map/ppermute | solution.py:315
  33.1 80.0 %collective-permute-start.12 = (bf16[2,1024,256]{2,1,0:T(8,128)(2,1)}, bf16[2,1024,256]{2,1,0:T(8,128)(2,1)}, u32[]{:S(2)}, u32[]{:S(2)}) collective-permute-start(bf16[2,1024,256]{2,1,0:T(8,128)(2,1)} %refs_0_.1), channel_id=1, source_target_pairs={{0,8},{2,10},{4,12},{6,14},{8,0},{10,2},{12,4},{14,6},{16,24},{18,... | collective-permute-start | bytes 3145736 | tf_op jit(solution)/shard_map/ppermute | solution.py:315
  33.6 52.6 %collective-permute-start.7 = (bf16[272,512]{1,0:T(8,128)(2,1)S(1)}, bf16[272,512]{1,0:T(8,128)(2,1)S(1)}, u32[]{:S(2)}, u32[]{:S(2)}) collective-permute-start(bf16[272,512]{1,0:T(8,128)(2,1)S(1)} %concatenate.43), channel_id=1, source_target_pairs={{0,8},{2,10},{4,12},{6,14},{8,0},{10,2},{12,4},{14,6},{16,24},{18,... | collective-permute-start | bytes 835592 | tf_op jit(solution)/shard_map/ppermute | solution.py:315
  86.2 27.8 %collective-permute-start.13 = (bf16[2,1024,256]{2,1,0:T(8,128)(2,1)}, bf16[2,1024,256]{2,1,0:T(8,128)(2,1)}, u32[]{:S(2)}, u32[]{:S(2)}) collective-permute-start(bf16[2,1024,256]{2,1,0:T(8,128)(2,1)} %collective-permute-done.11.refs_1_), channel_id=1, source_target_pairs={{0,8},{2,10},{4,12},{6,14},{8,0},{10,2},{12,4},{14,6},{16,24},{18,... | collective-permute-start | bytes 3145736 | tf_op jit(solution)/shard_map/ppermute | solution.py:315
  86.6 23.1 %collective-permute-start.8 = (bf16[128,512]{1,0:T(8,128)(2,1)S(1)}, bf16[128,512]{1,0:T(8,128)(2,1)S(1)}, u32[]{:S(2)}, u32[]{:S(2)}) collective-permute-start(bf16[128,512]{1,0:T(8,128)(2,1)S(1)} %fusion.9), channel_id=1, source_target_pairs={{0,16},{2,18},{4,20},{6,22},{8,24},{10,26},{12,28},{14,30},{16,0},... | collective-permute-start | bytes 393224 | tf_op jit(solution)/shard_map/ppermute | solution.py:315
  109.7 26.3 %collective-permute-start.14 = (bf16[2,1024,256]{2,1,0:T(8,128)(2,1)}, bf16[2,1024,256]{2,1,0:T(8,128)(2,1)}, u32[]{:S(2)}, u32[]{:S(2)}) collective-permute-start(bf16[2,1024,256]{2,1,0:T(8,128)(2,1)} %refs_0_.1), channel_id=1, source_target_pairs={{0,4},{2,6},{4,0},{6,2},{8,12},{10,14},{12,8},{14,10},{16,20},{18,... | collective-permute-start | bytes 3145736 | tf_op jit(solution)/shard_map/ppermute | solution.py:315
  110.8 47.7 %collective-permute-start.15 = (bf16[2,1024,256]{2,1,0:T(8,128)(2,1)}, bf16[2,1024,256]{2,1,0:T(8,128)(2,1)}, u32[]{:S(2)}, u32[]{:S(2)}) collective-permute-start(bf16[2,1024,256]{2,1,0:T(8,128)(2,1)} %collective-permute-done.11.refs_1_), channel_id=1, source_target_pairs={{0,4},{2,6},{4,0},{6,2},{8,12},{10,14},{12,8},{14,10},{16,20},{18,... | collective-permute-start | bytes 3145736 | tf_op jit(solution)/shard_map/ppermute | solution.py:315
  113.1 7.2 %collective-permute-start.9 = (bf16[256,512]{1,0:T(8,128)(2,1)S(1)}, bf16[256,512]{1,0:T(8,128)(2,1)S(1)}, u32[]{:S(2)}, u32[]{:S(2)}) collective-permute-start(bf16[256,512]{1,0:T(8,128)(2,1)S(1)} %get-tuple-element.55), channel_id=1, source_target_pairs={{0,2},{2,0},{4,6},{6,4},{8,10},{10,8},{12,14},{14,12},{16,18},{18,... | collective-permute-start | bytes 786440 | tf_op jit(solution)/shard_map/ppermute | solution.py:315
  113.1 67.8 %collective-permute-start.19 = (bf16[2,1024,256]{2,1,0:T(8,128)(2,1)}, bf16[2,1024,256]{2,1,0:T(8,128)(2,1)S(1)}, u32[]{:S(2)}, u32[]{:S(2)}) collective-permute-start(bf16[2,1024,256]{2,1,0:T(8,128)(2,1)} %collective-permute-done.12.refs_2_), channel_id=1, source_target_pairs={{0,4},{2,6},{4,0},{6,2},{8,12},{10,14},{12,8},{14,10},{16,20},{18,... | collective-permute-start | bytes 3145736 | tf_op jit(solution)/shard_map/ppermute | solution.py:315
  114.0 85.7 %collective-permute-start.20 = (bf16[2,1024,256]{2,1,0:T(8,128)(2,1)}, bf16[2,1024,256]{2,1,0:T(8,128)(2,1)S(1)}, u32[]{:S(2)}, u32[]{:S(2)}) collective-permute-start(bf16[2,1024,256]{2,1,0:T(8,128)(2,1)} %collective-permute-done.13.refs_3_), channel_id=1, source_target_pairs={{0,4},{2,6},{4,0},{6,2},{8,12},{10,14},{12,8},{14,10},{16,20},{18,... | collective-permute-start | bytes 3145736 | tf_op jit(solution)/shard_map/ppermute | solution.py:315
  120.3 4.0 %collective-permute-start.2 = (bf16[128,1024]{1,0:T(8,128)(2,1)}, bf16[128,1024]{1,0:T(8,128)(2,1)S(1)}, u32[]{:S(2)}, u32[]{:S(2)}) collective-permute-start(bf16[128,1024]{1,0:T(8,128)(2,1)} %attend.1.a_ref), channel_id=1, source_target_pairs={{0,2},{2,0},{4,6},{6,4},{8,10},{10,8},{12,14},{14,12},{16,18},{18,... | collective-permute-start | bytes 786440 | tf_op jit(solution)/shard_map/ppermute | solution.py:315
  124.3 11.7 %collective-permute-start.10 = (bf16[128,1024]{1,0:T(8,128)(2,1)}, bf16[128,1024]{1,0:T(8,128)(2,1)S(1)}, u32[]{:S(2)}, u32[]{:S(2)}) collective-permute-start(bf16[128,1024]{1,0:T(8,128)(2,1)} %finish.1.n_ref), channel_id=1, source_target_pairs={{0,2},{2,0},{4,6},{6,4},{8,10},{10,8},{12,14},{14,12},{16,18},{18,... | collective-permute-start | bytes 786440 | tf_op jit(solution)/shard_map/ppermute | solution.py:315
  166.7 39.4 %collective-permute-start.16 = (bf16[64,1536]{1,0:T(8,128)(2,1)}, bf16[64,1536]{1,0:T(8,128)(2,1)S(1)}, u32[]{:S(2)}, u32[]{:S(2)}) collective-permute-start(bf16[64,1536]{1,0:T(8,128)(2,1)} %get-tuple-element.24), channel_id=1, source_target_pairs={{0,1},{1,0},{2,3},{3,2},{4,5},{5,4},{6,7},{7,6},{8,9},{9,8},{10,11... | collective-permute-start | bytes 589832 | tf_op jit(solution)/shard_map/ppermute | solution.py:546
  168.2 39.2 %collective-permute-start.17 = (bf16[64,1536]{1,0:T(8,128)(2,1)}, bf16[64,1536]{1,0:T(8,128)(2,1)S(1)}, u32[]{:S(2)}, u32[]{:S(2)}) collective-permute-start(bf16[64,1536]{1,0:T(8,128)(2,1)} %get-tuple-element.25), channel_id=1, source_target_pairs={{0,2},{2,0},{4,6},{6,4},{8,10},{10,8},{12,14},{14,12},{16,18},{18,... | collective-permute-start | bytes 589832 | tf_op jit(solution)/shard_map/ppermute | solution.py:315
  168.2 39.2 %collective-permute-start.18 = (bf16[64,1536]{1,0:T(8,128)(2,1)}, bf16[64,1536]{1,0:T(8,128)(2,1)S(1)}, u32[]{:S(2)}, u32[]{:S(2)}) collective-permute-start(bf16[64,1536]{1,0:T(8,128)(2,1)} %get-tuple-element.26), channel_id=1, source_target_pairs={{0,3},{1,2},{2,1},{3,0},{4,7},{5,6},{6,5},{7,4},{8,11},{9,10},{10,... | collective-permute-start | bytes 589832 | tf_op jit(solution)/shard_map/ppermute | solution.py:548
  204.6 4.5 %collective-permute-start.21 = (bf16[64,512]{1,0:T(8,128)(2,1)}, bf16[64,512]{1,0:T(8,128)(2,1)S(1)}, u32[]{:S(2)}, u32[]{:S(2)}) collective-permute-start(bf16[64,512]{1,0:T(8,128)(2,1)} %get-tuple-element.28), channel_id=1, source_target_pairs={{0,1},{1,0},{2,3},{3,2},{4,5},{5,4},{6,7},{7,6},{8,9},{9,8},{10,11... | collective-permute-start | bytes 196616 | tf_op jit(solution)/shard_map/ppermute | solution.py:546
  206.1 3.0 %collective-permute-start.22 = (bf16[64,512]{1,0:T(8,128)(2,1)}, bf16[64,512]{1,0:T(8,128)(2,1)S(1)}, u32[]{:S(2)}, u32[]{:S(2)}) collective-permute-start(bf16[64,512]{1,0:T(8,128)(2,1)} %get-tuple-element.29), channel_id=1, source_target_pairs={{0,2},{2,0},{4,6},{6,4},{8,10},{10,8},{12,14},{14,12},{16,18},{18,... | collective-permute-start | bytes 196616 | tf_op jit(solution)/shard_map/ppermute | solution.py:315
  206.1 4.0 %collective-permute-start.23 = (bf16[64,512]{1,0:T(8,128)(2,1)}, bf16[64,512]{1,0:T(8,128)(2,1)S(1)}, u32[]{:S(2)}, u32[]{:S(2)}) collective-permute-start(bf16[64,512]{1,0:T(8,128)(2,1)} %get-tuple-element.30), channel_id=1, source_target_pairs={{0,3},{1,2},{2,1},{3,0},{4,7},{5,6},{6,5},{7,4},{8,11},{9,10},{10,... | collective-permute-start | bytes 196616 | tf_op jit(solution)/shard_map/ppermute | solution.py:548
  (19 other events, 114.1 us)

commit v2 on v1

--- a/solution.py
+++ b/solution.py
@@ -6,6 +6,7 @@
 from jax.experimental import pallas as pl
 from jax.experimental.pallas import tpu as pltpu
 from jax.sharding import PartitionSpec as P
+
 
 HEAD = 128
 SSD_HEAD = 64
@@ -23,7 +24,7 @@
 SMEM = pl.BlockSpec(memory_space=pltpu.SMEM)
 
 
-def call(kernel, outs, ins, flops, scratch=(), scalars=1, name=None):
+def call(kernel, outs, ins, flops, scratch=(), scalars=1):
     moved = sum(a.size * a.dtype.itemsize for a in list(ins) + list(outs))
     return pl.pallas_call(
         kernel,
@@ -32,7 +33,6 @@
         out_specs=[VMEM] * len(outs),
         scratch_shapes=list(scratch),
         cost_estimate=pl.CostEstimate(flops=flops, bytes_accessed=moved, transcendentals=0),
-        name=name,
     )(*ins)
 
 
@@ -232,7 +232,7 @@
 
 
 def finish_kernel(place, y_ref, read_ref, expl_ref, own_ref, got_ref, gate_ref, gain_ref, out_ref):
-    rows, cols = y_ref.shape
+    _, cols = y_ref.shape
     wide = read_ref.shape[1]
     heads = cols // SSD_HEAD
     groups = wide // STATE
@@ -271,43 +271,52 @@
         ).astype(BF16)
 
 
-def project_kernel(count, place, a_ref, ap_ref, n_ref, np_ref, *refs):
-    shards = refs[:count]
-    own_ref, x_ref, c_ref, cx_ref = refs[count:]
-    rows = a_ref.shape[0]
+def first_kernel(count, *refs):
+    lefts = refs[: count[0]]
+    shards = refs[count[0] : count[0] + count[1]]
+    out_ref = refs[-1]
+    left = jnp.concatenate([a[...] for a in lefts], axis=0)
+    at = 0
+    for shard in shards:
+        span = shard.shape[1]
+        out_ref[:, at : at + span] = nn(left, shard[...])
+        at += span
+
+
+def second_kernel(count, place, sum_ref, *refs):
+    lefts = refs[: count[0]]
+    shards = refs[count[0] : count[0] + count[1]]
+    outs = refs[count[0] + count[1] :]
+    rows = lefts[0].shape[0]
     half = rows // 2
-    left = jnp.concatenate([a_ref[...], ap_ref[...]], axis=0)
-    right = jnp.concatenate([n_ref[...], np_ref[...]], axis=0)
-    for j in range(count):
-        span = shards[j].shape[2]
-        at = j * span
-        total = (nn(left, shards[j][0]) + nn(right, shards[j][1])).astype(BF16)
+    left = jnp.concatenate([a[...] for a in lefts], axis=0)
+    at = 0
+    for shard in shards:
+        span = shard.shape[1]
+        total = (sum_ref[:, at : at + span] + nn(left, shard[...])).astype(BF16)
         for side in range(2):
 
             @pl.when(place[0] == side)
             def _():
-                a, b = side * half, (1 - side) * half
-                own_ref[:, at : at + span] = total[a : a + half]
-                x_ref[:, at : at + span] = total[b : b + half]
-                c_ref[:, at : at + span] = total[rows + a : rows + a + half]
-                cx_ref[:, at : at + span] = total[rows + b : rows + b + half]
-
-
-def place_kernel(masks, spans, place, *refs):
+                for i in range(count[0]):
+                    a = i * rows + side * half
+                    b = i * rows + (1 - side) * half
+                    outs[2 * i][:, at : at + span] = total[a : a + half]
+                    outs[2 * i + 1][:, at : at + span] = total[b : b + half]
+
+        at += span
+
+
+def place_kernel(shape, place, *refs):
+    sources, columns, span = shape
     out_ref = refs[-1]
-    for i, group in enumerate(masks):
-        own, x, c, cx = refs[4 * i : 4 * i + 4]
-        span = spans
-        for j, _ in enumerate(group):
-            index = sum(len(m) for m in masks[:i]) + j
+    for i in range(sources):
+        for j in range(columns):
             at = j * span
-            mine = pl.multiple_of(place[2 * index] * span, span)
-            theirs = pl.multiple_of(place[2 * index + 1] * span, span)
-            out_ref[:, pl.ds(mine, span)] = (
-                own[:, at : at + span].astype(F32) + x[:, at : at + span].astype(F32)
-            ).astype(BF16)
-            out_ref[:, pl.ds(theirs, span)] = (
-                c[:, at : at + span].astype(F32) + cx[:, at : at + span].astype(F32)
+            to = pl.multiple_of(place[i * columns + j] * span, span)
+            out_ref[:, pl.ds(to, span)] = (
+                refs[2 * i][:, at : at + span].astype(F32)
+                + refs[2 * i + 1][:, at : at + span].astype(F32)
             ).astype(BF16)
 
 
@@ -318,6 +327,14 @@
 def shift(a, count, by):
     return lax.ppermute(
         a, "sp", [(i, i + by) for i in range(count) if 0 <= i + by < count]
+    )
+
+
+def cross(a, count, mask):
+    return lax.ppermute(
+        a,
+        ("sp", "tp"),
+        [(2 * i + j, 2 * (i ^ mask) + 1 - j) for i in range(count) for j in range(2)],
     )
 
 
@@ -430,15 +447,21 @@
     prev_pair = shift(pairs, count, 1)
     next_pair = shift(pairs, count, -1)
 
-    shards = {0: final_mapping_matrix}
+    span = final_mapping_matrix.shape[2]
+    fast = tps == 2 and span % 128 == 0 and count == 16
+    shared = [1, 4] if fast else [1]
     bits = []
     bit = count // 2
     while bit >= 2:
-        bits.append(bit)
+        if bit not in shared:
+            bits.append(bit)
         bit //= 2
-    for bit in bits:
-        for mask in list(shards):
-            shards[mask ^ bit] = flip(shards[mask], count, bit)
+    halves = [{0: final_mapping_matrix[0]}, {0: final_mapping_matrix[1]}]
+    for shards in halves:
+        for bit in bits:
+            for mask in list(shards):
+                shards[mask ^ bit] = flip(shards[mask], count, bit)
+    masks = list(halves[0])
 
     keep, send, read, inner, expl = call(
         block_kernel,
@@ -467,7 +490,6 @@
             pltpu.VMEM((rows, cols), BF16),
             pltpu.VMEM((rows, wide), BF16),
         ],
-        name="block",
     )
     own_state, got_state = exchange_states(keep, send, count, me)
 
@@ -496,9 +518,15 @@
         ],
         flops=3 * 10**9,
         scalars=2,
-        name="attend",
-    )
-    attended_pair = flip(attended, count, 1)
+    )
+
+    def spread_rows(a):
+        blocks = [a]
+        for bit in reversed(shared):
+            blocks += [flip(b, count, bit) for b in blocks]
+        return blocks
+
+    attended_blocks = spread_rows(attended)
 
     (normed,) = call(
         finish_kernel,
@@ -514,51 +542,48 @@
             cluster_scaling_factor.reshape(1, cols),
         ],
         flops=3 * 10**9,
-        name="finish",
-    )
-    normed_pair = flip(normed, count, 1)
-
-    masks = list(shards)
-    span = final_mapping_matrix.shape[2]
-    if tps == 2 and span % 128 == 0:
-        cut = len(masks) - max(1, len(masks) // 4)
-        groups = [masks[:cut], masks[cut:]]
+    )
+    normed_blocks = spread_rows(normed)
+    if fast:
+        group = [0, 4, 1, 5]
+        width = span * len(masks)
+        sizes = (len(group), len(masks))
+        flops = 2 * len(group) * rows * cols * width
+        (early,) = call(
+            functools.partial(first_kernel, sizes),
+            [sds((len(group) * rows, width), F32)],
+            [*attended_blocks, *[halves[0][m] for m in masks]],
+            flops=flops,
+            scalars=0,
+        )
+        outs = call(
+            functools.partial(second_kernel, sizes),
+            [sds((rows // 2, width), BF16)] * (2 * len(group)),
+            [
+                side.astype(jnp.int32).reshape(1),
+                early,
+                *normed_blocks,
+                *[halves[1][m] for m in masks],
+            ],
+            flops=flops,
+        )
         pieces = []
-        diag = [(2 * i + j, 2 * (i ^ 1) + 1 - j) for i in range(count) for j in range(2)]
-        for group in groups:
-            width = span * len(group)
-            outs = call(
-                functools.partial(project_kernel, len(group)),
-                [sds((rows // 2, width), BF16)] * 4,
-                [
-                    side.astype(jnp.int32).reshape(1),
-                    attended,
-                    attended_pair,
-                    normed,
-                    normed_pair,
-                    *[shards[m] for m in group],
-                ],
-                flops=4 * 10**8 * len(group),
-                name="project",
-            )
-            pieces += [
-                outs[0],
-                lax.ppermute(outs[1], "tp", [(0, 1), (1, 0)]),
-                flip(outs[2], count, 1),
-                lax.ppermute(outs[3], ("sp", "tp"), diag),
-            ]
         order = []
-        for m in masks:
-            order += [me ^ m, me ^ 1 ^ m]
+        for i, m in enumerate(group):
+            pieces.append(outs[2 * i] if m == 0 else flip(outs[2 * i], count, m))
+            pieces.append(cross(outs[2 * i + 1], count, m))
+            order += [me ^ m ^ b for b in masks]
         (out,) = call(
-            functools.partial(place_kernel, groups, span),
+            functools.partial(place_kernel, (len(group), len(masks), span)),
             [sds((rows // 2, span * count), BF16)],
             [jnp.stack(order).astype(jnp.int32), *pieces],
             flops=10**6,
-            name="place",
         )
         return out
 
+    attended_pair = attended_blocks[1]
+    normed_pair = normed_blocks[1]
+    shards = {m: jnp.stack([halves[0][m], halves[1][m]]) for m in masks}
     left = jnp.concatenate(
         [
             jnp.concatenate([attended, normed], axis=1),
@@ -607,4 +632,5 @@
         P(None, "tp", "sp"),
     )
     out_specs = P(("sp", "tp"), None)
+
     return jax.shard_map(local, mesh=mesh, in_specs=in_specs, out_specs=out_specs, check_vma=False)

time: 217 us -> 143 us (0.66); the launches traced: 213 us -> 142 us
  waiting for transfers between devices: 140 us -> 60 us
  starting transfers between devices: 31 us -> 37.8 us
  local copies, waits for them, and re-layouts: 6.84 us -> 10.4 us
    ppermute x16 -> x20, waiting for transfers between devices: 135 us -> 54.4 us  [flip(): return lax.ppermute(a, 'sp', [(i, i ^ mask) for i in range(count)])]
    ppermute x16 -> x20, starting transfers between devices: 19.7 us -> 23.7 us  [flip(): return lax.ppermute(a, 'sp', [(i, i ^ mask) for i in range(count)])]
    unnamed x39 -> x47, local copies, waits for them, and re-layouts: 3.54 us -> 5.78 us
  transfers between devices with their start and end apart: 24 -> 28, of which waited for: 10 -> 13; matrix products, arithmetic and copies ran while one was open for 3% -> 8% of each run, Pallas kernels for 10% -> 9%
where the time goes in v2:
time: 143 us; the launch traced here: 142 us
  waiting for transfers between devices  60 us (42%)
  starting transfers between devices  37.8 us (26%)
  Pallas kernels  27.4 us (19%)
  local copies, waits for them, and re-layouts  10.4 us (7%)
  other arithmetic  6.04 us (4%)
    ppermute x20, waiting for transfers between devices, flip(): return lax.ppermute(a, 'sp', [(i, i ^ mask) for i in range(count)])  54.4 us
    pallas_call x6, Pallas kernels, call(): pl.pallas_call(kernel, out_shape=outs, in_specs=[SMEM] * scalars + [VMEM]...  27.4 us
    ppermute x20, starting transfers between devices, flip(): return lax.ppermute(a, 'sp', [(i, i ^ mask) for i in range(count)])  23.7 us
    ppermute x4, starting transfers between devices, shift(): lax.ppermute(a, 'sp', [(i, i + by) for i in range(count) if 0 <= i + by <...  7.8 us
    ppermute x4, starting transfers between devices, cross(): lax.ppermute(a, ('sp', 'tp'), [(2 * i + j, 2 * (i ^ mask) + 1 - j) for i...  6.33 us
    unnamed x47, local copies, waits for them, and re-layouts  5.78 us
    ppermute x4, waiting for transfers between devices, cross(): lax.ppermute(a, ('sp', 'tp'), [(2 * i + j, 2 * (i ^ mask) + 1 - j) for i...  4.64 us
  transfers between devices with their start and end apart: 28, of which 13 were waited for; matrix products, arithmetic and copies ran while one was open for 8% of the time, Pallas kernels for 9%

profile of v2, /device:TPU:0, one launch (start us, length us, event | category | flops | bytes accessed | tf_op | source)
XLA Modules:
  0.0 142.0 jit_solution(17567897962140914799)
XLA Ops:
  1.6 2.4 %collective-permute-start.8 = (bf16[16,2048]{1,0:T(8,128)(2,1)S(1)}, bf16[16,2048]{1,0:T(8,128)(2,1)S(1)}, u32[]{:S(2)}, u32[]{:S(2)}) collective-permute-start(bf16[16,2048]{1,0:T(8,128)(2,1)S(1)} %pad_maximum_fusion.4), channel_id=1, source_target_pairs={{0,2},{2,4},{4,6},{6,8},{8,10},{10,12},{12,14},{14,16},{16,18},{18... | collective-permute-start | bytes 196616 | tf_op jit(solution)/shard_map/ppermute | solution.py:328
  9.9 5.9 %shard_map.156 = (bf16[272,512]{1,0:T(8,128)(2,1)}, bf16[272,512]{1,0:T(8,128)(2,1)}, bf16[128,512]{1,0:T(8,128)(2,1)}, f32[128,1024]{1,0:T(8,128)}, f32[128,32]{1,0:T(8,128)}) custom-call(s32[1]{0:T(128)} %bitcast.18.place, bf16[128,1024]{1,0:T(8,128)(2,1)} %x_ref.1, bf16[128,512]{1,0:T(8,128)(2,1)} %w_ref.1, bf16[128,512]{1,0:T(8,128)(2,1)} %r_ref.1, ...), custom_call_target="tpu_custom_call" | custom-call | flops 4000000000 | bytes 1937540 | tf_op jit(solution)/shard_map/pallas_call | solution.py:29
  15.8 3.0 %collective-permute-start.10 = (bf16[272,512]{1,0:T(8,128)(2,1)}, bf16[272,512]{1,0:T(8,128)(2,1)S(1)}, u32[]{:S(2)}, u32[]{:S(2)}) collective-permute-start(bf16[272,512]{1,0:T(8,128)(2,1)} %get-tuple-element.21), channel_id=1, source_target_pairs={{0,2},{2,0},{4,6},{6,4},{8,10},{10,8},{12,14},{14,12},{16,18},{18,... | collective-permute-start | bytes 835592 | tf_op jit(solution)/shard_map/ppermute | solution.py:324
  19.5 2.6 %collective-permute-start = (bf16[128,1024]{1,0:T(8,128)(2,1)}, bf16[128,1024]{1,0:T(8,128)(2,1)}, u32[]{:S(2)}, u32[]{:S(2)}) collective-permute-start(bf16[128,1024]{1,0:T(8,128)(2,1)} %constant_dynamic-update-slice_fusion), channel_id=1, source_target_pairs={{0,2},{2,4},{4,6},{6,8},{8,10},{10,12},{12,14},{14,16},{16,18},{18... | collective-permute-start | bytes 786440 | tf_op jit(solution)/shard_map/ppermute | solution.py:328
  25.7 4.1 %collective-permute-start.11 = (bf16[272,512]{1,0:T(8,128)(2,1)S(1)}, bf16[272,512]{1,0:T(8,128)(2,1)S(1)}, u32[]{:S(2)}, u32[]{:S(2)}) collective-permute-start(bf16[272,512]{1,0:T(8,128)(2,1)S(1)} %concatenate.41), channel_id=1, source_target_pairs={{0,4},{2,6},{4,0},{6,2},{8,12},{10,14},{12,8},{14,10},{16,20},{18,... | collective-permute-start | bytes 835592 | tf_op jit(solution)/shard_map/ppermute | solution.py:324
  29.9 2.7 %collective-permute-start.5 = (bf16[1024,256]{1,0:T(8,128)(2,1)S(1)}, bf16[1024,256]{1,0:T(8,128)(2,1)S(1)}, u32[]{:S(2)}, u32[]{:S(2)}) collective-permute-start(bf16[1024,256]{1,0:T(8,128)(2,1)S(1)} %get-tuple-element.50.refs_4_), channel_id=1, source_target_pairs={{0,16},{2,18},{4,20},{6,22},{8,24},{10,26},{12,28},{14,30},{16,0},... | collective-permute-start | bytes 1572872 | tf_op jit(solution)/shard_map/ppermute | solution.py:324
  33.4 5.8 %collective-permute-done.11 = bf16[272,512]{1,0:T(8,128)(2,1)S(1)} collective-permute-done((bf16[272,512]{1,0:T(8,128)(2,1)S(1)}, bf16[272,512]{1,0:T(8,128)(2,1)S(1)}, u32[]{:S(2)}, u32[]{:S(2)}) %collective-permute-start.11) | collective-permute-done | bytes 278560 | tf_op jit(solution)/shard_map/ppermute | solution.py:324
  39.7 1.6 %collective-permute-start.12 = (bf16[272,512]{1,0:T(8,128)(2,1)S(1)}, bf16[272,512]{1,0:T(8,128)(2,1)S(1)}, u32[]{:S(2)}, u32[]{:S(2)}) collective-permute-start(bf16[272,512]{1,0:T(8,128)(2,1)S(1)} %concatenate.43), channel_id=1, source_target_pairs={{0,8},{2,10},{4,12},{6,14},{8,0},{10,2},{12,4},{14,6},{16,24},{18,... | collective-permute-start | bytes 835592 | tf_op jit(solution)/shard_map/ppermute | solution.py:324
  42.1 11.7 %collective-permute-done.12 = bf16[272,512]{1,0:T(8,128)(2,1)S(1)} collective-permute-done((bf16[272,512]{1,0:T(8,128)(2,1)S(1)}, bf16[272,512]{1,0:T(8,128)(2,1)S(1)}, u32[]{:S(2)}, u32[]{:S(2)}) %collective-permute-start.12) | collective-permute-done | bytes 278560 | tf_op jit(solution)/shard_map/ppermute | solution.py:324
  54.1 5.2 %collective-permute-start.13 = (bf16[128,512]{1,0:T(8,128)(2,1)S(1)}, bf16[128,512]{1,0:T(8,128)(2,1)S(1)}, u32[]{:S(2)}, u32[]{:S(2)}) collective-permute-start(bf16[128,512]{1,0:T(8,128)(2,1)S(1)} %fusion.9), channel_id=1, source_target_pairs={{0,16},{2,18},{4,20},{6,22},{8,24},{10,26},{12,28},{14,30},{16,0},... | collective-permute-start | bytes 393224 | tf_op jit(solution)/shard_map/ppermute | solution.py:324
  61.0 9.4 %collective-permute-done.13 = bf16[128,512]{1,0:T(8,128)(2,1)S(1)} collective-permute-done((bf16[128,512]{1,0:T(8,128)(2,1)S(1)}, bf16[128,512]{1,0:T(8,128)(2,1)S(1)}, u32[]{:S(2)}, u32[]{:S(2)}) %collective-permute-start.13) | collective-permute-done | bytes 131104 | tf_op jit(solution)/shard_map/ppermute | solution.py:324
  71.6 5.1 %shard_map.154.refs_0_ = bf16[128,1024]{1,0:T(8,128)(2,1)} custom-call(s32[2]{0:T(128)} %pad_add_fusion.place, f32[8]{0:T(128)} %sink.1, bf16[128,1024]{1,0:T(8,128)(2,1)} %q_ref.1, bf16[128,512]{1,0:T(8,128)(2,1)} %k_ref.1, bf16[128,512]{1,0:T(8,128)(2,1)} %v_ref.1, bf16[128,1024]{1,0:T(8,128)(2,1)} %collective-permute-done.prev_ref, ...), custom_call_target="tpu_custom_call" | custom-call | flops 3000000000 | bytes 1703976 | tf_op jit(solution)/shard_map/pallas_call | solution.py:29
  76.8 3.4 %collective-permute-start.2 = (bf16[128,1024]{1,0:T(8,128)(2,1)}, bf16[128,1024]{1,0:T(8,128)(2,1)S(1)}, u32[]{:S(2)}, u32[]{:S(2)}) collective-permute-start(bf16[128,1024]{1,0:T(8,128)(2,1)} %shard_map.154.refs_0_), channel_id=1, source_target_pairs={{0,8},{2,10},{4,12},{6,14},{8,0},{10,2},{12,4},{14,6},{16,24},{18,... | collective-permute-start | bytes 786440 | tf_op jit(solution)/shard_map/ppermute | solution.py:324
  81.1 3.3 %shard_map.157.refs_0_ = bf16[128,1024]{1,0:T(8,128)(2,1)} custom-call(s32[1]{0:T(128)} %bitcast.18.place, f32[128,1024]{1,0:T(8,128)} %get-tuple-element.18.y_ref, bf16[128,512]{1,0:T(8,128)(2,1)} %get-tuple-element.19.read_ref, f32[128,32]{1,0:T(8,128)} %get-tuple-element.20.expl_ref, bf16[256,512]{1,0:T(8,128)(2,1)} %get-tuple-element.58.own_ref, ...), custom_call_target="tpu_custom_call" | custom-call | flops 3000000000 | bytes 1724420 | tf_op jit(solution)/shard_map/pallas_call | solution.py:29
  84.4 7.4 %collective-permute-done.2.refs_1_ = bf16[128,1024]{1,0:T(8,128)(2,1)S(1)} collective-permute-done((bf16[128,1024]{1,0:T(8,128)(2,1)}, bf16[128,1024]{1,0:T(8,128)(2,1)S(1)}, u32[]{:S(2)}, u32[]{:S(2)}) %collective-permute-start.2) | collective-permute-done | bytes 262176 | tf_op jit(solution)/shard_map/ppermute | solution.py:324
  91.8 2.3 %collective-permute-start.19 = (bf16[1024,256]{1,0:T(8,128)(2,1)S(1)}, bf16[1024,256]{1,0:T(8,128)(2,1)S(1)}, u32[]{:S(2)}, u32[]{:S(2)}) collective-permute-start(bf16[1024,256]{1,0:T(8,128)(2,1)S(1)} %get-tuple-element.49.refs_4_), channel_id=1, source_target_pairs={{0,4},{2,6},{4,0},{6,2},{8,12},{10,14},{12,8},{14,10},{16,20},{18,... | collective-permute-start | bytes 1572872 | tf_op jit(solution)/shard_map/ppermute | solution.py:324
  96.5 6.6 %collective-permute-done.15.refs_1_ = bf16[128,1024]{1,0:T(8,128)(2,1)S(1)} collective-permute-done((bf16[128,1024]{1,0:T(8,128)(2,1)}, bf16[128,1024]{1,0:T(8,128)(2,1)S(1)}, u32[]{:S(2)}, u32[]{:S(2)}) %collective-permute-start.15) | collective-permute-done | bytes 262176 | tf_op jit(solution)/shard_map/ppermute | solution.py:324
  104.0 4.4 %shard_map.155.sum_ref = f32[512,1024]{1,0:T(8,128)} custom-call(bf16[128,1024]{1,0:T(8,128)(2,1)} %shard_map.154.refs_0_, bf16[128,1024]{1,0:T(8,128)(2,1)} %copy-done.8, bf16[128,1024]{1,0:T(8,128)(2,1)} %collective-permute-done.3.refs_2_, bf16[128,1024]{1,0:T(8,128)(2,1)} %copy-done.9, bf16[1024,256]{1,0:T(8,128)(2,1)} %copy-done.1, ...), custom_call_target="tpu_custom_call" | custom-call | flops 1073741824 | bytes 5242880 | tf_op jit(solution)/shard_map/pallas_call | solution.py:29
  108.4 9.0 %collective-permute-done.20.refs_7_ = bf16[1024,256]{1,0:T(8,128)(2,1)} collective-permute-done((bf16[1024,256]{1,0:T(8,128)(2,1)}, bf16[1024,256]{1,0:T(8,128)(2,1)}, u32[]{:S(2)}, u32[]{:S(2)}) %collective-permute-start.20) | collective-permute-done | bytes 524320 | tf_op jit(solution)/shard_map/ppermute | solution.py:324
  118.2 6.4 %shard_map.158 = (bf16[64,1024]{1,0:T(8,128)(2,1)}, bf16[64,1024]{1,0:T(8,128)(2,1)}, bf16[64,1024]{1,0:T(8,128)(2,1)}, bf16[64,1024]{1,0:T(8,128)(2,1)}, bf16[6...) custom-call(s32[1]{0:T(128)} %bitcast.16.place, ...), custom_call_target="tpu_custom_call" | custom-call | flops 1073741824 | bytes 6291460 | tf_op jit(solution)/shard_map/pallas_call | solution.py:29
  126.1 2.0 %collective-permute-start.23 = (bf16[64,1024]{1,0:T(8,128)(2,1)}, bf16[64,1024]{1,0:T(8,128)(2,1)S(1)}, u32[]{:S(2)}, u32[]{:S(2)}) collective-permute-start(bf16[64,1024]{1,0:T(8,128)(2,1)} %get-tuple-element.26), channel_id=1, source_target_pairs={{0,9},{1,8},{2,11},{3,10},{4,13},{5,12},{6,15},{7,14},{8,1},{9,0},... | collective-permute-start | bytes 393224 | tf_op jit(solution)/shard_map/ppermute | solution.py:334
  128.0 1.6 %collective-permute-start.25 = (bf16[64,1024]{1,0:T(8,128)(2,1)}, bf16[64,1024]{1,0:T(8,128)(2,1)S(1)}, u32[]{:S(2)}, u32[]{:S(2)}) collective-permute-start(bf16[64,1024]{1,0:T(8,128)(2,1)} %get-tuple-element.28), channel_id=1, source_target_pairs={{0,3},{1,2},{2,1},{3,0},{4,7},{5,6},{6,5},{7,4},{8,11},{9,10},{10,... | collective-permute-start | bytes 393224 | tf_op jit(solution)/shard_map/ppermute | solution.py:334
  136.7 2.5 %collective-permute-done.27.refs_7_ = bf16[64,1024]{1,0:T(8,128)(2,1)S(1)} collective-permute-done((bf16[64,1024]{1,0:T(8,128)(2,1)}, bf16[64,1024]{1,0:T(8,128)(2,1)S(1)}, u32[]{:S(2)}, u32[]{:S(2)}) %collective-permute-start.27) | collective-permute-done | bytes 131104 | tf_op jit(solution)/shard_map/ppermute | solution.py:334
  139.8 2.2 %shard_map.159 = bf16[64,4096]{1,0:T(8,128)(2,1)} custom-call(s32[16]{0:T(128)} %stack.71.place, bf16[64,1024]{1,0:T(8,128)(2,1)} %get-tuple-element.23.refs_0_, bf16[64,1024]{1,0:T(8,128)(2,1)} %copy-done.12, bf16[64,1024]{1,0:T(8,128)(2,1)} %copy-done.13, bf16[64,1024]{1,0:T(8,128)(2,1)} %copy-done.14, bf16[64,1024]{1,0:T(8,128)(2,1)} %copy-done.15, ...), custom_call_target="tpu_custom_call" | custom-call | flops 1000000 | bytes 1572928 | tf_op jit(solution)/shard_map/pallas_call | solution.py:29
  (118 shorter events, 30.9 us)
Async XLA Ops:
  1.6 6.7 %collective-permute-start.8 = (bf16[16,2048]{1,0:T(8,128)(2,1)S(1)}, bf16[16,2048]{1,0:T(8,128)(2,1)S(1)}, u32[]{:S(2)}, u32[]{:S(2)}) collective-permute-start(bf16[16,2048]{1,0:T(8,128)(2,1)S(1)} %pad_maximum_fusion.4), channel_id=1, source_target_pairs={{0,2},{2,4},{4,6},{6,8},{8,10},{10,12},{12,14},{14,16},{16,18},{18... | collective-permute-start | bytes 196616 | tf_op jit(solution)/shard_map/ppermute | solution.py:328
  15.8 8.5 %collective-permute-start.10 = (bf16[272,512]{1,0:T(8,128)(2,1)}, bf16[272,512]{1,0:T(8,128)(2,1)S(1)}, u32[]{:S(2)}, u32[]{:S(2)}) collective-permute-start(bf16[272,512]{1,0:T(8,128)(2,1)} %get-tuple-element.21), channel_id=1, source_target_pairs={{0,2},{2,0},{4,6},{6,4},{8,10},{10,8},{12,14},{14,12},{16,18},{18,... | collective-permute-start | bytes 835592 | tf_op jit(solution)/shard_map/ppermute | solution.py:324
  19.5 52.1 %collective-permute-start = (bf16[128,1024]{1,0:T(8,128)(2,1)}, bf16[128,1024]{1,0:T(8,128)(2,1)}, u32[]{:S(2)}, u32[]{:S(2)}) collective-permute-start(bf16[128,1024]{1,0:T(8,128)(2,1)} %constant_dynamic-update-slice_fusion), channel_id=1, source_target_pairs={{0,2},{2,4},{4,6},{6,8},{8,10},{10,12},{12,14},{14,16},{16,18},{18... | collective-permute-start | bytes 786440 | tf_op jit(solution)/shard_map/ppermute | solution.py:328
  22.1 49.5 %collective-permute-start.1 = (bf16[128,1024]{1,0:T(8,128)(2,1)}, bf16[128,1024]{1,0:T(8,128)(2,1)}, u32[]{:S(2)}, u32[]{:S(2)}) collective-permute-start(bf16[128,1024]{1,0:T(8,128)(2,1)} %constant_dynamic-update-slice_fusion), channel_id=1, source_target_pairs={{2,0},{4,2},{6,4},{8,6},{10,8},{12,10},{14,12},{16,14},{18,16},{20... | collective-permute-start | bytes 786440 | tf_op jit(solution)/shard_map/ppermute | solution.py:328
  25.7 13.5 %collective-permute-start.11 = (bf16[272,512]{1,0:T(8,128)(2,1)S(1)}, bf16[272,512]{1,0:T(8,128)(2,1)S(1)}, u32[]{:S(2)}, u32[]{:S(2)}) collective-permute-start(bf16[272,512]{1,0:T(8,128)(2,1)S(1)} %concatenate.41), channel_id=1, source_target_pairs={{0,4},{2,6},{4,0},{6,2},{8,12},{10,14},{12,8},{14,10},{16,20},{18,... | collective-permute-start | bytes 835592 | tf_op jit(solution)/shard_map/ppermute | solution.py:324
  29.9 50.2 %collective-permute-start.5 = (bf16[1024,256]{1,0:T(8,128)(2,1)S(1)}, bf16[1024,256]{1,0:T(8,128)(2,1)S(1)}, u32[]{:S(2)}, u32[]{:S(2)}) collective-permute-start(bf16[1024,256]{1,0:T(8,128)(2,1)S(1)} %get-tuple-element.50.refs_4_), channel_id=1, source_target_pairs={{0,16},{2,18},{4,20},{6,22},{8,24},{10,26},{12,28},{14,30},{16,0},... | collective-permute-start | bytes 1572872 | tf_op jit(solution)/shard_map/ppermute | solution.py:324
  32.5 61.7 %collective-permute-start.6 = (bf16[1024,256]{1,0:T(8,128)(2,1)S(1)}, bf16[1024,256]{1,0:T(8,128)(2,1)S(1)}, u32[]{:S(2)}, u32[]{:S(2)}) collective-permute-start(bf16[1024,256]{1,0:T(8,128)(2,1)S(1)} %get-tuple-element.50.refs_4_), channel_id=1, source_target_pairs={{0,4},{2,6},{4,0},{6,2},{8,12},{10,14},{12,8},{14,10},{16,20},{18,... | collective-permute-start | bytes 1572872 | tf_op jit(solution)/shard_map/ppermute | solution.py:324
  39.7 14.2 %collective-permute-start.12 = (bf16[272,512]{1,0:T(8,128)(2,1)S(1)}, bf16[272,512]{1,0:T(8,128)(2,1)S(1)}, u32[]{:S(2)}, u32[]{:S(2)}) collective-permute-start(bf16[272,512]{1,0:T(8,128)(2,1)S(1)} %concatenate.43), channel_id=1, source_target_pairs={{0,8},{2,10},{4,12},{6,14},{8,0},{10,2},{12,4},{14,6},{16,24},{18,... | collective-permute-start | bytes 835592 | tf_op jit(solution)/shard_map/ppermute | solution.py:324
  54.1 16.2 %collective-permute-start.13 = (bf16[128,512]{1,0:T(8,128)(2,1)S(1)}, bf16[128,512]{1,0:T(8,128)(2,1)S(1)}, u32[]{:S(2)}, u32[]{:S(2)}) collective-permute-start(bf16[128,512]{1,0:T(8,128)(2,1)S(1)} %fusion.9), channel_id=1, source_target_pairs={{0,16},{2,18},{4,20},{6,22},{8,24},{10,26},{12,28},{14,30},{16,0},... | collective-permute-start | bytes 393224 | tf_op jit(solution)/shard_map/ppermute | solution.py:324
  70.4 23.7 %collective-permute-start.18 = (bf16[1024,256]{1,0:T(8,128)(2,1)S(1)}, bf16[1024,256]{1,0:T(8,128)(2,1)}, u32[]{:S(2)}, u32[]{:S(2)}) collective-permute-start(bf16[1024,256]{1,0:T(8,128)(2,1)S(1)} %get-tuple-element.49.refs_4_), channel_id=1, source_target_pairs={{0,16},{2,18},{4,20},{6,22},{8,24},{10,26},{12,28},{14,30},{16,0},... | collective-permute-start | bytes 1572872 | tf_op jit(solution)/shard_map/ppermute | solution.py:324
  71.6 8.7 %collective-permute-start.14 = (bf16[256,512]{1,0:T(8,128)(2,1)S(1)}, bf16[256,512]{1,0:T(8,128)(2,1)S(1)}, u32[]{:S(2)}, u32[]{:S(2)}) collective-permute-start(bf16[256,512]{1,0:T(8,128)(2,1)S(1)} %get-tuple-element.57), channel_id=1, source_target_pairs={{0,2},{2,0},{4,6},{6,4},{8,10},{10,8},{12,14},{14,12},{16,18},{18,... | collective-permute-start | bytes 786440 | tf_op jit(solution)/shard_map/ppermute | solution.py:324
  76.8 15.1 %collective-permute-start.2 = (bf16[128,1024]{1,0:T(8,128)(2,1)}, bf16[128,1024]{1,0:T(8,128)(2,1)S(1)}, u32[]{:S(2)}, u32[]{:S(2)}) collective-permute-start(bf16[128,1024]{1,0:T(8,128)(2,1)} %shard_map.154.refs_0_), channel_id=1, source_target_pairs={{0,8},{2,10},{4,12},{6,14},{8,0},{10,2},{12,4},{14,6},{16,24},{18,... | collective-permute-start | bytes 786440 | tf_op jit(solution)/shard_map/ppermute | solution.py:324
  80.1 14.0 %collective-permute-start.3 = (bf16[128,1024]{1,0:T(8,128)(2,1)}, bf16[128,1024]{1,0:T(8,128)(2,1)}, u32[]{:S(2)}, u32[]{:S(2)}) collective-permute-start(bf16[128,1024]{1,0:T(8,128)(2,1)} %shard_map.154.refs_0_), channel_id=1, source_target_pairs={{0,2},{2,0},{4,6},{6,4},{8,10},{10,8},{12,14},{14,12},{16,18},{18,... | collective-permute-start | bytes 786440 | tf_op jit(solution)/shard_map/ppermute | solution.py:324
  80.4 22.8 %collective-permute-start.7 = (bf16[1024,256]{1,0:T(8,128)(2,1)S(1)}, bf16[1024,256]{1,0:T(8,128)(2,1)S(1)}, u32[]{:S(2)}, u32[]{:S(2)}) collective-permute-start(bf16[1024,256]{1,0:T(8,128)(2,1)S(1)} %collective-permute-done.5.refs_5_), channel_id=1, source_target_pairs={{0,4},{2,6},{4,0},{6,2},{8,12},{10,14},{12,8},{14,10},{16,20},{18,... | collective-permute-start | bytes 1572872 | tf_op jit(solution)/shard_map/ppermute | solution.py:324
  91.8 16.6 %collective-permute-start.19 = (bf16[1024,256]{1,0:T(8,128)(2,1)S(1)}, bf16[1024,256]{1,0:T(8,128)(2,1)S(1)}, u32[]{:S(2)}, u32[]{:S(2)}) collective-permute-start(bf16[1024,256]{1,0:T(8,128)(2,1)S(1)} %get-tuple-element.49.refs_4_), channel_id=1, source_target_pairs={{0,4},{2,6},{4,0},{6,2},{8,12},{10,14},{12,8},{14,10},{16,20},{18,... | collective-permute-start | bytes 1572872 | tf_op jit(solution)/shard_map/ppermute | solution.py:324
  94.1 23.3 %collective-permute-start.20 = (bf16[1024,256]{1,0:T(8,128)(2,1)}, bf16[1024,256]{1,0:T(8,128)(2,1)}, u32[]{:S(2)}, u32[]{:S(2)}) collective-permute-start(bf16[1024,256]{1,0:T(8,128)(2,1)} %collective-permute-done.18.refs_5_), channel_id=1, source_target_pairs={{0,4},{2,6},{4,0},{6,2},{8,12},{10,14},{12,8},{14,10},{16,20},{18,... | collective-permute-start | bytes 1572872 | tf_op jit(solution)/shard_map/ppermute | solution.py:324
  94.3 8.8 %collective-permute-start.15 = (bf16[128,1024]{1,0:T(8,128)(2,1)}, bf16[128,1024]{1,0:T(8,128)(2,1)S(1)}, u32[]{:S(2)}, u32[]{:S(2)}) collective-permute-start(bf16[128,1024]{1,0:T(8,128)(2,1)} %shard_map.157.refs_0_), channel_id=1, source_target_pairs={{0,8},{2,10},{4,12},{6,14},{8,0},{10,2},{12,4},{14,6},{16,24},{18,... | collective-permute-start | bytes 786440 | tf_op jit(solution)/shard_map/ppermute | solution.py:324
  96.3 21.1 %collective-permute-start.16 = (bf16[128,1024]{1,0:T(8,128)(2,1)}, bf16[128,1024]{1,0:T(8,128)(2,1)S(1)}, u32[]{:S(2)}, u32[]{:S(2)}) collective-permute-start(bf16[128,1024]{1,0:T(8,128)(2,1)} %shard_map.157.refs_0_), channel_id=1, source_target_pairs={{0,2},{2,0},{4,6},{6,4},{8,10},{10,8},{12,14},{14,12},{16,18},{18,... | collective-permute-start | bytes 786440 | tf_op jit(solution)/shard_map/ppermute | solution.py:324
  103.1 14.3 %collective-permute-start.17 = (bf16[128,1024]{1,0:T(8,128)(2,1)S(1)}, bf16[128,1024]{1,0:T(8,128)(2,1)}, u32[]{:S(2)}, u32[]{:S(2)}) collective-permute-start(bf16[128,1024]{1,0:T(8,128)(2,1)S(1)} %collective-permute-done.15.refs_1_), channel_id=1, source_target_pairs={{0,2},{2,0},{4,6},{6,4},{8,10},{10,8},{12,14},{14,12},{16,18},{18,... | collective-permute-start | bytes 786440 | tf_op jit(solution)/shard_map/ppermute | solution.py:324
  124.5 6.1 %collective-permute-start.21 = (bf16[64,1024]{1,0:T(8,128)(2,1)}, bf16[64,1024]{1,0:T(8,128)(2,1)S(1)}, u32[]{:S(2)}, u32[]{:S(2)}) collective-permute-start(bf16[64,1024]{1,0:T(8,128)(2,1)} %get-tuple-element.24), channel_id=1, source_target_pairs={{0,1},{1,0},{2,3},{3,2},{4,5},{5,4},{6,7},{7,6},{8,9},{9,8},{10,11... | collective-permute-start | bytes 393224 | tf_op jit(solution)/shard_map/ppermute | solution.py:334
  126.1 6.1 %collective-permute-start.22 = (bf16[64,1024]{1,0:T(8,128)(2,1)}, bf16[64,1024]{1,0:T(8,128)(2,1)S(1)}, u32[]{:S(2)}, u32[]{:S(2)}) collective-permute-start(bf16[64,1024]{1,0:T(8,128)(2,1)} %get-tuple-element.25), channel_id=1, source_target_pairs={{0,8},{2,10},{4,12},{6,14},{8,0},{10,2},{12,4},{14,6},{16,24},{18,... | collective-permute-start | bytes 393224 | tf_op jit(solution)/shard_map/ppermute | solution.py:324
  126.1 7.9 %collective-permute-start.23 = (bf16[64,1024]{1,0:T(8,128)(2,1)}, bf16[64,1024]{1,0:T(8,128)(2,1)S(1)}, u32[]{:S(2)}, u32[]{:S(2)}) collective-permute-start(bf16[64,1024]{1,0:T(8,128)(2,1)} %get-tuple-element.26), channel_id=1, source_target_pairs={{0,9},{1,8},{2,11},{3,10},{4,13},{5,12},{6,15},{7,14},{8,1},{9,0},... | collective-permute-start | bytes 393224 | tf_op jit(solution)/shard_map/ppermute | solution.py:334
  128.0 7.1 %collective-permute-start.25 = (bf16[64,1024]{1,0:T(8,128)(2,1)}, bf16[64,1024]{1,0:T(8,128)(2,1)S(1)}, u32[]{:S(2)}, u32[]{:S(2)}) collective-permute-start(bf16[64,1024]{1,0:T(8,128)(2,1)} %get-tuple-element.28), channel_id=1, source_target_pairs={{0,3},{1,2},{2,1},{3,0},{4,7},{5,6},{6,5},{7,4},{8,11},{9,10},{10,... | collective-permute-start | bytes 393224 | tf_op jit(solution)/shard_map/ppermute | solution.py:334
  132.1 7.0 %collective-permute-start.27 = (bf16[64,1024]{1,0:T(8,128)(2,1)}, bf16[64,1024]{1,0:T(8,128)(2,1)S(1)}, u32[]{:S(2)}, u32[]{:S(2)}) collective-permute-start(bf16[64,1024]{1,0:T(8,128)(2,1)} %get-tuple-element.30), channel_id=1, source_target_pairs={{0,11},{1,10},{2,9},{3,8},{4,15},{5,14},{6,13},{7,12},{8,3},{9,2},... | collective-permute-start | bytes 393224 | tf_op jit(solution)/shard_map/ppermute | solution.py:334
  (27 other events, 243.7 us)

commit v3 on v2

--- a/solution.py
+++ b/solution.py
@@ -24,7 +24,7 @@
 SMEM = pl.BlockSpec(memory_space=pltpu.SMEM)
 
 
-def call(kernel, outs, ins, flops, scratch=(), scalars=1):
+def call(kernel, outs, ins, flops, scratch=(), scalars=0):
     moved = sum(a.size * a.dtype.itemsize for a in list(ins) + list(outs))
     return pl.pallas_call(
         kernel,
@@ -59,12 +59,11 @@
 
 
 def block_kernel(
-    place,
     x_ref,
     w_ref,
     r_ref,
-    prev_ref,
-    next_ref,
+    pair_ref,
+    outer_ref,
     tx_ref,
     tw_ref,
     tr_ref,
@@ -82,6 +81,7 @@
 ):
     rows, cols = x_ref.shape
     wide = w_ref.shape[1]
+    core = lax.axis_index("sp") & 1
     heads = cols // SSD_HEAD
     groups = wide // STATE
     per = heads // groups
@@ -89,9 +89,11 @@
     start = 0
     for src, taps, dst in ((x_ref, tx_ref, xs), (w_ref, tw_ref, ws), (r_ref, tr_ref, read_ref)):
         span = src.shape[1]
-        line[0:EDGE, 0:span] = prev_ref[:, start : start + span].astype(F32)
+        pair = pair_ref[:, start : start + span].astype(F32)
+        outer = outer_ref[:, start : start + span].astype(F32)
+        line[0:EDGE, 0:span] = jnp.where(core == 0, outer, pair)
         line[EDGE : EDGE + rows, 0:span] = src[...].astype(F32)
-        line[EDGE + rows : 2 * EDGE + rows, 0:span] = next_ref[:, start : start + span].astype(F32)
+        line[EDGE + rows : 2 * EDGE + rows, 0:span] = jnp.where(core == 0, pair, outer)
         step = min(span, 256)
         for at in range(0, span, step):
             total = jnp.zeros((rows, step), F32)
@@ -104,7 +106,16 @@
         start += span
 
     steps = jax.nn.softplus(inc_ref[...])
-    logs = -jnp.exp(fade_ref[...]) * steps + spike_ref[...]
+    square = lax.broadcasted_iota(jnp.int32, (heads, heads), 0)
+    square = square == lax.broadcasted_iota(jnp.int32, (heads, heads), 1)
+    rates = jnp.concatenate(
+        [
+            jnp.sum(jnp.where(square, jnp.exp(fade_ref[d : d + 1, :]), 0.0), axis=1, keepdims=True)
+            for d in range(2)
+        ],
+        axis=0,
+    )
+    logs = -rates * steps + spike_ref[...]
     first = lax.broadcasted_iota(jnp.int32, (rows, rows), 0)
     second = lax.broadcasted_iota(jnp.int32, (rows, rows), 1)
     lower = first >= second
@@ -130,11 +141,11 @@
     for side in range(2):
         part = tail[:, side * half : (side + 1) * half]
 
-        @pl.when(place[0] == side)
+        @pl.when(core == side)
         def _():
             keep_ref[2 * STATE : 2 * STATE + EDGE, :] = part
 
-        @pl.when(place[0] != side)
+        @pl.when(core != side)
         def _():
             send_ref[2 * STATE : 2 * STATE + EDGE, :] = part
 
@@ -171,19 +182,21 @@
                 continue
             part = whole[:, a - base : b - base]
 
-            @pl.when(place[0] == side)
+            @pl.when(core == side)
             def _():
                 keep_ref[0 : 2 * STATE, a - side * half : b - side * half] = part
 
-            @pl.when(place[0] != side)
+            @pl.when(core != side)
             def _():
                 send_ref[0 : 2 * STATE, a - side * half : b - side * half] = part
 
 
 def attend_kernel(
-    place, sink, q_ref, k_ref, v_ref, prev_ref, next_ref, cos_ref, sin_ref, out_ref
+    sink, q_ref, k_ref, v_ref, pair_ref, outer_ref, cos_ref, sin_ref, out_ref
 ):
     rows = q_ref.shape[0]
+    me = lax.axis_index("sp")
+    last = lax.axis_size("sp") - 1
     kv = k_ref.shape[1] // HEAD
     sharing = q_ref.shape[1] // k_ref.shape[1]
     wide = k_ref.shape[1]
@@ -199,23 +212,30 @@
     across = lax.broadcasted_iota(jnp.int32, (rows, 3 * rows), 1)
     far = across - rows - within
     allowed = (far <= WINDOW) & (far >= -WINDOW)
-    allowed = allowed & ((across >= rows) | (place[0] > 0))
-    allowed = allowed & ((across < 2 * rows) | (place[0] < place[1] - 1))
+    allowed = allowed & ((across >= rows) | (me > 0))
+    allowed = allowed & ((across < 2 * rows) | (me < last))
+    even = (me & 1) == 0
     for g in range(kv):
         at = g * HEAD
+        near = [
+            (pair_ref[:, a : a + HEAD].astype(F32), outer_ref[:, a : a + HEAD].astype(F32))
+            for a in (at, wide + at)
+        ]
+        before = [jnp.where(even, o, p) for p, o in near]
+        after = [jnp.where(even, p, o) for p, o in near]
         keys = jnp.concatenate(
             [
-                turn(prev_ref[:, at : at + HEAD], 0),
+                turn(before[0], 0),
                 turn(k_ref[:, at : at + HEAD], rows),
-                turn(next_ref[:, at : at + HEAD], 2 * rows),
+                turn(after[0], 2 * rows),
             ],
             axis=0,
         )
         values = jnp.concatenate(
             [
-                prev_ref[:, wide + at : wide + at + HEAD],
+                before[1].astype(BF16),
                 v_ref[:, at : at + HEAD],
-                next_ref[:, wide + at : wide + at + HEAD],
+                after[1].astype(BF16),
             ],
             axis=0,
         )
@@ -231,8 +251,9 @@
             out_ref[:, h * HEAD : (h + 1) * HEAD] = nn(chance, values).astype(BF16)
 
 
-def finish_kernel(place, y_ref, read_ref, expl_ref, own_ref, got_ref, gate_ref, gain_ref, out_ref):
+def finish_kernel(y_ref, read_ref, expl_ref, own_ref, got_ref, gate_ref, gain_ref, out_ref):
     _, cols = y_ref.shape
+    core = lax.axis_index("sp") & 1
     wide = read_ref.shape[1]
     heads = cols // SSD_HEAD
     groups = wide // STATE
@@ -247,7 +268,7 @@
             span = min(size, half)
             side = low // half
             off = low - side * half
-            mine = place[0] == side
+            mine = core == side
             pieces.append(
                 jnp.where(
                     mine,
@@ -283,22 +304,30 @@
         at += span
 
 
-def second_kernel(count, place, sum_ref, *refs):
-    lefts = refs[: count[0]]
-    shards = refs[count[0] : count[0] + count[1]]
-    outs = refs[count[0] + count[1] :]
+def second_kernel(count, sum_ref, *refs):
+    place = lax.axis_index("tp")
+    blocks, shards, base = count
+    lefts = refs[:blocks]
+    tops = refs[blocks : blocks + shards]
+    lows = refs[blocks + shards : blocks + 2 * shards]
+    outs = refs[blocks + 2 * shards :]
     rows = lefts[0].shape[0]
     half = rows // 2
+    deep = tops[0].shape[0]
     left = jnp.concatenate([a[...] for a in lefts], axis=0)
     at = 0
-    for shard in shards:
-        span = shard.shape[1]
-        total = (sum_ref[:, at : at + span] + nn(left, shard[...])).astype(BF16)
+    for top, low in zip(tops, lows):
+        span = top.shape[1]
+        total = (
+            sum_ref[:, base + at : base + at + span]
+            + nn(left[:, :deep], top[...])
+            + nn(left[:, deep:], low[...])
+        ).astype(BF16)
         for side in range(2):
 
-            @pl.when(place[0] == side)
+            @pl.when(place == side)
             def _():
-                for i in range(count[0]):
+                for i in range(blocks):
                     a = i * rows + side * half
                     b = i * rows + (1 - side) * half
                     outs[2 * i][:, at : at + span] = total[a : a + half]
@@ -307,27 +336,79 @@
         at += span
 
 
-def place_kernel(shape, place, *refs):
-    sources, columns, span = shape
+def place_kernel(group, masks, span, *refs):
+    me = lax.axis_index("sp")
     out_ref = refs[-1]
-    for i in range(sources):
-        for j in range(columns):
+    for i, block in enumerate(group):
+        for j, mask in enumerate(masks):
             at = j * span
-            to = pl.multiple_of(place[i * columns + j] * span, span)
+            to = pl.multiple_of((me ^ (block ^ mask)) * span, span)
             out_ref[:, pl.ds(to, span)] = (
                 refs[2 * i][:, at : at + span].astype(F32)
                 + refs[2 * i + 1][:, at : at + span].astype(F32)
             ).astype(BF16)
 
 
+def edge_kernel(*refs):
+    even = (lax.axis_index("sp") & 1) == 0
+    start = 0
+    for i in range(0, 6, 2):
+        lead = refs[i][...].astype(F32)
+        tail = refs[i + 1][...].astype(F32)
+        span = lead.shape[1]
+        refs[6][:, start : start + span] = jnp.where(even, tail, lead).astype(BF16)
+        refs[7][:, start : start + span] = jnp.where(even, lead, tail).astype(BF16)
+        start += span
+
+
+def edges(raw):
+    specs = []
+    for a in raw:
+        end = a.shape[0] // EDGE - 1
+        specs.append(pl.BlockSpec((EDGE, a.shape[1]), lambda i: (0, 0)))
+        specs.append(pl.BlockSpec((EDGE, a.shape[1]), lambda i, end=end: (end, 0)))
+    width = sum(a.shape[1] for a in raw)
+    return pl.pallas_call(
+        edge_kernel,
+        grid=(1,),
+        out_shape=[jax.ShapeDtypeStruct((EDGE, width), BF16)] * 2,
+        in_specs=specs,
+        out_specs=[pl.BlockSpec((EDGE, width), lambda i: (0, 0))] * 2,
+        name="edges",
+    )(*[a for a in raw for _ in range(2)])
+
+
+def join_kernel(keep_ref, got_ref, out_ref):
+    even = (lax.axis_index("sp") & 1) == 0
+    end = 2 * STATE
+
+    def load(low, high):
+        mine = keep_ref[low:high, :].astype(F32)
+        theirs = got_ref[low:high, :].astype(F32)
+        return jnp.where(even, mine, theirs), jnp.where(even, theirs, mine)
+
+    low, high = load(end, end + EDGE)
+    low = low[0:2] + low[2:4]
+    high = high[0:2] + high[2:4]
+    fades = low * high
+    top = fades.astype(BF16).astype(F32)
+    rest = fades - top
+    out_ref[end : end + EDGE, :] = jnp.concatenate(
+        [top, rest, jnp.zeros((EDGE - 4, top.shape[1]), F32)], axis=0
+    ).astype(BF16)
+    a, b = load(0, STATE)
+    out_ref[0:STATE, :] = (a * high[0:1] + b).astype(BF16)
+    a, b = load(STATE, end)
+    out_ref[STATE:end, :] = (b * low[1:2] + a).astype(BF16)
+
+
 def flip(a, count, mask):
     return lax.ppermute(a, "sp", [(i, i ^ mask) for i in range(count)])
 
 
-def shift(a, count, by):
-    return lax.ppermute(
-        a, "sp", [(i, i + by) for i in range(count) if 0 <= i + by < count]
-    )
+def outer(a, count):
+    pairs = [(i, i + 1) for i in range(1, count - 1, 2)]
+    return lax.ppermute(a, "sp", pairs + [(j, i) for i, j in pairs])
 
 
 def cross(a, count, mask):
@@ -336,6 +417,13 @@
         ("sp", "tp"),
         [(2 * i + j, 2 * (i ^ mask) + 1 - j) for i in range(count) for j in range(2)],
     )
+
+
+def join_pair(keep, got):
+    (payload,) = call(
+        join_kernel, [jax.ShapeDtypeStruct(keep.shape, BF16)], [keep, got], flops=10**6
+    )
+    return payload
 
 
 def exchange_states(keep, send, count, me):
@@ -352,19 +440,31 @@
             tail[1:2] + tail[3:4],
         )
 
-    mine = split(keep)
-    theirs = split(got)
     pick = lambda flag, a, b: jax.tree.map(lambda u, v: jnp.where(flag, u, v), a, b)
-    low = pick(core == 0, mine, theirs)
-    high = pick(core == 0, theirs, mine)
     join = lambda low, high: (
         low[0] * high[2] + high[0],
         high[1] * low[3] + low[1],
         low[2] * high[2],
         low[3] * high[3],
     )
-    pair = (low, high)
-    total = join(low, high)
+
+    def pack(total):
+        fades = jnp.concatenate([total[2], total[3]], axis=0)
+        top = fades.astype(BF16)
+        rest = (fades - top.astype(F32)).astype(BF16)
+        return jnp.concatenate(
+            [
+                total[0].astype(BF16),
+                total[1].astype(BF16),
+                top,
+                rest,
+                jnp.zeros((EDGE - 4, half), BF16),
+            ],
+            axis=0,
+        )
+
+    seen = payload = join_pair(keep, got)
+    total = split(payload)
     into_f = jnp.zeros((STATE, half), F32)
     into_b = jnp.zeros((STATE, half), F32)
     gap_f = jnp.ones((1, half), F32)
@@ -379,20 +479,10 @@
             into_f = jnp.where(upper, other * gap_f + into_f, into_f)
             into_b = jnp.where(upper, into_b, other * gap_b + into_b)
         else:
-            fades = jnp.concatenate([total[2], total[3]], axis=0)
-            top = fades.astype(BF16)
-            rest = (fades - top.astype(F32)).astype(BF16)
-            payload = jnp.concatenate(
-                [
-                    total[0].astype(BF16),
-                    total[1].astype(BF16),
-                    top,
-                    rest,
-                    jnp.zeros((EDGE - 4, half), BF16),
-                ],
-                axis=0,
-            )
+            if payload is None:
+                payload = pack(total)
             other = split(flip(payload, count, bit))
+            payload = None
             low = pick(upper, other, total)
             high = pick(upper, total, other)
             into_f = jnp.where(upper, other[0] * gap_f + into_f, into_f)
@@ -401,12 +491,15 @@
             gap_b = jnp.where(upper, gap_b, gap_b * other[3])
             total = join(low, high)
         bit *= 2
-    low, high = pair
+    keep, got = lax.optimization_barrier((keep, got, seen))[:2]
+    mine, theirs = split(keep), split(got)
+    low = pick(core == 0, mine, theirs)
+    high = pick(core == 0, theirs, mine)
     first = jnp.concatenate([into_f, into_b * high[3] + high[1]], axis=0).astype(BF16)
     second = jnp.concatenate([into_f * low[2] + low[0], into_b], axis=0).astype(BF16)
     own = jnp.where(core == 0, first, second)
     away = jnp.where(core == 0, second, first)
-    return own, flip(away, count, 1)
+    return own, flip(away, count, 1), seen
 
 
 def local(
@@ -429,23 +522,17 @@
 ):
     rows = asking_matrix.shape[0]
     me = lax.axis_index("sp")
-    side = lax.axis_index("tp")
     count = lax.axis_size("sp")
     tps = lax.axis_size("tp")
     cols = duality_source_matrix.shape[1]
     wide = storing_direction_matrix.shape[1]
     heads = cols // SSD_HEAD
-    core = (me & 1).astype(jnp.int32).reshape(1)
     sds = jax.ShapeDtypeStruct
 
     raw = (duality_source_matrix, storing_direction_matrix, fetching_direction_matrix)
-    tail = jnp.concatenate([a[rows - EDGE :] for a in raw], axis=1)
-    lead = jnp.concatenate([a[:EDGE] for a in raw], axis=1)
-    prev_edge = shift(tail, count, 1)
-    next_edge = shift(lead, count, -1)
-    pairs = jnp.concatenate([matching_key_matrix, carried_value_matrix], axis=1)
-    prev_pair = shift(pairs, count, 1)
-    next_pair = shift(pairs, count, -1)
+    to_pair, to_outer = edges(raw)
+    pair_edge = flip(to_pair, count, 1)
+    outer_edge = outer(to_outer, count)
 
     span = final_mapping_matrix.shape[2]
     fast = tps == 2 and span % 128 == 0 and count == 16
@@ -456,12 +543,16 @@
         if bit not in shared:
             bits.append(bit)
         bit //= 2
-    halves = [{0: final_mapping_matrix[0]}, {0: final_mapping_matrix[1]}]
-    for shards in halves:
+
+    def gather(piece):
+        shards = {0: piece}
         for bit in bits:
             for mask in list(shards):
                 shards[mask ^ bit] = flip(shards[mask], count, bit)
-    masks = list(halves[0])
+        return shards
+
+    halves = [gather(final_mapping_matrix[0])]
+    masks = sorted(halves[0])
 
     keep, send, read, inner, expl = call(
         block_kernel,
@@ -473,15 +564,14 @@
             sds((rows, 2 * heads), F32),
         ],
         [
-            core,
             *raw,
-            prev_edge,
-            next_edge,
+            pair_edge,
+            outer_edge,
             duality_kernel_coefficients,
             storing_kernel_coefficients,
             fetching_kernel_coefficients,
             raw_increment_lengths.reshape(2 * heads, rows),
-            logarithmic_fading_speeds.reshape(2 * heads, 1),
+            logarithmic_fading_speeds,
             token_fading_spikes.reshape(2 * heads, rows),
         ],
         flops=4 * 10**9,
@@ -491,33 +581,40 @@
             pltpu.VMEM((rows, wide), BF16),
         ],
     )
-    own_state, got_state = exchange_states(keep, send, count, me)
+    own_state, got_state, seen = exchange_states(keep, send, count, me)
+    later, weights, matching_key, carried_value = lax.optimization_barrier(
+        (me, final_mapping_matrix, matching_key_matrix, carried_value_matrix, seen)
+    )[:4]
+    right_rows = weights[1]
+    middle = right_rows.shape[0] // 2
+    halves += [gather(right_rows[:middle]), gather(right_rows[middle:])]
+    pairs = jnp.concatenate([matching_key, carried_value], axis=1)
+    pair_kv = flip(pairs, count, 1)
+    outer_kv = outer(pairs, count)
 
     halfway = HEAD // 2
     spacing = ROTARY_BASE ** (-jnp.arange(halfway, dtype=F32) * 2.0 / HEAD)
-    places = ((me - 1) * rows + jnp.arange(3 * rows, dtype=jnp.int32)).astype(F32)
+    places = ((later - 1) * rows + jnp.arange(3 * rows, dtype=jnp.int32)).astype(F32)
     angles = places[:, None] * spacing[None, :]
     cosine = jnp.cos(angles)
     sine = jnp.sin(angles)
     cosine = jnp.concatenate([cosine, cosine], axis=1)
     sine = jnp.concatenate([-sine, sine], axis=1)
-    where = jnp.stack([me, jnp.int32(count)]).astype(jnp.int32)
     (attended,) = call(
         attend_kernel,
         [sds(asking_matrix.shape, BF16)],
         [
-            where,
             absorber_score_vector,
             asking_matrix,
             matching_key_matrix,
             carried_value_matrix,
-            prev_pair,
-            next_pair,
+            pair_kv,
+            outer_kv,
             cosine,
             sine,
         ],
         flops=3 * 10**9,
-        scalars=2,
+        scalars=1,
     )
 
     def spread_rows(a):
@@ -532,7 +629,6 @@
         finish_kernel,
         [sds((rows, cols), BF16)],
         [
-            core,
             inner,
             read,
             expl,
@@ -554,36 +650,39 @@
             [sds((len(group) * rows, width), F32)],
             [*attended_blocks, *[halves[0][m] for m in masks]],
             flops=flops,
-            scalars=0,
-        )
-        outs = call(
-            functools.partial(second_kernel, sizes),
-            [sds((rows // 2, width), BF16)] * (2 * len(group)),
-            [
-                side.astype(jnp.int32).reshape(1),
-                early,
-                *normed_blocks,
-                *[halves[1][m] for m in masks],
-            ],
-            flops=flops,
         )
         pieces = []
-        order = []
-        for i, m in enumerate(group):
-            pieces.append(outs[2 * i] if m == 0 else flip(outs[2 * i], count, m))
-            pieces.append(cross(outs[2 * i + 1], count, m))
-            order += [me ^ m ^ b for b in masks]
+        cut = len(masks)
+        for turn, chosen in enumerate((masks,)):
+            wide_part = span * len(chosen)
+            outs = call(
+                functools.partial(second_kernel, (len(group), len(chosen), turn * span * cut)),
+                [sds((rows // 2, wide_part), BF16)] * (2 * len(group)),
+                [
+                    early,
+                    *normed_blocks,
+                    *[halves[1][m] for m in chosen],
+                    *[halves[2][m] for m in chosen],
+                ],
+                flops=flops,
+            )
+            for i, m in enumerate(group):
+                kept, gone = outs[2 * i], outs[2 * i + 1]
+                pieces.append(kept if m == 0 else flip(kept, count, m))
+                pieces.append(cross(gone, count, m))
         (out,) = call(
-            functools.partial(place_kernel, (len(group), len(masks), span)),
+            functools.partial(place_kernel, group, masks, span),
             [sds((rows // 2, span * count), BF16)],
-            [jnp.stack(order).astype(jnp.int32), *pieces],
+            pieces,
             flops=10**6,
         )
         return out
 
     attended_pair = attended_blocks[1]
     normed_pair = normed_blocks[1]
-    shards = {m: jnp.stack([halves[0][m], halves[1][m]]) for m in masks}
+    shards = {
+        m: jnp.stack([halves[0][m], jnp.concatenate([halves[1][m], halves[2][m]])]) for m in masks
+    }
     left = jnp.concatenate(
         [
             jnp.concatenate([attended, normed], axis=1),

time: 143 us -> 136 us (0.951)
  starting transfers between devices: 37.8 us -> 32.9 us
  Pallas kernels: 27.4 us -> 31 us
  local copies, waits for them, and re-layouts: 10.4 us -> 8.01 us
  waiting for transfers between devices: 60 us -> 57.8 us
    ppermute x4 -> x2, starting transfers between devices: 7.8 us -> 2.01 us  [outer(): return lax.ppermute(a, 'sp', pairs + [(j, i) for i, j in pairs])]
    ppermute x20 -> x25, starting transfers between devices: 23.7 us -> 26.9 us  [flip(): return lax.ppermute(a, 'sp', [(i, i ^ mask) for i in range(count)])]
    ppermute x20 -> x25, waiting for transfers between devices: 54.4 us -> 51.4 us  [flip(): return lax.ppermute(a, 'sp', [(i, i ^ mask) for i in range(count)])]
    concatenate x3 -> x2, local copies, waits for them, and re-layouts: 1.02 us -> 3.9 us  [the longest x1 3.24 us: pack(): jnp.concatenate([total[0].astype(BF16), total[1].astype(BF16), top, rest,...]
    ppermute x4, starting transfers between devices: 6.33 us -> 3.95 us  [cross(): lax.ppermute(a, ('sp', 'tp'), [(2 * i + j, 2 * (i ^ mask) + 1 - j) for i...]
    pallas_call x6 -> x7, Pallas kernels: 27.4 us -> 29.5 us  [call(): pl.pallas_call(kernel, out_shape=outs, in_specs=[SMEM] * scalars + [VMEM]...]
    ppermute x4, waiting for transfers between devices: 4.64 us -> 6.39 us  [cross(): lax.ppermute(a, ('sp', 'tp'), [(2 * i + j, 2 * (i ^ mask) + 1 - j) for i...]
    unnamed x47 -> x67, local copies, waits for them, and re-layouts: 5.78 us -> 4.03 us
  transfers between devices with their start and end apart: 28 -> 31, of which waited for: 13 -> 14; matrix products, arithmetic and copies ran while one was open for 8% -> 8% of each run, Pallas kernels for 9% -> 11%
where the time goes in v3:
time: 136 us
  waiting for transfers between devices  57.8 us (42%)
  starting transfers between devices  32.9 us (24%)
  Pallas kernels  31 us (23%)
  local copies, waits for them, and re-layouts  8.01 us (6%)
  other arithmetic  5.83 us (4%)
    ppermute x25, waiting for transfers between devices, flip(): return lax.ppermute(a, 'sp', [(i, i ^ mask) for i in range(count)])  51.4 us
    pallas_call x7, Pallas kernels, call(): pl.pallas_call(kernel, out_shape=outs, in_specs=[SMEM] * scalars + [VMEM]...  29.5 us
    ppermute x25, starting transfers between devices, flip(): return lax.ppermute(a, 'sp', [(i, i ^ mask) for i in range(count)])  26.9 us
    ppermute x4, waiting for transfers between devices, cross(): lax.ppermute(a, ('sp', 'tp'), [(2 * i + j, 2 * (i ^ mask) + 1 - j) for i...  6.39 us
    unnamed x67, local copies, waits for them, and re-layouts  4.03 us
    ppermute x4, starting transfers between devices, cross(): lax.ppermute(a, ('sp', 'tp'), [(2 * i + j, 2 * (i ^ mask) + 1 - j) for i...  3.95 us
    concatenate x1, local copies, waits for them, and re-layouts, pack(): jnp.concatenate([total[0].astype(BF16), total[1].astype(BF16), top, rest,...  3.24 us
  transfers between devices with their start and end apart: 31, of which 14 were waited for; matrix products, arithmetic and copies ran while one was open for 8% of the time, Pallas kernels for 11%

profile of v3, /device:TPU:0, one launch (start us, length us, event | category | flops | bytes accessed | tf_op | source)
XLA Modules:
  0.0 135.9 jit_solution(15902799475854852519)
XLA Ops:
  3.7 6.1 %shard_map.154 = (bf16[272,512]{1,0:T(8,128)(2,1)}, bf16[272,512]{1,0:T(8,128)(2,1)}, bf16[128,512]{1,0:T(8,128)(2,1)}, f32[128,1024]{1,0:T(8,128)}, f32[128,32]{1,0:T(8,128)}) custom-call(bf16[128,1024]{1,0:T(8,128)(2,1)} %x_ref.1, bf16[128,512]{1,0:T(8,128)(2,1)} %w_ref.1, bf16[128,512]{1,0:T(8,128)(2,1)} %r_ref.1, bf16[16,2048]{1,0:T(8,128)(2,1)} %copy-done.31, ...), custom_call_target="tpu_custom_call" | custom-call | flops 4000000000 | bytes 1937536 | tf_op jit(solution)/shard_map/pallas_call | solution.py:29
  9.9 5.6 %collective-permute-start.2 = (bf16[272,512]{1,0:T(8,128)(2,1)}, bf16[272,512]{1,0:T(8,128)(2,1)S(1)}, u32[]{:S(2)}, u32[]{:S(2)}) collective-permute-start(bf16[272,512]{1,0:T(8,128)(2,1)} %get-tuple-element.29), channel_id=1, source_target_pairs={{0,2},{2,0},{4,6},{6,4},{8,10},{10,8},{12,14},{14,12},{16,18},{18,... | collective-permute-start | bytes 835592 | tf_op jit(solution)/shard_map/ppermute | solution.py:406
  15.5 4.0 %collective-permute-start.9 = (bf16[1024,256]{1,0:T(8,128)(2,1)S(1)}, bf16[1024,256]{1,0:T(8,128)(2,1)}, u32[]{:S(2)}, u32[]{:S(2)}) collective-permute-start(bf16[1024,256]{1,0:T(8,128)(2,1)S(1)} %slice_bitcast_fusion.refs_4_), channel_id=1, source_target_pairs={{0,16},{2,18},{4,20},{6,22},{8,24},{10,26},{12,28},{14,30},{16,0},... | collective-permute-start | bytes 1572872 | tf_op jit(solution)/shard_map/ppermute | solution.py:406
  19.5 1.7 %collective-permute-start.8 = (bf16[1024,256]{1,0:T(8,128)(2,1)S(1)}, bf16[1024,256]{1,0:T(8,128)(2,1)}, u32[]{:S(2)}, u32[]{:S(2)}) collective-permute-start(bf16[1024,256]{1,0:T(8,128)(2,1)S(1)} %slice_bitcast_fusion.refs_4_), channel_id=1, source_target_pairs={{0,4},{2,6},{4,0},{6,2},{8,12},{10,14},{12,8},{14,10},{16,20},{18,... | collective-permute-start | bytes 1572872 | tf_op jit(solution)/shard_map/ppermute | solution.py:406
  21.9 1.9 %shard_map.155 = bf16[272,512]{1,0:T(8,128)(2,1)} custom-call(bf16[272,512]{1,0:T(8,128)(2,1)} %get-tuple-element.37.keep_ref, bf16[272,512]{1,0:T(8,128)(2,1)} %copy-done.3), custom_call_target="tpu_custom_call" | custom-call | flops 1000000 | bytes 835584 | tf_op jit(solution)/shard_map/pallas_call | solution.py:29
  29.2 10.5 %collective-permute-done.11 = bf16[272,512]{1,0:T(8,128)(2,1)S(1)} collective-permute-done((bf16[272,512]{1,0:T(8,128)(2,1)}, bf16[272,512]{1,0:T(8,128)(2,1)S(1)}, u32[]{:S(2)}, u32[]{:S(2)}) %collective-permute-start.11) | collective-permute-done | bytes 278560 | tf_op jit(solution)/shard_map/ppermute | solution.py:406
  40.9 3.2 %concatenate.27 = bf16[272,512]{1,0:T(8,128)(2,1)} concatenate(bf16[128,512]{1,0:T(8,128)(2,1)S(1)} %get-tuple-element.64, bf16[128,512]{1,0:T(8,128)(2,1)S(1)} %get-tuple-element.63, bf16[2,512]{1,0:T(2,128)(2,1)S(1)} %fusion.17, bf16[2,512]{1,0:T(2,128)(2,1)S(1)} %subtract_convert_fusion, bf16[12,512]{1,0:T(8,128)(2,1)S(1)} %broadcast_in_dim.2), dimensions={0} | concatenate | bytes 557056 | tf_op jit(solution)/shard_map/concatenate | solution.py:455
  44.1 4.0 %collective-permute-start.12 = (bf16[272,512]{1,0:T(8,128)(2,1)}, bf16[272,512]{1,0:T(8,128)(2,1)S(1)}, u32[]{:S(2)}, u32[]{:S(2)}) collective-permute-start(bf16[272,512]{1,0:T(8,128)(2,1)} %concatenate.27), channel_id=1, source_target_pairs={{0,8},{2,10},{4,12},{6,14},{8,0},{10,2},{12,4},{14,6},{16,24},{18,... | collective-permute-start | bytes 835592 | tf_op jit(solution)/shard_map/ppermute | solution.py:406
  48.2 6.1 %collective-permute-done.12 = bf16[272,512]{1,0:T(8,128)(2,1)S(1)} collective-permute-done((bf16[272,512]{1,0:T(8,128)(2,1)}, bf16[272,512]{1,0:T(8,128)(2,1)S(1)}, u32[]{:S(2)}, u32[]{:S(2)}) %collective-permute-start.12) | collective-permute-done | bytes 278560 | tf_op jit(solution)/shard_map/ppermute | solution.py:406
  56.0 6.3 %collective-permute-done.13 = bf16[128,512]{1,0:T(8,128)(2,1)S(1)} collective-permute-done((bf16[128,512]{1,0:T(8,128)(2,1)S(1)}, bf16[128,512]{1,0:T(8,128)(2,1)S(1)}, u32[]{:S(2)}, u32[]{:S(2)}) %collective-permute-start.13) | collective-permute-done | bytes 131104 | tf_op jit(solution)/shard_map/ppermute | solution.py:406
  64.8 5.1 %shard_map.156.refs_0_ = bf16[128,1024]{1,0:T(8,128)(2,1)} custom-call(f32[8]{0:T(128)} %sink.1, bf16[128,1024]{1,0:T(8,128)(2,1)} %q_ref.1, bf16[128,512]{1,0:T(8,128)(2,1)} %k_ref.1, bf16[128,512]{1,0:T(8,128)(2,1)} %v_ref.1, bf16[128,1024]{1,0:T(8,128)(2,1)} %collective-permute-done.3.pair_ref, bf16[128,1024]{1,0:T(8,128)(2,1)} %collective-permute-done.4.outer_ref, ...), custom_call_target="tpu_custom_call" | custom-call | flops 3000000000 | bytes 1703968 | tf_op jit(solution)/shard_map/pallas_call | solution.py:29
  69.9 1.8 %collective-permute-start.22 = (bf16[512,256]{1,0:T(8,128)(2,1)S(1)}, bf16[512,256]{1,0:T(8,128)(2,1)S(1)}, u32[]{:S(2)}, u32[]{:S(2)}) collective-permute-start(bf16[512,256]{1,0:T(8,128)(2,1)S(1)} %get-tuple-element.59.refs_8_), channel_id=1, source_target_pairs={{0,16},{2,18},{4,20},{6,22},{8,24},{10,26},{12,28},{14,30},{16,0},... | collective-permute-start | bytes 786440 | tf_op jit(solution)/shard_map/ppermute | solution.py:406
  71.7 1.9 %collective-permute-start.10 = (bf16[1024,256]{1,0:T(8,128)(2,1)}, bf16[1024,256]{1,0:T(8,128)(2,1)S(1)}, u32[]{:S(2)}, u32[]{:S(2)}) collective-permute-start(bf16[1024,256]{1,0:T(8,128)(2,1)} %collective-permute-done.9.refs_6_), channel_id=1, source_target_pairs={{0,4},{2,6},{4,0},{6,2},{8,12},{10,14},{12,8},{14,10},{16,20},{18,... | collective-permute-start | bytes 1572872 | tf_op jit(solution)/shard_map/ppermute | solution.py:406
  73.7 6.6 %collective-permute-done.19.refs_6_ = bf16[512,256]{1,0:T(8,128)(2,1)S(1)} collective-permute-done((bf16[512,256]{1,0:T(8,128)(2,1)S(1)}, bf16[512,256]{1,0:T(8,128)(2,1)S(1)}, u32[]{:S(2)}, u32[]{:S(2)}) %collective-permute-start.19) | collective-permute-done | bytes 262176 | tf_op jit(solution)/shard_map/ppermute | solution.py:406
  81.0 3.3 %shard_map.158.refs_0_ = bf16[128,1024]{1,0:T(8,128)(2,1)} custom-call(f32[128,1024]{1,0:T(8,128)} %get-tuple-element.33.y_ref, bf16[128,512]{1,0:T(8,128)(2,1)} %get-tuple-element.34.read_ref, f32[128,32]{1,0:T(8,128)} %get-tuple-element.35.expl_ref, bf16[256,512]{1,0:T(8,128)(2,1)} %get-tuple-element.66.own_ref, bf16[256,512]{1,0:T(8,128)(2,1)} %copy-done.30, ...), custom_call_target="tpu_custom_call" | custom-call | flops 3000000000 | bytes 1724416 | tf_op jit(solution)/shard_map/pallas_call | solution.py:29
  84.3 6.9 %collective-permute-done.5.refs_1_ = bf16[128,1024]{1,0:T(8,128)(2,1)S(1)} collective-permute-done((bf16[128,1024]{1,0:T(8,128)(2,1)}, bf16[128,1024]{1,0:T(8,128)(2,1)S(1)}, u32[]{:S(2)}, u32[]{:S(2)}) %collective-permute-start.5) | collective-permute-done | bytes 262176 | tf_op jit(solution)/shard_map/ppermute | solution.py:406
  91.5 2.1 %collective-permute-start.20 = (bf16[512,256]{1,0:T(8,128)(2,1)S(1)}, bf16[512,256]{1,0:T(8,128)(2,1)S(1)}, u32[]{:S(2)}, u32[]{:S(2)}) collective-permute-start(bf16[512,256]{1,0:T(8,128)(2,1)S(1)} %collective-permute-done.19.refs_6_), channel_id=1, source_target_pairs={{0,4},{2,6},{4,0},{6,2},{8,12},{10,14},{12,8},{14,10},{16,20},{18,... | collective-permute-start | bytes 786440 | tf_op jit(solution)/shard_map/ppermute | solution.py:406
  93.7 6.5 %collective-permute-done.15.refs_1_ = bf16[128,1024]{1,0:T(8,128)(2,1)S(1)} collective-permute-done((bf16[128,1024]{1,0:T(8,128)(2,1)}, bf16[128,1024]{1,0:T(8,128)(2,1)S(1)}, u32[]{:S(2)}, u32[]{:S(2)}) %collective-permute-start.15) | collective-permute-done | bytes 262176 | tf_op jit(solution)/shard_map/ppermute | solution.py:406
  100.2 4.5 %shard_map.157.sum_ref = f32[512,1024]{1,0:T(8,128)} custom-call(bf16[128,1024]{1,0:T(8,128)(2,1)} %shard_map.156.refs_0_, bf16[128,1024]{1,0:T(8,128)(2,1)} %copy-done.15, bf16[128,1024]{1,0:T(8,128)(2,1)} %copy-done.17, bf16[128,1024]{1,0:T(8,128)(2,1)} %copy-done.20, bf16[1024,256]{1,0:T(8,128)(2,1)} %copy-done.1, ...), custom_call_target="tpu_custom_call" | custom-call | flops 1073741824 | bytes 5242880 | tf_op jit(solution)/shard_map/pallas_call | solution.py:29
  106.3 5.1 %collective-permute-done.23.refs_11_ = bf16[512,256]{1,0:T(8,128)(2,1)S(1)} collective-permute-done((bf16[512,256]{1,0:T(8,128)(2,1)S(1)}, bf16[512,256]{1,0:T(8,128)(2,1)S(1)}, u32[]{:S(2)}, u32[]{:S(2)}) %collective-permute-start.23) | collective-permute-done | bytes 262176 | tf_op jit(solution)/shard_map/ppermute | solution.py:406
  112.0 6.3 %shard_map.159 = (bf16[64,1024]{1,0:T(8,128)(2,1)}, bf16[64,1024]{1,0:T(8,128)(2,1)}, bf16[64,1024]{1,0:T(8,128)(2,1)}, bf16[64,1024]{1,0:T(8,128)(2,1)}, bf16[6...) custom-call(f32[512,1024]{1,0:T(8,128)} %shard_map.157.sum_ref, ...), custom_call_target="tpu_custom_call" | custom-call | flops 1073741824 | bytes 6291456 | tf_op jit(solution)/shard_map/pallas_call | solution.py:29
  127.9 1.9 %collective-permute-done.28.refs_5_ = bf16[64,1024]{1,0:T(8,128)(2,1)S(1)} collective-permute-done((bf16[64,1024]{1,0:T(8,128)(2,1)}, bf16[64,1024]{1,0:T(8,128)(2,1)S(1)}, u32[]{:S(2)}, u32[]{:S(2)}) %collective-permute-start.28) | collective-permute-done | bytes 131104 | tf_op jit(solution)/shard_map/ppermute | solution.py:415
  129.8 3.3 %collective-permute-done.30.refs_7_ = bf16[64,1024]{1,0:T(8,128)(2,1)S(1)} collective-permute-done((bf16[64,1024]{1,0:T(8,128)(2,1)}, bf16[64,1024]{1,0:T(8,128)(2,1)S(1)}, u32[]{:S(2)}, u32[]{:S(2)}) %collective-permute-start.30) | collective-permute-done | bytes 131104 | tf_op jit(solution)/shard_map/ppermute | solution.py:415
  133.8 2.2 %shard_map.160 = bf16[64,4096]{1,0:T(8,128)(2,1)} custom-call(bf16[64,1024]{1,0:T(8,128)(2,1)} %get-tuple-element.39.refs_0_, bf16[64,1024]{1,0:T(8,128)(2,1)} %copy-done.21, bf16[64,1024]{1,0:T(8,128)(2,1)} %copy-done.22, bf16[64,1024]{1,0:T(8,128)(2,1)} %copy-done.23, bf16[64,1024]{1,0:T(8,128)(2,1)} %copy-done.24, bf16[64,1024]{1,0:T(8,128)(2,1)} %copy-done.25, ...), custom_call_target="tpu_custom_call" | custom-call | flops 1000000 | bytes 1572864 | tf_op jit(solution)/shard_map/pallas_call | solution.py:29
  (136 shorter events, 28.6 us)
Async XLA Ops:
  9.9 11.4 %collective-permute-start.2 = (bf16[272,512]{1,0:T(8,128)(2,1)}, bf16[272,512]{1,0:T(8,128)(2,1)S(1)}, u32[]{:S(2)}, u32[]{:S(2)}) collective-permute-start(bf16[272,512]{1,0:T(8,128)(2,1)} %get-tuple-element.29), channel_id=1, source_target_pairs={{0,2},{2,0},{4,6},{6,4},{8,10},{10,8},{12,14},{14,12},{16,18},{18,... | collective-permute-start | bytes 835592 | tf_op jit(solution)/shard_map/ppermute | solution.py:406
  15.5 54.4 %collective-permute-start.9 = (bf16[1024,256]{1,0:T(8,128)(2,1)S(1)}, bf16[1024,256]{1,0:T(8,128)(2,1)}, u32[]{:S(2)}, u32[]{:S(2)}) collective-permute-start(bf16[1024,256]{1,0:T(8,128)(2,1)S(1)} %slice_bitcast_fusion.refs_4_), channel_id=1, source_target_pairs={{0,16},{2,18},{4,20},{6,22},{8,24},{10,26},{12,28},{14,30},{16,0},... | collective-permute-start | bytes 1572872 | tf_op jit(solution)/shard_map/ppermute | solution.py:406
  19.5 52.2 %collective-permute-start.8 = (bf16[1024,256]{1,0:T(8,128)(2,1)S(1)}, bf16[1024,256]{1,0:T(8,128)(2,1)}, u32[]{:S(2)}, u32[]{:S(2)}) collective-permute-start(bf16[1024,256]{1,0:T(8,128)(2,1)S(1)} %slice_bitcast_fusion.refs_4_), channel_id=1, source_target_pairs={{0,4},{2,6},{4,0},{6,2},{8,12},{10,14},{12,8},{14,10},{16,20},{18,... | collective-permute-start | bytes 1572872 | tf_op jit(solution)/shard_map/ppermute | solution.py:406
  23.9 15.8 %collective-permute-start.11 = (bf16[272,512]{1,0:T(8,128)(2,1)}, bf16[272,512]{1,0:T(8,128)(2,1)S(1)}, u32[]{:S(2)}, u32[]{:S(2)}) collective-permute-start(bf16[272,512]{1,0:T(8,128)(2,1)} %shard_map.155), channel_id=1, source_target_pairs={{0,4},{2,6},{4,0},{6,2},{8,12},{10,14},{12,8},{14,10},{16,20},{18,... | collective-permute-start | bytes 835592 | tf_op jit(solution)/shard_map/ppermute | solution.py:406
  26.3 37.3 %collective-permute-start.3 = (bf16[128,1024]{1,0:T(8,128)(2,1)}, bf16[128,1024]{1,0:T(8,128)(2,1)}, u32[]{:S(2)}, u32[]{:S(2)}) collective-permute-start(bf16[128,1024]{1,0:T(8,128)(2,1)} %constant_dynamic-update-slice_fusion), channel_id=1, source_target_pairs={{0,2},{2,0},{4,6},{6,4},{8,10},{10,8},{12,14},{14,12},{16,18},{18,... | collective-permute-start | bytes 786440 | tf_op jit(solution)/shard_map/ppermute | solution.py:406
  26.3 38.5 %collective-permute-start.4 = (bf16[128,1024]{1,0:T(8,128)(2,1)}, bf16[128,1024]{1,0:T(8,128)(2,1)}, u32[]{:S(2)}, u32[]{:S(2)}) collective-permute-start(bf16[128,1024]{1,0:T(8,128)(2,1)} %constant_dynamic-update-slice_fusion), channel_id=1, source_target_pairs={{2,4},{6,8},{10,12},{14,16},{18,20},{22,24},{26,28},{4,2},{8,6},{1... | collective-permute-start | bytes 786440 | tf_op jit(solution)/shard_map/ppermute | solution.py:411
  44.1 10.2 %collective-permute-start.12 = (bf16[272,512]{1,0:T(8,128)(2,1)}, bf16[272,512]{1,0:T(8,128)(2,1)S(1)}, u32[]{:S(2)}, u32[]{:S(2)}) collective-permute-start(bf16[272,512]{1,0:T(8,128)(2,1)} %concatenate.27), channel_id=1, source_target_pairs={{0,8},{2,10},{4,12},{6,14},{8,0},{10,2},{12,4},{14,6},{16,24},{18,... | collective-permute-start | bytes 835592 | tf_op jit(solution)/shard_map/ppermute | solution.py:406
  54.5 7.8 %collective-permute-start.13 = (bf16[128,512]{1,0:T(8,128)(2,1)S(1)}, bf16[128,512]{1,0:T(8,128)(2,1)S(1)}, u32[]{:S(2)}, u32[]{:S(2)}) collective-permute-start(bf16[128,512]{1,0:T(8,128)(2,1)S(1)} %fusion.7), channel_id=1, source_target_pairs={{0,16},{2,18},{4,20},{6,22},{8,24},{10,26},{12,28},{14,30},{16,0},... | collective-permute-start | bytes 393224 | tf_op jit(solution)/shard_map/ppermute | solution.py:406
  62.3 18.0 %collective-permute-start.19 = (bf16[512,256]{1,0:T(8,128)(2,1)S(1)}, bf16[512,256]{1,0:T(8,128)(2,1)S(1)}, u32[]{:S(2)}, u32[]{:S(2)}) collective-permute-start(bf16[512,256]{1,0:T(8,128)(2,1)S(1)} %get-tuple-element.60.refs_4_), channel_id=1, source_target_pairs={{0,16},{2,18},{4,20},{6,22},{8,24},{10,26},{12,28},{14,30},{16,0},... | collective-permute-start | bytes 786440 | tf_op jit(solution)/shard_map/ppermute | solution.py:406
  63.6 27.8 %collective-permute-start.18 = (bf16[512,256]{1,0:T(8,128)(2,1)S(1)}, bf16[512,256]{1,0:T(8,128)(2,1)S(1)}, u32[]{:S(2)}, u32[]{:S(2)}) collective-permute-start(bf16[512,256]{1,0:T(8,128)(2,1)S(1)} %get-tuple-element.60.refs_4_), channel_id=1, source_target_pairs={{0,4},{2,6},{4,0},{6,2},{8,12},{10,14},{12,8},{14,10},{16,20},{18,... | collective-permute-start | bytes 786440 | tf_op jit(solution)/shard_map/ppermute | solution.py:406
  64.8 15.5 %collective-permute-start.14 = (bf16[256,512]{1,0:T(8,128)(2,1)S(1)}, bf16[256,512]{1,0:T(8,128)(2,1)S(1)}, u32[]{:S(2)}, u32[]{:S(2)}) collective-permute-start(bf16[256,512]{1,0:T(8,128)(2,1)S(1)} %get-tuple-element.65), channel_id=1, source_target_pairs={{0,2},{2,0},{4,6},{6,4},{8,10},{10,8},{12,14},{14,12},{16,18},{18,... | collective-permute-start | bytes 786440 | tf_op jit(solution)/shard_map/ppermute | solution.py:406
  69.9 21.4 %collective-permute-start.22 = (bf16[512,256]{1,0:T(8,128)(2,1)S(1)}, bf16[512,256]{1,0:T(8,128)(2,1)S(1)}, u32[]{:S(2)}, u32[]{:S(2)}) collective-permute-start(bf16[512,256]{1,0:T(8,128)(2,1)S(1)} %get-tuple-element.59.refs_8_), channel_id=1, source_target_pairs={{0,16},{2,18},{4,20},{6,22},{8,24},{10,26},{12,28},{14,30},{16,0},... | collective-permute-start | bytes 786440 | tf_op jit(solution)/shard_map/ppermute | solution.py:406
  71.7 21.8 %collective-permute-start.10 = (bf16[1024,256]{1,0:T(8,128)(2,1)}, bf16[1024,256]{1,0:T(8,128)(2,1)S(1)}, u32[]{:S(2)}, u32[]{:S(2)}) collective-permute-start(bf16[1024,256]{1,0:T(8,128)(2,1)} %collective-permute-done.9.refs_6_), channel_id=1, source_target_pairs={{0,4},{2,6},{4,0},{6,2},{8,12},{10,14},{12,8},{14,10},{16,20},{18,... | collective-permute-start | bytes 1572872 | tf_op jit(solution)/shard_map/ppermute | solution.py:406
  80.3 11.0 %collective-permute-start.5 = (bf16[128,1024]{1,0:T(8,128)(2,1)}, bf16[128,1024]{1,0:T(8,128)(2,1)S(1)}, u32[]{:S(2)}, u32[]{:S(2)}) collective-permute-start(bf16[128,1024]{1,0:T(8,128)(2,1)} %shard_map.156.refs_0_), channel_id=1, source_target_pairs={{0,8},{2,10},{4,12},{6,14},{8,0},{10,2},{12,4},{14,6},{16,24},{18,... | collective-permute-start | bytes 786440 | tf_op jit(solution)/shard_map/ppermute | solution.py:406
  80.3 11.2 %collective-permute-start.6 = (bf16[128,1024]{1,0:T(8,128)(2,1)}, bf16[128,1024]{1,0:T(8,128)(2,1)S(1)}, u32[]{:S(2)}, u32[]{:S(2)}) collective-permute-start(bf16[128,1024]{1,0:T(8,128)(2,1)} %shard_map.156.refs_0_), channel_id=1, source_target_pairs={{0,2},{2,0},{4,6},{6,4},{8,10},{10,8},{12,14},{14,12},{16,18},{18,... | collective-permute-start | bytes 786440 | tf_op jit(solution)/shard_map/ppermute | solution.py:406
  91.3 8.9 %collective-permute-start.15 = (bf16[128,1024]{1,0:T(8,128)(2,1)}, bf16[128,1024]{1,0:T(8,128)(2,1)S(1)}, u32[]{:S(2)}, u32[]{:S(2)}) collective-permute-start(bf16[128,1024]{1,0:T(8,128)(2,1)} %shard_map.158.refs_0_), channel_id=1, source_target_pairs={{0,8},{2,10},{4,12},{6,14},{8,0},{10,2},{12,4},{14,6},{16,24},{18,... | collective-permute-start | bytes 786440 | tf_op jit(solution)/shard_map/ppermute | solution.py:406
  91.4 13.3 %collective-permute-start.21 = (bf16[512,256]{1,0:T(8,128)(2,1)S(1)}, bf16[512,256]{1,0:T(8,128)(2,1)S(1)}, u32[]{:S(2)}, u32[]{:S(2)}) collective-permute-start(bf16[512,256]{1,0:T(8,128)(2,1)S(1)} %get-tuple-element.59.refs_8_), channel_id=1, source_target_pairs={{0,4},{2,6},{4,0},{6,2},{8,12},{10,14},{12,8},{14,10},{16,20},{18,... | collective-permute-start | bytes 786440 | tf_op jit(solution)/shard_map/ppermute | solution.py:406
  91.5 14.8 %collective-permute-start.20 = (bf16[512,256]{1,0:T(8,128)(2,1)S(1)}, bf16[512,256]{1,0:T(8,128)(2,1)S(1)}, u32[]{:S(2)}, u32[]{:S(2)}) collective-permute-start(bf16[512,256]{1,0:T(8,128)(2,1)S(1)} %collective-permute-done.19.refs_6_), channel_id=1, source_target_pairs={{0,4},{2,6},{4,0},{6,2},{8,12},{10,14},{12,8},{14,10},{16,20},{18,... | collective-permute-start | bytes 786440 | tf_op jit(solution)/shard_map/ppermute | solution.py:406
  93.6 17.8 %collective-permute-start.23 = (bf16[512,256]{1,0:T(8,128)(2,1)S(1)}, bf16[512,256]{1,0:T(8,128)(2,1)S(1)}, u32[]{:S(2)}, u32[]{:S(2)}) collective-permute-start(bf16[512,256]{1,0:T(8,128)(2,1)S(1)} %collective-permute-done.22.refs_10_), channel_id=1, source_target_pairs={{0,4},{2,6},{4,0},{6,2},{8,12},{10,14},{12,8},{14,10},{16,20},{18,... | collective-permute-start | bytes 786440 | tf_op jit(solution)/shard_map/ppermute | solution.py:406
  93.7 17.7 %collective-permute-start.16 = (bf16[128,1024]{1,0:T(8,128)(2,1)}, bf16[128,1024]{1,0:T(8,128)(2,1)}, u32[]{:S(2)}, u32[]{:S(2)}) collective-permute-start(bf16[128,1024]{1,0:T(8,128)(2,1)} %shard_map.158.refs_0_), channel_id=1, source_target_pairs={{0,2},{2,0},{4,6},{6,4},{8,10},{10,8},{12,14},{14,12},{16,18},{18,... | collective-permute-start | bytes 786440 | tf_op jit(solution)/shard_map/ppermute | solution.py:406
  100.2 11.1 %collective-permute-start.17 = (bf16[128,1024]{1,0:T(8,128)(2,1)S(1)}, bf16[128,1024]{1,0:T(8,128)(2,1)}, u32[]{:S(2)}, u32[]{:S(2)}) collective-permute-start(bf16[128,1024]{1,0:T(8,128)(2,1)S(1)} %collective-permute-done.15.refs_1_), channel_id=1, source_target_pairs={{0,2},{2,0},{4,6},{6,4},{8,10},{10,8},{12,14},{14,12},{16,18},{18,... | collective-permute-start | bytes 786440 | tf_op jit(solution)/shard_map/ppermute | solution.py:406
  121.6 6.3 %collective-permute-start.26 = (bf16[64,1024]{1,0:T(8,128)(2,1)}, bf16[64,1024]{1,0:T(8,128)(2,1)S(1)}, u32[]{:S(2)}, u32[]{:S(2)}) collective-permute-start(bf16[64,1024]{1,0:T(8,128)(2,1)} %get-tuple-element.42), channel_id=1, source_target_pairs={{0,9},{1,8},{2,11},{3,10},{4,13},{5,12},{6,15},{7,14},{8,1},{9,0},... | collective-permute-start | bytes 393224 | tf_op jit(solution)/shard_map/ppermute | solution.py:415
  121.9 8.0 %collective-permute-start.28 = (bf16[64,1024]{1,0:T(8,128)(2,1)}, bf16[64,1024]{1,0:T(8,128)(2,1)S(1)}, u32[]{:S(2)}, u32[]{:S(2)}) collective-permute-start(bf16[64,1024]{1,0:T(8,128)(2,1)} %get-tuple-element.44), channel_id=1, source_target_pairs={{0,3},{1,2},{2,1},{3,0},{4,7},{5,6},{6,5},{7,4},{8,11},{9,10},{10,... | collective-permute-start | bytes 393224 | tf_op jit(solution)/shard_map/ppermute | solution.py:415
  126.2 6.9 %collective-permute-start.30 = (bf16[64,1024]{1,0:T(8,128)(2,1)}, bf16[64,1024]{1,0:T(8,128)(2,1)S(1)}, u32[]{:S(2)}, u32[]{:S(2)}) collective-permute-start(bf16[64,1024]{1,0:T(8,128)(2,1)} %get-tuple-element.46), channel_id=1, source_target_pairs={{0,11},{1,10},{2,9},{3,8},{4,15},{5,14},{6,13},{7,12},{8,3},{9,2},... | collective-permute-start | bytes 393224 | tf_op jit(solution)/shard_map/ppermute | solution.py:415
  (40 other events, 419.8 us)

commit v4 on v3

--- a/solution.py
+++ b/solution.py
@@ -22,6 +22,12 @@
 BF16 = jnp.bfloat16
 VMEM = pl.BlockSpec(memory_space=pltpu.VMEM)
 SMEM = pl.BlockSpec(memory_space=pltpu.SMEM)
+
+
+LIMIT = 16 * 2**20
+STAGGERED = ()
+PARTS = 1
+LATE = 2
 
 
 def call(kernel, outs, ins, flops, scratch=(), scalars=0):
@@ -33,6 +39,7 @@
         out_specs=[VMEM] * len(outs),
         scratch_shapes=list(scratch),
         cost_estimate=pl.CostEstimate(flops=flops, bytes_accessed=moved, transcendentals=0),
+        compiler_params=pltpu.CompilerParams(vmem_limit_bytes=LIMIT),
     )(*ins)
 
 
@@ -123,7 +130,12 @@
     run_f = nn(logs[0:heads], jnp.where(upper, 1.0, 0.0), HIGHEST)
     run_b = nn(logs[heads : 2 * heads], jnp.where(lower, 1.0, 0.0), HIGHEST)
     tall = jnp.concatenate([run_f, run_b], axis=0).T
-    expl_ref[...] = jnp.exp(tall)
+    grown = jnp.exp(tall)
+    coarse = grown.astype(BF16)
+    fine = (grown - coarse.astype(F32)).astype(BF16)
+    expl_ref[...] = jnp.concatenate(
+        [coarse[:, 0:heads], fine[:, 0:heads], coarse[:, heads:], fine[:, heads:]], axis=1
+    )
     tot_f = run_f[:, rows - 1 : rows]
     tot_b = run_b[:, 0:1]
     end_f = jnp.exp(tot_f - run_f) * steps[0:heads]
@@ -138,17 +150,7 @@
     tail = jnp.concatenate(
         [high.astype(F32), low.astype(F32), jnp.zeros((EDGE - 4, cols), F32)], axis=0
     ).astype(BF16)
-    for side in range(2):
-        part = tail[:, side * half : (side + 1) * half]
-
-        @pl.when(core == side)
-        def _():
-            keep_ref[2 * STATE : 2 * STATE + EDGE, :] = part
-
-        @pl.when(core != side)
-        def _():
-            send_ref[2 * STATE : 2 * STATE + EDGE, :] = part
-
+    bodies = []
     for g in range(groups):
         wg = ws[:, g * STATE : (g + 1) * STATE]
         rg = read_ref[:, g * STATE : (g + 1) * STATE]
@@ -172,23 +174,12 @@
             got = nn(jnp.concatenate([mixed, grow_f, grow_b], axis=0), xs[:, at : at + SSD_HEAD])
             y_ref[:, at : at + SSD_HEAD] = got[0:rows]
             fresh.append(got[rows : rows + 2 * STATE].astype(BF16))
-        whole = jnp.concatenate(fresh, axis=1)
-        size = per * SSD_HEAD
-        base = g * size
-        for side in range(2):
-            a = max(base, side * half)
-            b = min(base + size, (side + 1) * half)
-            if a >= b:
-                continue
-            part = whole[:, a - base : b - base]
-
-            @pl.when(core == side)
-            def _():
-                keep_ref[0 : 2 * STATE, a - side * half : b - side * half] = part
-
-            @pl.when(core != side)
-            def _():
-                send_ref[0 : 2 * STATE, a - side * half : b - side * half] = part
+        bodies.append(jnp.concatenate(fresh, axis=1))
+    whole = jnp.concatenate([jnp.concatenate(bodies, axis=1), tail], axis=0)
+    near = whole[:, :half].astype(F32)
+    away = whole[:, half:].astype(F32)
+    keep_ref[...] = jnp.where(core == 0, near, away).astype(BF16)
+    send_ref[...] = jnp.where(core == 0, away, near).astype(BF16)
 
 
 def attend_kernel(
@@ -259,7 +250,8 @@
     groups = wide // STATE
     size = cols // groups
     half = cols // 2
-    spread = head_spread(heads, cols)
+    spread = head_spread(heads, cols).astype(BF16)
+    spread = jnp.concatenate([spread, spread], axis=0)
     for g in range(groups):
         at = g * size
         rg = read_ref[:, g * STATE : (g + 1) * STATE]
@@ -278,8 +270,8 @@
             )
         states = pieces[0] if len(pieces) == 1 else jnp.concatenate(pieces, axis=1)
         local = spread[:, at : at + size]
-        fade_f = nn(expl_ref[:, 0:heads], local, HIGHEST)
-        fade_b = nn(expl_ref[:, heads : 2 * heads], local, HIGHEST)
+        fade_f = nn(expl_ref[:, 0 : 2 * heads], local)
+        fade_b = nn(expl_ref[:, 2 * heads : 4 * heads], local)
         both = (
             y_ref[:, at : at + size]
             + fade_f * nn(rg, states[0:STATE])
@@ -304,49 +296,63 @@
         at += span
 
 
-def second_kernel(count, sum_ref, *refs):
+def second_kernel(count, base, sum_ref, *refs):
     place = lax.axis_index("tp")
-    blocks, shards, base = count
+    blocks, shards = count
     lefts = refs[:blocks]
-    tops = refs[blocks : blocks + shards]
-    lows = refs[blocks + shards : blocks + 2 * shards]
-    outs = refs[blocks + 2 * shards :]
+    pieces = refs[blocks : blocks + 2 * shards]
+    outs = refs[blocks + 2 * shards : -3]
+    held, early, sems = refs[-3:]
     rows = lefts[0].shape[0]
     half = rows // 2
-    deep = tops[0].shape[0]
+    deep, span = pieces[0].shape
+    whole = deep + pieces[shards].shape[0]
+    copies = []
+    for j in range(shards):
+        for k in range(2):
+            i = 2 * j + k
+            copies.append(
+                pltpu.make_async_copy(
+                    pieces[k * shards + j],
+                    held.at[j, 0:deep] if k == 0 else held.at[j, deep:whole],
+                    sems.at[i],
+                )
+            )
+        at = j * span
+        copies.append(
+            pltpu.make_async_copy(
+                sum_ref.at[:, base + at : base + at + span], early.at[j], sems.at[2 * shards + j]
+            )
+        )
+    for copy in copies:
+        copy.start()
     left = jnp.concatenate([a[...] for a in lefts], axis=0)
-    at = 0
-    for top, low in zip(tops, lows):
-        span = top.shape[1]
-        total = (
-            sum_ref[:, base + at : base + at + span]
-            + nn(left[:, :deep], top[...])
-            + nn(left[:, deep:], low[...])
-        ).astype(BF16)
-        for side in range(2):
-
-            @pl.when(place == side)
-            def _():
-                for i in range(blocks):
-                    a = i * rows + side * half
-                    b = i * rows + (1 - side) * half
-                    outs[2 * i][:, at : at + span] = total[a : a + half]
-                    outs[2 * i + 1][:, at : at + span] = total[b : b + half]
-
-        at += span
-
-
-def place_kernel(group, masks, span, *refs):
+    for j in range(shards):
+        at = j * span
+        for copy in copies[3 * j : 3 * j + 3]:
+            copy.wait()
+        total = early[j] + nn(left, held[j])
+        for i in range(blocks):
+            top = total[i * rows : i * rows + half]
+            low = total[i * rows + half : (i + 1) * rows]
+            outs[2 * i][:, at : at + span] = jnp.where(place == 0, top, low).astype(BF16)
+            outs[2 * i + 1][:, at : at + span] = jnp.where(place == 0, low, top).astype(BF16)
+
+
+def place_kernel(group, parts, span, *refs):
     me = lax.axis_index("sp")
     out_ref = refs[-1]
-    for i, block in enumerate(group):
-        for j, mask in enumerate(masks):
-            at = j * span
-            to = pl.multiple_of((me ^ (block ^ mask)) * span, span)
-            out_ref[:, pl.ds(to, span)] = (
-                refs[2 * i][:, at : at + span].astype(F32)
-                + refs[2 * i + 1][:, at : at + span].astype(F32)
-            ).astype(BF16)
+    at = 0
+    for masks in parts:
+        for block in group:
+            for j, mask in enumerate(masks):
+                low = j * span
+                to = pl.multiple_of((me ^ (block ^ mask)) * span, span)
+                out_ref[:, pl.ds(to, span)] = (
+                    refs[at][:, low : low + span].astype(F32)
+                    + refs[at + 1][:, low : low + span].astype(F32)
+                ).astype(BF16)
+            at += 2
 
 
 def edge_kernel(*refs):
@@ -374,6 +380,7 @@
         out_shape=[jax.ShapeDtypeStruct((EDGE, width), BF16)] * 2,
         in_specs=specs,
         out_specs=[pl.BlockSpec((EDGE, width), lambda i: (0, 0))] * 2,
+        compiler_params=pltpu.CompilerParams(vmem_limit_bytes=LIMIT),
         name="edges",
     )(*[a for a in raw for _ in range(2)])
 
@@ -426,79 +433,104 @@
     return payload
 
 
-def exchange_states(keep, send, count, me):
+def tails(ref):
+    end = 2 * STATE
+    tail = ref[end : end + EDGE, :].astype(F32)
+    return tail[0:2] + tail[2:4]
+
+
+def merge_kernel(bit, first, closing, *refs):
+    me = lax.axis_index("sp")
+    upper = (me & bit) != 0
+    end = 2 * STATE
+    own_ref, other_ref = refs[0], refs[1]
+    carry_ref = None if first else refs[2]
+    out_ref, next_ref = refs[-2:]
+    mine, theirs = tails(own_ref), tails(other_ref)
+    own_f, own_b = own_ref[0:STATE, :].astype(F32), own_ref[STATE:end, :].astype(F32)
+    far_f, far_b = other_ref[0:STATE, :].astype(F32), other_ref[STATE:end, :].astype(F32)
+    zero = jnp.zeros_like(own_f)
+    if first:
+        gap_f = gap_b = jnp.ones_like(mine[0:1])
+        next_ref[0:STATE, :] = jnp.where(upper, far_f, zero)
+        next_ref[STATE:end, :] = jnp.where(upper, zero, far_b)
+    else:
+        gap_f = carry_ref[end : end + 1, :]
+        gap_b = carry_ref[end + 1 : end + 2, :]
+        next_ref[0:STATE, :] = carry_ref[0:STATE, :] + jnp.where(upper, far_f * gap_f, zero)
+        next_ref[STATE:end, :] = carry_ref[STATE:end, :] + jnp.where(upper, zero, far_b * gap_b)
+    gap_f = jnp.where(upper, gap_f * theirs[0:1], gap_f)
+    gap_b = jnp.where(upper, gap_b, gap_b * theirs[1:2])
+    pad = jnp.zeros((6, gap_f.shape[1]), F32)
+    next_ref[end : end + 8, :] = jnp.concatenate([gap_f, gap_b, pad], axis=0)
+    low_f, high_f = jnp.where(upper, far_f, own_f), jnp.where(upper, own_f, far_f)
+    low_b, high_b = jnp.where(upper, far_b, own_b), jnp.where(upper, own_b, far_b)
+    low, high = jnp.where(upper, theirs, mine), jnp.where(upper, mine, theirs)
+    total_f = low_f * high[0:1] + high_f
+    total_b = high_b * low[1:2] + low_b
+    if closing:
+        out_ref[...] = jnp.where((me & (2 * bit)) != 0, total_b, total_f).astype(BF16)
+        return
+    out_ref[0:STATE, :] = total_f.astype(BF16)
+    out_ref[STATE:end, :] = total_b.astype(BF16)
+    fades = low * high
+    top = fades.astype(BF16).astype(F32)
+    pad = jnp.zeros((EDGE - 4, fades.shape[1]), F32)
+    out_ref[end : end + EDGE, :] = jnp.concatenate([top, fades - top, pad], axis=0).astype(BF16)
+
+
+def close_kernel(bit, other_ref, carry_ref, keep_ref, got_ref, own_ref, away_ref):
+    me = lax.axis_index("sp")
+    upper = (me & bit) != 0
+    even = (me & 1) == 0
+    end = 2 * STATE
+    other = other_ref[...].astype(F32)
+    zero = jnp.zeros_like(other)
+    gap_f = carry_ref[end : end + 1, :]
+    gap_b = carry_ref[end + 1 : end + 2, :]
+    into_f = carry_ref[0:STATE, :] + jnp.where(upper, other * gap_f, zero)
+    into_b = carry_ref[STATE:end, :] + jnp.where(upper, zero, other * gap_b)
+    mine, theirs = tails(keep_ref), tails(got_ref)
+    keep_f, keep_b = keep_ref[0:STATE, :].astype(F32), keep_ref[STATE:end, :].astype(F32)
+    got_f, got_b = got_ref[0:STATE, :].astype(F32), got_ref[STATE:end, :].astype(F32)
+    low_f = jnp.where(even, keep_f, got_f)
+    high_b = jnp.where(even, got_b, keep_b)
+    low, high = jnp.where(even, mine, theirs), jnp.where(even, theirs, mine)
+    second_f = into_f * low[0:1] + low_f
+    first_b = into_b * high[1:2] + high_b
+    own_ref[0:STATE, :] = jnp.where(even, into_f, second_f).astype(BF16)
+    own_ref[STATE:end, :] = jnp.where(even, first_b, into_b).astype(BF16)
+    away_ref[0:STATE, :] = jnp.where(even, second_f, into_f).astype(BF16)
+    away_ref[STATE:end, :] = jnp.where(even, into_b, first_b).astype(BF16)
+
+
+def exchange_states(keep, send, count):
     half = keep.shape[1]
-    core = me & 1
+    sds = jax.ShapeDtypeStruct
     got = flip(send, count, 1)
-
-    def split(a):
-        tail = a[2 * STATE :].astype(F32)
-        return (
-            a[:STATE].astype(F32),
-            a[STATE : 2 * STATE].astype(F32),
-            tail[0:1] + tail[2:3],
-            tail[1:2] + tail[3:4],
+    seen = payload = join_pair(keep, got)
+    carry = None
+    bit = 2
+    while 2 * bit < count:
+        other = flip(payload, count, bit)
+        closing = 4 * bit >= count
+        payload, carry = call(
+            functools.partial(merge_kernel, bit, carry is None, closing),
+            [
+                sds((STATE, half) if closing else keep.shape, BF16),
+                sds((2 * STATE + 8, half), F32),
+            ],
+            [payload, other] + ([] if carry is None else [carry]),
+            flops=10**6,
         )
-
-    pick = lambda flag, a, b: jax.tree.map(lambda u, v: jnp.where(flag, u, v), a, b)
-    join = lambda low, high: (
-        low[0] * high[2] + high[0],
-        high[1] * low[3] + low[1],
-        low[2] * high[2],
-        low[3] * high[3],
-    )
-
-    def pack(total):
-        fades = jnp.concatenate([total[2], total[3]], axis=0)
-        top = fades.astype(BF16)
-        rest = (fades - top.astype(F32)).astype(BF16)
-        return jnp.concatenate(
-            [
-                total[0].astype(BF16),
-                total[1].astype(BF16),
-                top,
-                rest,
-                jnp.zeros((EDGE - 4, half), BF16),
-            ],
-            axis=0,
-        )
-
-    seen = payload = join_pair(keep, got)
-    total = split(payload)
-    into_f = jnp.zeros((STATE, half), F32)
-    into_b = jnp.zeros((STATE, half), F32)
-    gap_f = jnp.ones((1, half), F32)
-    gap_b = jnp.ones((1, half), F32)
-    bit = 2
-    while bit < count:
-        upper = (me & bit) != 0
-        last = bit * 2 >= count
-        if last:
-            payload = jnp.where(upper, total[1], total[0]).astype(BF16)
-            other = flip(payload, count, bit).astype(F32)
-            into_f = jnp.where(upper, other * gap_f + into_f, into_f)
-            into_b = jnp.where(upper, into_b, other * gap_b + into_b)
-        else:
-            if payload is None:
-                payload = pack(total)
-            other = split(flip(payload, count, bit))
-            payload = None
-            low = pick(upper, other, total)
-            high = pick(upper, total, other)
-            into_f = jnp.where(upper, other[0] * gap_f + into_f, into_f)
-            into_b = jnp.where(upper, into_b, other[1] * gap_b + into_b)
-            gap_f = jnp.where(upper, gap_f * other[2], gap_f)
-            gap_b = jnp.where(upper, gap_b, gap_b * other[3])
-            total = join(low, high)
         bit *= 2
-    keep, got = lax.optimization_barrier((keep, got, seen))[:2]
-    mine, theirs = split(keep), split(got)
-    low = pick(core == 0, mine, theirs)
-    high = pick(core == 0, theirs, mine)
-    first = jnp.concatenate([into_f, into_b * high[3] + high[1]], axis=0).astype(BF16)
-    second = jnp.concatenate([into_f * low[2] + low[0], into_b], axis=0).astype(BF16)
-    own = jnp.where(core == 0, first, second)
-    away = jnp.where(core == 0, second, first)
+    other = flip(payload, count, bit)
+    own, away = call(
+        functools.partial(close_kernel, bit),
+        [sds((2 * STATE, half), BF16)] * 2,
+        [other, carry, keep, got],
+        flops=10**6,
+    )
     return own, flip(away, count, 1), seen
 
 
@@ -544,14 +576,26 @@
             bits.append(bit)
         bit //= 2
 
-    def gather(piece):
+    def turns(a):
+        got = []
+        for turn in range(2):
+            pairs = [(i, i ^ 8) for i in range(count) if ((i >> 2) & 1) == turn]
+            got.append(lax.ppermute(a, "sp", pairs))
+        return jnp.where((me & 4) == 0, got[0], got[1])
+
+    def gather(part, piece):
         shards = {0: piece}
         for bit in bits:
             for mask in list(shards):
-                shards[mask ^ bit] = flip(shards[mask], count, bit)
+                if fast and bit == 8 and part in STAGGERED:
+                    shards[mask ^ bit] = turns(shards[mask])
+                else:
+                    shards[mask ^ bit] = flip(shards[mask], count, bit)
         return shards
 
-    halves = [gather(final_mapping_matrix[0])]
+    deepest = final_mapping_matrix.shape[1]
+    middle = deepest - deepest // LATE
+    halves = [gather(0, final_mapping_matrix[0])]
     masks = sorted(halves[0])
 
     keep, send, read, inner, expl = call(
@@ -561,7 +605,7 @@
             sds((2 * STATE + EDGE, cols // 2), BF16),
             sds((rows, wide), BF16),
             sds((rows, cols), F32),
-            sds((rows, 2 * heads), F32),
+            sds((rows, 4 * heads), BF16),
         ],
         [
             *raw,
@@ -581,14 +625,12 @@
             pltpu.VMEM((rows, wide), BF16),
         ],
     )
-    own_state, got_state, seen = exchange_states(keep, send, count, me)
-    later, weights, matching_key, carried_value = lax.optimization_barrier(
+    own_state, got_state, seen = exchange_states(keep, send, count)
+    later, weights, _, _ = lax.optimization_barrier(
         (me, final_mapping_matrix, matching_key_matrix, carried_value_matrix, seen)
     )[:4]
-    right_rows = weights[1]
-    middle = right_rows.shape[0] // 2
-    halves += [gather(right_rows[:middle]), gather(right_rows[middle:])]
-    pairs = jnp.concatenate([matching_key, carried_value], axis=1)
+    halves += [gather(1, weights[1, :middle]), gather(2, weights[1, middle:])]
+    pairs = jnp.concatenate([matching_key_matrix, carried_value_matrix], axis=1)
     pair_kv = flip(pairs, count, 1)
     outer_kv = outer(pairs, count)
 
@@ -652,26 +694,35 @@
             flops=flops,
         )
         pieces = []
-        cut = len(masks)
-        for turn, chosen in enumerate((masks,)):
+        cut = len(masks) // PARTS
+        parted = [masks[i : i + cut] for i in range(0, len(masks), cut)]
+        for turn, chosen in enumerate(parted):
             wide_part = span * len(chosen)
-            outs = call(
-                functools.partial(second_kernel, (len(group), len(chosen), turn * span * cut)),
-                [sds((rows // 2, wide_part), BF16)] * (2 * len(group)),
-                [
-                    early,
-                    *normed_blocks,
-                    *[halves[1][m] for m in chosen],
-                    *[halves[2][m] for m in chosen],
+            parts = [halves[1][m] for m in chosen] + [halves[2][m] for m in chosen]
+            anywhere = pl.BlockSpec(memory_space=pl.ANY)
+            deep = parts[0].shape[0] + parts[-1].shape[0]
+            outs = pl.pallas_call(
+                functools.partial(second_kernel, (len(group), len(chosen)), turn * cut * span),
+                out_shape=[sds((rows // 2, wide_part), BF16)] * (2 * len(group)),
+                in_specs=[anywhere] + [VMEM] * len(group) + [anywhere] * len(parts),
+                out_specs=[VMEM] * (2 * len(group)),
+                scratch_shapes=[
+                    pltpu.VMEM((len(chosen), deep, span), BF16),
+                    pltpu.VMEM((len(chosen), len(group) * rows, span), F32),
+                    pltpu.SemaphoreType.DMA((len(parts) + len(chosen),)),
                 ],
-                flops=flops,
-            )
+                cost_estimate=pl.CostEstimate(
+                    flops=flops // PARTS, bytes_accessed=6 * 2**20, transcendentals=0
+                ),
+                compiler_params=pltpu.CompilerParams(vmem_limit_bytes=LIMIT),
+                name="second",
+            )(early, *normed_blocks, *parts)
             for i, m in enumerate(group):
                 kept, gone = outs[2 * i], outs[2 * i + 1]
                 pieces.append(kept if m == 0 else flip(kept, count, m))
                 pieces.append(cross(gone, count, m))
         (out,) = call(
-            functools.partial(place_kernel, group, masks, span),
+            functools.partial(place_kernel, group, parted, span),
             [sds((rows // 2, span * count), BF16)],
             pieces,
             flops=10**6,

time: 136 us -> 131 us (0.963)
  Pallas kernels: 31 us -> 13.8 us
  starting transfers between devices: 32.9 us -> 46 us
  other arithmetic: 5.83 us -> 0.95 us
  waiting for transfers between devices: 57.8 us -> 60.8 us
    pallas_call x7 -> x9, Pallas kernels: 29.5 us -> 10.3 us  [call(): pl.pallas_call(kernel, out_shape=outs, in_specs=[SMEM] * scalars + [VMEM]...]
    ppermute x25, starting transfers between devices: 26.9 us -> 37.2 us  [flip(): return lax.ppermute(a, 'sp', [(i, i ^ mask) for i in range(count)])]
    ppermute x25, waiting for transfers between devices: 51.4 us -> 56 us  [flip(): return lax.ppermute(a, 'sp', [(i, i ^ mask) for i in range(count)])]
    unnamed x67 -> x43, local copies, waits for them, and re-layouts: 4.03 us -> 7.76 us
    pallas_call x0 -> x1, Pallas kernels: none -> 3.43 us  [local(): pl.pallas_call(functools.partial(second_kernel, (len(group), len(chosen))...]
    concatenate x2 -> x1, local copies, waits for them, and re-layouts: 3.9 us -> 0.67 us  [local(): pairs = jnp.concatenate([matching_key_matrix, carried_value_matrix], axis=1)]
    ppermute x4, starting transfers between devices: 3.95 us -> 6.7 us  [cross(): lax.ppermute(a, ('sp', 'tp'), [(2 * i + j, 2 * (i ^ mask) + 1 - j) for i...]
    convert_element_type x8 -> x0, other arithmetic: 2.09 us -> none  [the longest x1 1.09 us: pack(): total[1].astype(BF16)]
  transfers between devices with their start and end apart: 31 -> 31, of which waited for: 14 -> 15; matrix products, arithmetic and copies ran while one was open for 8% -> 2% of each run, Pallas kernels for 11% -> 5%
where the time goes in v4:
time: 131 us; the launch traced here: 130 us
  waiting for transfers between devices  60.8 us (46%)
  starting transfers between devices  46 us (35%)
  Pallas kernels  13.8 us (11%)
  local copies, waits for them, and re-layouts  8.5 us (6%)
    ppermute x25, waiting for transfers between devices, flip(): return lax.ppermute(a, 'sp', [(i, i ^ mask) for i in range(count)])  56 us
    ppermute x25, starting transfers between devices, flip(): return lax.ppermute(a, 'sp', [(i, i ^ mask) for i in range(count)])  37.2 us
    pallas_call x9, Pallas kernels, call(): pl.pallas_call(kernel, out_shape=outs, in_specs=[SMEM] * scalars + [VMEM]...  10.3 us
    unnamed x43, local copies, waits for them, and re-layouts  7.76 us
    ppermute x4, starting transfers between devices, cross(): lax.ppermute(a, ('sp', 'tp'), [(2 * i + j, 2 * (i ^ mask) + 1 - j) for i...  6.7 us
    ppermute x4, waiting for transfers between devices, cross(): lax.ppermute(a, ('sp', 'tp'), [(2 * i + j, 2 * (i ^ mask) + 1 - j) for i...  4.77 us
    pallas_call x1, Pallas kernels, local(): pl.pallas_call(functools.partial(second_kernel, (len(group), len(chosen))...  3.43 us
  transfers between devices with their start and end apart: 31, of which 15 were waited for; matrix products, arithmetic and copies ran while one was open for 2% of the time, Pallas kernels for 5%

profile of v4, /device:TPU:0, one launch (start us, length us, event | category | flops | bytes accessed | tf_op | source)
XLA Modules:
  0.0 130.3 jit_solution(3247494324057530525)
XLA Ops:
  8.5 2.7 %shard_map.154 = (bf16[272,512]{1,0:T(8,128)(2,1)S(1)}, bf16[272,512]{1,0:T(8,128)(2,1)S(1)}, bf16[128,512]{1,0:T(8,128)(2,1)S(1)}, f32[128,1024]{1,0:T(8,128)S(1)}, bf16[128,64]{1,0:T(8,128)(2,1)S(1)}) custom-call(bf16[128,1024]{1,0:T(8,128)(2,1)S(1)} %copy-done, bf16[128,512]{1,0:T(8,128)(2,1)S(1)} %copy-done.1, bf16[128,512]{1,0:T(8,128)(2,1)S(1)} %copy-done.2, ...), custom_call_target="tpu_custom_call" | custom-call | flops 4000000000 | bytes 1937536 | tf_op jit(solution)/shard_map/pallas_call | solution.py:35
  11.3 5.6 %collective-permute-start.4 = (bf16[272,512]{1,0:T(8,128)(2,1)S(1)}, bf16[272,512]{1,0:T(8,128)(2,1)S(1)}, u32[]{:S(2)}, u32[]{:S(2)}) collective-permute-start(bf16[272,512]{1,0:T(8,128)(2,1)S(1)} %get-tuple-element.31), channel_id=1, source_target_pairs={{0,2},{2,0},{4,6},{6,4},{8,10},{10,8},{12,14},{14,12},{16,18},{18,... | collective-permute-start | bytes 835592 | tf_op jit(solution)/shard_map/ppermute | solution.py:413
  20.0 3.8 %collective-permute-start.11 = (bf16[272,512]{1,0:T(8,128)(2,1)S(1)}, bf16[272,512]{1,0:T(8,128)(2,1)S(1)}, u32[]{:S(2)}, u32[]{:S(2)}) collective-permute-start(bf16[272,512]{1,0:T(8,128)(2,1)S(1)} %shard_map.155.refs_0_), channel_id=1, source_target_pairs={{0,4},{2,6},{4,0},{6,2},{8,12},{10,14},{12,8},{14,10},{16,20},{18,... | collective-permute-start | bytes 835592 | tf_op jit(solution)/shard_map/ppermute | solution.py:413
  23.8 3.0 %collective-permute-start.9 = (bf16[1024,256]{1,0:T(8,128)(2,1)S(1)}, bf16[1024,256]{1,0:T(8,128)(2,1)S(1)}, u32[]{:S(2)}, u32[]{:S(2)}) collective-permute-start(bf16[1024,256]{1,0:T(8,128)(2,1)S(1)} %slice_bitcast_fusion.refs_4_), channel_id=1, source_target_pairs={{0,16},{2,18},{4,20},{6,22},{8,24},{10,26},{12,28},{14,30},{16,0},... | collective-permute-start | bytes 1572872 | tf_op jit(solution)/shard_map/ppermute | solution.py:413
  28.4 6.8 %collective-permute-done.11.refs_1_ = bf16[272,512]{1,0:T(8,128)(2,1)S(1)} collective-permute-done((bf16[272,512]{1,0:T(8,128)(2,1)S(1)}, bf16[272,512]{1,0:T(8,128)(2,1)S(1)}, u32[]{:S(2)}, u32[]{:S(2)}) %collective-permute-start.11) | collective-permute-done | bytes 278560 | tf_op jit(solution)/shard_map/ppermute | solution.py:413
  35.4 5.5 %collective-permute-start.12 = (bf16[272,512]{1,0:T(8,128)(2,1)S(1)}, bf16[272,512]{1,0:T(8,128)(2,1)S(1)}, u32[]{:S(2)}, u32[]{:S(2)}) collective-permute-start(bf16[272,512]{1,0:T(8,128)(2,1)S(1)} %get-tuple-element.36.refs_0_), channel_id=1, source_target_pairs={{0,8},{2,10},{4,12},{6,14},{8,0},{10,2},{12,4},{14,6},{16,24},{18,... | collective-permute-start | bytes 835592 | tf_op jit(solution)/shard_map/ppermute | solution.py:413
  41.9 14.5 %collective-permute-done.12.refs_1_ = bf16[272,512]{1,0:T(8,128)(2,1)S(1)} collective-permute-done((bf16[272,512]{1,0:T(8,128)(2,1)S(1)}, bf16[272,512]{1,0:T(8,128)(2,1)S(1)}, u32[]{:S(2)}, u32[]{:S(2)}) %collective-permute-start.12) | collective-permute-done | bytes 278560 | tf_op jit(solution)/shard_map/ppermute | solution.py:413
  56.7 4.1 %shard_map.156.refs_0_ = bf16[128,1024]{1,0:T(8,128)(2,1)S(1)} custom-call(f32[8]{0:T(128)S(1)} %copy-done.14, bf16[128,1024]{1,0:T(8,128)(2,1)S(1)} %copy-done.5, bf16[128,512]{1,0:T(8,128)(2,1)S(1)} %copy-done.3, bf16[128,512]{1,0:T(8,128)(2,1)S(1)} %copy-done.4, bf16[128,1024]{1,0:T(8,128)(2,1)S(1)} %collective-permute-done.pair_ref, ...), custom_call_target="tpu_custom_call" | custom-call | flops 3000000000 | bytes 1703968 | tf_op jit(solution)/shard_map/pallas_call | solution.py:35
  60.8 1.9 %collective-permute-start.5 = (bf16[128,1024]{1,0:T(8,128)(2,1)S(1)}, bf16[128,1024]{1,0:T(8,128)(2,1)S(1)}, u32[]{:S(2)}, u32[]{:S(2)}) collective-permute-start(bf16[128,1024]{1,0:T(8,128)(2,1)S(1)} %shard_map.156.refs_0_), channel_id=1, source_target_pairs={{0,8},{2,10},{4,12},{6,14},{8,0},{10,2},{12,4},{14,6},{16,24},{18,... | collective-permute-start | bytes 786440 | tf_op jit(solution)/shard_map/ppermute | solution.py:413
  64.8 2.8 %collective-permute-start.18 = (bf16[512,256]{1,0:T(8,128)(2,1)S(1)}, bf16[512,256]{1,0:T(8,128)(2,1)S(1)}, u32[]{:S(2)}, u32[]{:S(2)}) collective-permute-start(bf16[512,256]{1,0:T(8,128)(2,1)S(1)} %get-tuple-element.52.refs_4_), channel_id=1, source_target_pairs={{0,4},{2,6},{4,0},{6,2},{8,12},{10,14},{12,8},{14,10},{16,20},{18,... | collective-permute-start | bytes 786440 | tf_op jit(solution)/shard_map/ppermute | solution.py:413
  67.6 2.5 %collective-permute-done.5.refs_1_ = bf16[128,1024]{1,0:T(8,128)(2,1)S(1)} collective-permute-done((bf16[128,1024]{1,0:T(8,128)(2,1)S(1)}, bf16[128,1024]{1,0:T(8,128)(2,1)S(1)}, u32[]{:S(2)}, u32[]{:S(2)}) %collective-permute-start.5) | collective-permute-done | bytes 262176 | tf_op jit(solution)/shard_map/ppermute | solution.py:413
  70.1 2.5 %collective-permute-start.22 = (bf16[512,256]{1,0:T(8,128)(2,1)S(1)}, bf16[512,256]{1,0:T(8,128)(2,1)S(1)}, u32[]{:S(2)}, u32[]{:S(2)}) collective-permute-start(bf16[512,256]{1,0:T(8,128)(2,1)S(1)} %get-tuple-element.51.refs_8_), channel_id=1, source_target_pairs={{0,16},{2,18},{4,20},{6,22},{8,24},{10,26},{12,28},{14,30},{16,0},... | collective-permute-start | bytes 786440 | tf_op jit(solution)/shard_map/ppermute | solution.py:413
  72.7 2.3 %collective-permute-start.10 = (bf16[1024,256]{1,0:T(8,128)(2,1)S(1)}, bf16[1024,256]{1,0:T(8,128)(2,1)S(1)}, u32[]{:S(2)}, u32[]{:S(2)}) collective-permute-start(bf16[1024,256]{1,0:T(8,128)(2,1)S(1)} %collective-permute-done.9.refs_6_), channel_id=1, source_target_pairs={{0,4},{2,6},{4,0},{6,2},{8,12},{10,14},{12,8},{14,10},{16,20},{18,... | collective-permute-start | bytes 1572872 | tf_op jit(solution)/shard_map/ppermute | solution.py:413
  75.6 9.0 %collective-permute-done.19.refs_6_ = bf16[512,256]{1,0:T(8,128)(2,1)S(1)} collective-permute-done((bf16[512,256]{1,0:T(8,128)(2,1)S(1)}, bf16[512,256]{1,0:T(8,128)(2,1)S(1)}, u32[]{:S(2)}, u32[]{:S(2)}) %collective-permute-start.19) | collective-permute-done | bytes 262176 | tf_op jit(solution)/shard_map/ppermute | solution.py:413
  84.6 5.5 %collective-permute-done.22.refs_10_ = bf16[512,256]{1,0:T(8,128)(2,1)S(1)} collective-permute-done((bf16[512,256]{1,0:T(8,128)(2,1)S(1)}, bf16[512,256]{1,0:T(8,128)(2,1)S(1)}, u32[]{:S(2)}, u32[]{:S(2)}) %collective-permute-start.22) | collective-permute-done | bytes 262176 | tf_op jit(solution)/shard_map/ppermute | solution.py:413
  90.1 4.0 %collective-permute-start.21 = (bf16[512,256]{1,0:T(8,128)(2,1)S(1)}, bf16[512,256]{1,0:T(8,128)(2,1)S(1)}, u32[]{:S(2)}, u32[]{:S(2)}) collective-permute-start(bf16[512,256]{1,0:T(8,128)(2,1)S(1)} %get-tuple-element.51.refs_8_), channel_id=1, source_target_pairs={{0,4},{2,6},{4,0},{6,2},{8,12},{10,14},{12,8},{14,10},{16,20},{18,... | collective-permute-start | bytes 786440 | tf_op jit(solution)/shard_map/ppermute | solution.py:413
  94.1 2.0 %collective-permute-start.23 = (bf16[512,256]{1,0:T(8,128)(2,1)S(1)}, bf16[512,256]{1,0:T(8,128)(2,1)S(1)}, u32[]{:S(2)}, u32[]{:S(2)}) collective-permute-start(bf16[512,256]{1,0:T(8,128)(2,1)S(1)} %collective-permute-done.22.refs_10_), channel_id=1, source_target_pairs={{0,4},{2,6},{4,0},{6,2},{8,12},{10,14},{12,8},{14,10},{16,20},{18,... | collective-permute-start | bytes 786440 | tf_op jit(solution)/shard_map/ppermute | solution.py:413
  97.9 3.3 %collective-permute-done.21.refs_9_ = bf16[512,256]{1,0:T(8,128)(2,1)S(1)} collective-permute-done((bf16[512,256]{1,0:T(8,128)(2,1)S(1)}, bf16[512,256]{1,0:T(8,128)(2,1)S(1)}, u32[]{:S(2)}, u32[]{:S(2)}) %collective-permute-start.21) | collective-permute-done | bytes 262176 | tf_op jit(solution)/shard_map/ppermute | solution.py:413
  101.2 5.6 %collective-permute-done.20.refs_7_ = bf16[512,256]{1,0:T(8,128)(2,1)S(1)} collective-permute-done((bf16[512,256]{1,0:T(8,128)(2,1)S(1)}, bf16[512,256]{1,0:T(8,128)(2,1)S(1)}, u32[]{:S(2)}, u32[]{:S(2)}) %collective-permute-start.20) | collective-permute-done | bytes 262176 | tf_op jit(solution)/shard_map/ppermute | solution.py:413
  106.8 4.7 %collective-permute-done.23.refs_11_ = bf16[512,256]{1,0:T(8,128)(2,1)S(1)} collective-permute-done((bf16[512,256]{1,0:T(8,128)(2,1)S(1)}, bf16[512,256]{1,0:T(8,128)(2,1)S(1)}, u32[]{:S(2)}, u32[]{:S(2)}) %collective-permute-start.23) | collective-permute-done | bytes 262176 | tf_op jit(solution)/shard_map/ppermute | solution.py:413
  111.6 3.4 %second.1 = (bf16[64,1024]{1,0:T(8,128)(2,1)S(1)}, bf16[64,1024]{1,0:T(8,128)(2,1)S(1)}, bf16[64,1024]{1,0:T(8,128)(2,1)S(1)}, bf16[64,1024]{1,0:T(8,128)(2,1)S(...) custom-call(f32[512,1024]{1,0:T(8,128)S(1)} %shard_map.157.sum_ref, ...), custom_call_target="tpu_custom_call" | custom-call | flops 1073741824 | bytes 6291456 | tf_op jit(solution)/shard_map/second/pallas_call | solution.py:704
  116.6 2.0 %collective-permute-start.26 = (bf16[64,1024]{1,0:T(8,128)(2,1)S(1)}, bf16[64,1024]{1,0:T(8,128)(2,1)S(1)}, u32[]{:S(2)}, u32[]{:S(2)}) collective-permute-start(bf16[64,1024]{1,0:T(8,128)(2,1)S(1)} %get-tuple-element.46), channel_id=1, source_target_pairs={{0,9},{1,8},{2,11},{3,10},{4,13},{5,12},{6,15},{7,14},{8,1},{9,0},... | collective-permute-start | bytes 393224 | tf_op jit(solution)/shard_map/ppermute | solution.py:422
  125.2 1.7 %collective-permute-done.29.refs_6_ = bf16[64,1024]{1,0:T(8,128)(2,1)S(1)} collective-permute-done((bf16[64,1024]{1,0:T(8,128)(2,1)S(1)}, bf16[64,1024]{1,0:T(8,128)(2,1)S(1)}, u32[]{:S(2)}, u32[]{:S(2)}) %collective-permute-start.29) | collective-permute-done | bytes 131104 | tf_op jit(solution)/shard_map/ppermute | solution.py:413
  127.0 2.4 %collective-permute-done.30.refs_7_ = bf16[64,1024]{1,0:T(8,128)(2,1)S(1)} collective-permute-done((bf16[64,1024]{1,0:T(8,128)(2,1)S(1)}, bf16[64,1024]{1,0:T(8,128)(2,1)S(1)}, u32[]{:S(2)}, u32[]{:S(2)}) %collective-permute-start.30) | collective-permute-done | bytes 131104 | tf_op jit(solution)/shard_map/ppermute | solution.py:422
  (99 shorter events, 28.2 us)
Async XLA Ops:
  11.3 8.5 %collective-permute-start.4 = (bf16[272,512]{1,0:T(8,128)(2,1)S(1)}, bf16[272,512]{1,0:T(8,128)(2,1)S(1)}, u32[]{:S(2)}, u32[]{:S(2)}) collective-permute-start(bf16[272,512]{1,0:T(8,128)(2,1)S(1)} %get-tuple-element.31), channel_id=1, source_target_pairs={{0,2},{2,0},{4,6},{6,4},{8,10},{10,8},{12,14},{14,12},{16,18},{18,... | collective-permute-start | bytes 835592 | tf_op jit(solution)/shard_map/ppermute | solution.py:413
  18.3 38.3 %collective-permute-start = (bf16[128,1024]{1,0:T(8,128)(2,1)}, bf16[128,1024]{1,0:T(8,128)(2,1)S(1)}, u32[]{:S(2)}, u32[]{:S(2)}) collective-permute-start(bf16[128,1024]{1,0:T(8,128)(2,1)} %constant_dynamic-update-slice_fusion), channel_id=1, source_target_pairs={{0,2},{2,0},{4,6},{6,4},{8,10},{10,8},{12,14},{14,12},{16,18},{18,... | collective-permute-start | bytes 786440 | tf_op jit(solution)/shard_map/ppermute | solution.py:413
  18.4 38.2 %collective-permute-start.1 = (bf16[128,1024]{1,0:T(8,128)(2,1)}, bf16[128,1024]{1,0:T(8,128)(2,1)}, u32[]{:S(2)}, u32[]{:S(2)}) collective-permute-start(bf16[128,1024]{1,0:T(8,128)(2,1)} %constant_dynamic-update-slice_fusion), channel_id=1, source_target_pairs={{2,4},{6,8},{10,12},{14,16},{18,20},{22,24},{26,28},{4,2},{8,6},{1... | collective-permute-start | bytes 786440 | tf_op jit(solution)/shard_map/ppermute | solution.py:418
  20.0 15.3 %collective-permute-start.11 = (bf16[272,512]{1,0:T(8,128)(2,1)S(1)}, bf16[272,512]{1,0:T(8,128)(2,1)S(1)}, u32[]{:S(2)}, u32[]{:S(2)}) collective-permute-start(bf16[272,512]{1,0:T(8,128)(2,1)S(1)} %shard_map.155.refs_0_), channel_id=1, source_target_pairs={{0,4},{2,6},{4,0},{6,2},{8,12},{10,14},{12,8},{14,10},{16,20},{18,... | collective-permute-start | bytes 835592 | tf_op jit(solution)/shard_map/ppermute | solution.py:413
  23.8 40.1 %collective-permute-start.9 = (bf16[1024,256]{1,0:T(8,128)(2,1)S(1)}, bf16[1024,256]{1,0:T(8,128)(2,1)S(1)}, u32[]{:S(2)}, u32[]{:S(2)}) collective-permute-start(bf16[1024,256]{1,0:T(8,128)(2,1)S(1)} %slice_bitcast_fusion.refs_4_), channel_id=1, source_target_pairs={{0,16},{2,18},{4,20},{6,22},{8,24},{10,26},{12,28},{14,30},{16,0},... | collective-permute-start | bytes 1572872 | tf_op jit(solution)/shard_map/ppermute | solution.py:413
  26.8 38.0 %collective-permute-start.8 = (bf16[1024,256]{1,0:T(8,128)(2,1)S(1)}, bf16[1024,256]{1,0:T(8,128)(2,1)S(1)}, u32[]{:S(2)}, u32[]{:S(2)}) collective-permute-start(bf16[1024,256]{1,0:T(8,128)(2,1)S(1)} %slice_bitcast_fusion.refs_4_), channel_id=1, source_target_pairs={{0,4},{2,6},{4,0},{6,2},{8,12},{10,14},{12,8},{14,10},{16,20},{18,... | collective-permute-start | bytes 1572872 | tf_op jit(solution)/shard_map/ppermute | solution.py:413
  35.4 20.9 %collective-permute-start.12 = (bf16[272,512]{1,0:T(8,128)(2,1)S(1)}, bf16[272,512]{1,0:T(8,128)(2,1)S(1)}, u32[]{:S(2)}, u32[]{:S(2)}) collective-permute-start(bf16[272,512]{1,0:T(8,128)(2,1)S(1)} %get-tuple-element.36.refs_0_), channel_id=1, source_target_pairs={{0,8},{2,10},{4,12},{6,14},{8,0},{10,2},{12,4},{14,6},{16,24},{18,... | collective-permute-start | bytes 835592 | tf_op jit(solution)/shard_map/ppermute | solution.py:413
  56.5 7.0 %collective-permute-start.13 = (bf16[128,512]{1,0:T(8,128)(2,1)S(1)}, bf16[128,512]{1,0:T(8,128)(2,1)S(1)}, u32[]{:S(2)}, u32[]{:S(2)}) collective-permute-start(bf16[128,512]{1,0:T(8,128)(2,1)S(1)} %get-tuple-element.38), channel_id=1, source_target_pairs={{0,16},{2,18},{4,20},{6,22},{8,24},{10,26},{12,28},{14,30},{16,0},... | collective-permute-start | bytes 393224 | tf_op jit(solution)/shard_map/ppermute | solution.py:413
  60.8 9.3 %collective-permute-start.5 = (bf16[128,1024]{1,0:T(8,128)(2,1)S(1)}, bf16[128,1024]{1,0:T(8,128)(2,1)S(1)}, u32[]{:S(2)}, u32[]{:S(2)}) collective-permute-start(bf16[128,1024]{1,0:T(8,128)(2,1)S(1)} %shard_map.156.refs_0_), channel_id=1, source_target_pairs={{0,8},{2,10},{4,12},{6,14},{8,0},{10,2},{12,4},{14,6},{16,24},{18,... | collective-permute-start | bytes 786440 | tf_op jit(solution)/shard_map/ppermute | solution.py:413
  62.7 10.0 %collective-permute-start.6 = (bf16[128,1024]{1,0:T(8,128)(2,1)S(1)}, bf16[128,1024]{1,0:T(8,128)(2,1)S(1)}, u32[]{:S(2)}, u32[]{:S(2)}) collective-permute-start(bf16[128,1024]{1,0:T(8,128)(2,1)S(1)} %shard_map.156.refs_0_), channel_id=1, source_target_pairs={{0,2},{2,0},{4,6},{6,4},{8,10},{10,8},{12,14},{14,12},{16,18},{18,... | collective-permute-start | bytes 786440 | tf_op jit(solution)/shard_map/ppermute | solution.py:413
  63.8 11.2 %collective-permute-start.14 = (bf16[256,512]{1,0:T(8,128)(2,1)S(1)}, bf16[256,512]{1,0:T(8,128)(2,1)S(1)}, u32[]{:S(2)}, u32[]{:S(2)}) collective-permute-start(bf16[256,512]{1,0:T(8,128)(2,1)S(1)} %get-tuple-element.41), channel_id=1, source_target_pairs={{0,2},{2,0},{4,6},{6,4},{8,10},{10,8},{12,14},{14,12},{16,18},{18,... | collective-permute-start | bytes 786440 | tf_op jit(solution)/shard_map/ppermute | solution.py:413
  63.9 20.7 %collective-permute-start.19 = (bf16[512,256]{1,0:T(8,128)(2,1)S(1)}, bf16[512,256]{1,0:T(8,128)(2,1)S(1)}, u32[]{:S(2)}, u32[]{:S(2)}) collective-permute-start(bf16[512,256]{1,0:T(8,128)(2,1)S(1)} %get-tuple-element.52.refs_4_), channel_id=1, source_target_pairs={{0,16},{2,18},{4,20},{6,22},{8,24},{10,26},{12,28},{14,30},{16,0},... | collective-permute-start | bytes 786440 | tf_op jit(solution)/shard_map/ppermute | solution.py:413
  64.8 29.3 %collective-permute-start.18 = (bf16[512,256]{1,0:T(8,128)(2,1)S(1)}, bf16[512,256]{1,0:T(8,128)(2,1)S(1)}, u32[]{:S(2)}, u32[]{:S(2)}) collective-permute-start(bf16[512,256]{1,0:T(8,128)(2,1)S(1)} %get-tuple-element.52.refs_4_), channel_id=1, source_target_pairs={{0,4},{2,6},{4,0},{6,2},{8,12},{10,14},{12,8},{14,10},{16,20},{18,... | collective-permute-start | bytes 786440 | tf_op jit(solution)/shard_map/ppermute | solution.py:413
  70.1 19.9 %collective-permute-start.22 = (bf16[512,256]{1,0:T(8,128)(2,1)S(1)}, bf16[512,256]{1,0:T(8,128)(2,1)S(1)}, u32[]{:S(2)}, u32[]{:S(2)}) collective-permute-start(bf16[512,256]{1,0:T(8,128)(2,1)S(1)} %get-tuple-element.51.refs_8_), channel_id=1, source_target_pairs={{0,16},{2,18},{4,20},{6,22},{8,24},{10,26},{12,28},{14,30},{16,0},... | collective-permute-start | bytes 786440 | tf_op jit(solution)/shard_map/ppermute | solution.py:413
  72.7 23.4 %collective-permute-start.10 = (bf16[1024,256]{1,0:T(8,128)(2,1)S(1)}, bf16[1024,256]{1,0:T(8,128)(2,1)S(1)}, u32[]{:S(2)}, u32[]{:S(2)}) collective-permute-start(bf16[1024,256]{1,0:T(8,128)(2,1)S(1)} %collective-permute-done.9.refs_6_), channel_id=1, source_target_pairs={{0,4},{2,6},{4,0},{6,2},{8,12},{10,14},{12,8},{14,10},{16,20},{18,... | collective-permute-start | bytes 1572872 | tf_op jit(solution)/shard_map/ppermute | solution.py:413
  75.0 19.1 %collective-permute-start.7 = (bf16[128,1024]{1,0:T(8,128)(2,1)S(1)}, bf16[128,1024]{1,0:T(8,128)(2,1)S(1)}, u32[]{:S(2)}, u32[]{:S(2)}) collective-permute-start(bf16[128,1024]{1,0:T(8,128)(2,1)S(1)} %collective-permute-done.5.refs_1_), channel_id=1, source_target_pairs={{0,2},{2,0},{4,6},{6,4},{8,10},{10,8},{12,14},{14,12},{16,18},{18,... | collective-permute-start | bytes 786440 | tf_op jit(solution)/shard_map/ppermute | solution.py:413
  84.6 11.5 %collective-permute-start.15 = (bf16[128,1024]{1,0:T(8,128)(2,1)S(1)}, bf16[128,1024]{1,0:T(8,128)(2,1)S(1)}, u32[]{:S(2)}, u32[]{:S(2)}) collective-permute-start(bf16[128,1024]{1,0:T(8,128)(2,1)S(1)} %shard_map.161.refs_0_), channel_id=1, source_target_pairs={{0,8},{2,10},{4,12},{6,14},{8,0},{10,2},{12,4},{14,6},{16,24},{18,... | collective-permute-start | bytes 786440 | tf_op jit(solution)/shard_map/ppermute | solution.py:413
  90.1 11.1 %collective-permute-start.21 = (bf16[512,256]{1,0:T(8,128)(2,1)S(1)}, bf16[512,256]{1,0:T(8,128)(2,1)S(1)}, u32[]{:S(2)}, u32[]{:S(2)}) collective-permute-start(bf16[512,256]{1,0:T(8,128)(2,1)S(1)} %get-tuple-element.51.refs_8_), channel_id=1, source_target_pairs={{0,4},{2,6},{4,0},{6,2},{8,12},{10,14},{12,8},{14,10},{16,20},{18,... | collective-permute-start | bytes 786440 | tf_op jit(solution)/shard_map/ppermute | solution.py:413
  94.0 12.8 %collective-permute-start.20 = (bf16[512,256]{1,0:T(8,128)(2,1)S(1)}, bf16[512,256]{1,0:T(8,128)(2,1)S(1)}, u32[]{:S(2)}, u32[]{:S(2)}) collective-permute-start(bf16[512,256]{1,0:T(8,128)(2,1)S(1)} %collective-permute-done.19.refs_6_), channel_id=1, source_target_pairs={{0,4},{2,6},{4,0},{6,2},{8,12},{10,14},{12,8},{14,10},{16,20},{18,... | collective-permute-start | bytes 786440 | tf_op jit(solution)/shard_map/ppermute | solution.py:413
  94.1 17.5 %collective-permute-start.23 = (bf16[512,256]{1,0:T(8,128)(2,1)S(1)}, bf16[512,256]{1,0:T(8,128)(2,1)S(1)}, u32[]{:S(2)}, u32[]{:S(2)}) collective-permute-start(bf16[512,256]{1,0:T(8,128)(2,1)S(1)} %collective-permute-done.22.refs_10_), channel_id=1, source_target_pairs={{0,4},{2,6},{4,0},{6,2},{8,12},{10,14},{12,8},{14,10},{16,20},{18,... | collective-permute-start | bytes 786440 | tf_op jit(solution)/shard_map/ppermute | solution.py:413
  96.1 15.5 %collective-permute-start.16 = (bf16[128,1024]{1,0:T(8,128)(2,1)S(1)}, bf16[128,1024]{1,0:T(8,128)(2,1)S(1)}, u32[]{:S(2)}, u32[]{:S(2)}) collective-permute-start(bf16[128,1024]{1,0:T(8,128)(2,1)S(1)} %shard_map.161.refs_0_), channel_id=1, source_target_pairs={{0,2},{2,0},{4,6},{6,4},{8,10},{10,8},{12,14},{14,12},{16,18},{18,... | collective-permute-start | bytes 786440 | tf_op jit(solution)/shard_map/ppermute | solution.py:413
  96.1 15.5 %collective-permute-start.17 = (bf16[128,1024]{1,0:T(8,128)(2,1)S(1)}, bf16[128,1024]{1,0:T(8,128)(2,1)S(1)}, u32[]{:S(2)}, u32[]{:S(2)}) collective-permute-start(bf16[128,1024]{1,0:T(8,128)(2,1)S(1)} %collective-permute-done.15.refs_1_), channel_id=1, source_target_pairs={{0,2},{2,0},{4,6},{6,4},{8,10},{10,8},{12,14},{14,12},{16,18},{18,... | collective-permute-start | bytes 786440 | tf_op jit(solution)/shard_map/ppermute | solution.py:413
  116.6 7.3 %collective-permute-start.26 = (bf16[64,1024]{1,0:T(8,128)(2,1)S(1)}, bf16[64,1024]{1,0:T(8,128)(2,1)S(1)}, u32[]{:S(2)}, u32[]{:S(2)}) collective-permute-start(bf16[64,1024]{1,0:T(8,128)(2,1)S(1)} %get-tuple-element.46), channel_id=1, source_target_pairs={{0,9},{1,8},{2,11},{3,10},{4,13},{5,12},{6,15},{7,14},{8,1},{9,0},... | collective-permute-start | bytes 393224 | tf_op jit(solution)/shard_map/ppermute | solution.py:422
  122.3 7.0 %collective-permute-start.30 = (bf16[64,1024]{1,0:T(8,128)(2,1)S(1)}, bf16[64,1024]{1,0:T(8,128)(2,1)S(1)}, u32[]{:S(2)}, u32[]{:S(2)}) collective-permute-start(bf16[64,1024]{1,0:T(8,128)(2,1)S(1)} %get-tuple-element.50), channel_id=1, source_target_pairs={{0,11},{1,10},{2,9},{3,8},{4,15},{5,14},{6,13},{7,12},{8,3},{9,2},... | collective-permute-start | bytes 393224 | tf_op jit(solution)/shard_map/ppermute | solution.py:422
  (28 other events, 237.3 us)

commit v5 on v4

--- a/solution.py
+++ b/solution.py
@@ -355,36 +355,6 @@
             at += 2
 
 
-def edge_kernel(*refs):
-    even = (lax.axis_index("sp") & 1) == 0
-    start = 0
-    for i in range(0, 6, 2):
-        lead = refs[i][...].astype(F32)
-        tail = refs[i + 1][...].astype(F32)
-        span = lead.shape[1]
-        refs[6][:, start : start + span] = jnp.where(even, tail, lead).astype(BF16)
-        refs[7][:, start : start + span] = jnp.where(even, lead, tail).astype(BF16)
-        start += span
-
-
-def edges(raw):
-    specs = []
-    for a in raw:
-        end = a.shape[0] // EDGE - 1
-        specs.append(pl.BlockSpec((EDGE, a.shape[1]), lambda i: (0, 0)))
-        specs.append(pl.BlockSpec((EDGE, a.shape[1]), lambda i, end=end: (end, 0)))
-    width = sum(a.shape[1] for a in raw)
-    return pl.pallas_call(
-        edge_kernel,
-        grid=(1,),
-        out_shape=[jax.ShapeDtypeStruct((EDGE, width), BF16)] * 2,
-        in_specs=specs,
-        out_specs=[pl.BlockSpec((EDGE, width), lambda i: (0, 0))] * 2,
-        compiler_params=pltpu.CompilerParams(vmem_limit_bytes=LIMIT),
-        name="edges",
-    )(*[a for a in raw for _ in range(2)])
-
-
 def join_kernel(keep_ref, got_ref, out_ref):
     even = (lax.axis_index("sp") & 1) == 0
     end = 2 * STATE
@@ -562,7 +532,11 @@
     sds = jax.ShapeDtypeStruct
 
     raw = (duality_source_matrix, storing_direction_matrix, fetching_direction_matrix)
-    to_pair, to_outer = edges(raw)
+    tail = jnp.concatenate([a[rows - EDGE :] for a in raw], axis=1)
+    lead = jnp.concatenate([a[:EDGE] for a in raw], axis=1)
+    even = (me & 1) == 0
+    to_pair = jnp.where(even, tail, lead)
+    to_outer = jnp.where(even, lead, tail)
     pair_edge = flip(to_pair, count, 1)
     outer_edge = outer(to_outer, count)
 
@@ -595,7 +569,7 @@
 
     deepest = final_mapping_matrix.shape[1]
     middle = deepest - deepest // LATE
-    halves = [gather(0, final_mapping_matrix[0])]
+    halves = [gather(0, final_mapping_matrix[0]), gather(1, final_mapping_matrix[1, :middle])]
     masks = sorted(halves[0])
 
     keep, send, read, inner, expl = call(
@@ -629,7 +603,7 @@
     later, weights, _, _ = lax.optimization_barrier(
         (me, final_mapping_matrix, matching_key_matrix, carried_value_matrix, seen)
     )[:4]
-    halves += [gather(1, weights[1, :middle]), gather(2, weights[1, middle:])]
+    halves.append(gather(2, weights[1, middle:]))
     pairs = jnp.concatenate([matching_key_matrix, carried_value_matrix], axis=1)
     pair_kv = flip(pairs, count, 1)
     outer_kv = outer(pairs, count)

time: 131 us -> 146 us (1.11)
  waiting for transfers between devices: 60.8 us -> 80.5 us
  starting transfers between devices: 46 us -> 37.4 us
  local copies, waits for them, and re-layouts: 8.5 us -> 12.5 us
    ppermute x25, waiting for transfers between devices: 56 us -> 73.6 us  [flip(): return lax.ppermute(a, 'sp', [(i, i ^ mask) for i in range(count)])]
    ppermute x25, starting transfers between devices: 37.2 us -> 30.5 us  [flip(): return lax.ppermute(a, 'sp', [(i, i ^ mask) for i in range(count)])]
    ppermute x4, waiting for transfers between devices: 4.77 us -> 6.89 us  [cross(): lax.ppermute(a, ('sp', 'tp'), [(2 * i + j, 2 * (i ^ mask) + 1 - j) for i...]
    slice x0 -> x2, local copies, waits for them, and re-layouts: none -> 1.55 us  [local(): tail = jnp.concatenate([a[rows - EDGE:] for a in raw], axis=1)]
    unnamed x43 -> x41, local copies, waits for them, and re-layouts: 7.76 us -> 9.26 us
  transfers between devices with their start and end apart: 31 -> 31, of which waited for: 15 -> 15; matrix products, arithmetic and copies ran while one was open for 2% -> 3% of each run, Pallas kernels for 5% -> 4%
where the time goes in v5:
time: 146 us; the launch traced here: 145 us
  waiting for transfers between devices  80.5 us (55%)
  starting transfers between devices  37.4 us (26%)
  Pallas kernels  13.2 us (9%)
  local copies, waits for them, and re-layouts  12.5 us (9%)
    ppermute x25, waiting for transfers between devices, flip(): return lax.ppermute(a, 'sp', [(i, i ^ mask) for i in range(count)])  73.6 us
    ppermute x25, starting transfers between devices, flip(): return lax.ppermute(a, 'sp', [(i, i ^ mask) for i in range(count)])  30.5 us
    pallas_call x9, Pallas kernels, call(): pl.pallas_call(kernel, out_shape=outs, in_specs=[SMEM] * scalars + [VMEM]...  9.78 us
    unnamed x41, local copies, waits for them, and re-layouts  9.26 us
    ppermute x4, waiting for transfers between devices, cross(): lax.ppermute(a, ('sp', 'tp'), [(2 * i + j, 2 * (i ^ mask) + 1 - j) for i...  6.89 us
    ppermute x4, starting transfers between devices, cross(): lax.ppermute(a, ('sp', 'tp'), [(2 * i + j, 2 * (i ^ mask) + 1 - j) for i...  5.44 us
    pallas_call x1, Pallas kernels, local(): pl.pallas_call(functools.partial(second_kernel, (len(group), len(chosen))...  3.43 us
  transfers between devices with their start and end apart: 31, of which 15 were waited for; matrix products, arithmetic and copies ran while one was open for 3% of the time, Pallas kernels for 4%

profile of v5, /device:TPU:0, one launch (start us, length us, event | category | flops | bytes accessed | tf_op | source)
XLA Modules:
  0.0 144.9 jit_solution(15022345294620592453)
XLA Ops:
  11.4 2.7 %shard_map.154 = (bf16[272,512]{1,0:T(8,128)(2,1)S(1)}, bf16[272,512]{1,0:T(8,128)(2,1)S(1)}, bf16[128,512]{1,0:T(8,128)(2,1)S(1)}, f32[128,1024]{1,0:T(8,128)S(1)}, bf16[128,64]{1,0:T(8,128)(2,1)S(1)}) custom-call(bf16[128,1024]{1,0:T(8,128)(2,1)S(1)} %copy-done.2, bf16[128,512]{1,0:T(8,128)(2,1)S(1)} %copy-done.3, bf16[128,512]{1,0:T(8,128)(2,1)S(1)} %copy-done.4, ...), custom_call_target="tpu_custom_call" | custom-call | flops 4000000000 | bytes 1937536 | tf_op jit(solution)/shard_map/pallas_call | solution.py:35
  14.8 4.2 %collective-permute-start.4 = (bf16[272,512]{1,0:T(8,128)(2,1)S(1)}, bf16[272,512]{1,0:T(8,128)(2,1)S(1)}, u32[]{:S(2)}, u32[]{:S(2)}) collective-permute-start(bf16[272,512]{1,0:T(8,128)(2,1)S(1)} %get-tuple-element.27), channel_id=1, source_target_pairs={{0,2},{2,0},{4,6},{6,4},{8,10},{10,8},{12,14},{14,12},{16,18},{18,... | collective-permute-start | bytes 835592 | tf_op jit(solution)/shard_map/ppermute | solution.py:383
  20.6 6.8 %collective-permute-start.19 = (bf16[512,256]{1,0:T(8,128)(2,1)S(1)}, bf16[512,256]{1,0:T(8,128)(2,1)S(1)}, u32[]{:S(2)}, u32[]{:S(2)}) collective-permute-start(bf16[512,256]{1,0:T(8,128)(2,1)S(1)} %slice_bitcast_fusion.2.refs_4_), channel_id=1, source_target_pairs={{0,16},{2,18},{4,20},{6,22},{8,24},{10,26},{12,28},{14,30},{16,0},... | collective-permute-start | bytes 786440 | tf_op jit(solution)/shard_map/ppermute | solution.py:383
  28.1 1.7 %collective-permute-start.11 = (bf16[272,512]{1,0:T(8,128)(2,1)S(1)}, bf16[272,512]{1,0:T(8,128)(2,1)S(1)}, u32[]{:S(2)}, u32[]{:S(2)}) collective-permute-start(bf16[272,512]{1,0:T(8,128)(2,1)S(1)} %shard_map.155.refs_0_), channel_id=1, source_target_pairs={{0,4},{2,6},{4,0},{6,2},{8,12},{10,14},{12,8},{14,10},{16,20},{18,... | collective-permute-start | bytes 835592 | tf_op jit(solution)/shard_map/ppermute | solution.py:383
  29.8 12.2 %collective-permute-done.11.refs_1_ = bf16[272,512]{1,0:T(8,128)(2,1)S(1)} collective-permute-done((bf16[272,512]{1,0:T(8,128)(2,1)S(1)}, bf16[272,512]{1,0:T(8,128)(2,1)S(1)}, u32[]{:S(2)}, u32[]{:S(2)}) %collective-permute-start.11) | collective-permute-done | bytes 278560 | tf_op jit(solution)/shard_map/ppermute | solution.py:383
  42.2 3.6 %collective-permute-start.12 = (bf16[272,512]{1,0:T(8,128)(2,1)S(1)}, bf16[272,512]{1,0:T(8,128)(2,1)S(1)}, u32[]{:S(2)}, u32[]{:S(2)}) collective-permute-start(bf16[272,512]{1,0:T(8,128)(2,1)S(1)} %get-tuple-element.32.refs_0_), channel_id=1, source_target_pairs={{0,8},{2,10},{4,12},{6,14},{8,0},{10,2},{12,4},{14,6},{16,24},{18,... | collective-permute-start | bytes 835592 | tf_op jit(solution)/shard_map/ppermute | solution.py:383
  46.8 4.7 %collective-permute-done.12.refs_1_ = bf16[272,512]{1,0:T(8,128)(2,1)S(1)} collective-permute-done((bf16[272,512]{1,0:T(8,128)(2,1)S(1)}, bf16[272,512]{1,0:T(8,128)(2,1)S(1)}, u32[]{:S(2)}, u32[]{:S(2)}) %collective-permute-start.12) | collective-permute-done | bytes 278560 | tf_op jit(solution)/shard_map/ppermute | solution.py:383
  51.5 2.7 %collective-permute-start.9 = (bf16[1024,256]{1,0:T(8,128)(2,1)S(1)}, bf16[1024,256]{1,0:T(8,128)(2,1)S(1)}, u32[]{:S(2)}, u32[]{:S(2)}) collective-permute-start(bf16[1024,256]{1,0:T(8,128)(2,1)S(1)} %slice_bitcast_fusion.refs_4_), channel_id=1, source_target_pairs={{0,16},{2,18},{4,20},{6,22},{8,24},{10,26},{12,28},{14,30},{16,0},... | collective-permute-start | bytes 1572872 | tf_op jit(solution)/shard_map/ppermute | solution.py:383
  54.7 3.6 %shard_map.156.refs_0_ = bf16[128,1024]{1,0:T(8,128)(2,1)S(1)} custom-call(f32[8]{0:T(128)S(1)} %copy-done.14, bf16[128,1024]{1,0:T(8,128)(2,1)S(1)} %copy-done.5, bf16[128,512]{1,0:T(8,128)(2,1)S(1)} %copy-done, bf16[128,512]{1,0:T(8,128)(2,1)S(1)} %copy-done.1, bf16[128,1024]{1,0:T(8,128)(2,1)S(1)} %collective-permute-done.pair_ref, ...), custom_call_target="tpu_custom_call" | custom-call | flops 3000000000 | bytes 1703968 | tf_op jit(solution)/shard_map/pallas_call | solution.py:35
  59.7 21.6 %collective-permute-done.13.other_ref = bf16[128,512]{1,0:T(8,128)(2,1)S(1)} collective-permute-done((bf16[128,512]{1,0:T(8,128)(2,1)S(1)}, bf16[128,512]{1,0:T(8,128)(2,1)S(1)}, u32[]{:S(2)}, u32[]{:S(2)}) %collective-permute-start.13) | collective-permute-done | bytes 131104 | tf_op jit(solution)/shard_map/ppermute | solution.py:383
  81.7 3.4 %collective-permute-start.8 = (bf16[1024,256]{1,0:T(8,128)(2,1)S(1)}, bf16[1024,256]{1,0:T(8,128)(2,1)S(1)}, u32[]{:S(2)}, u32[]{:S(2)}) collective-permute-start(bf16[1024,256]{1,0:T(8,128)(2,1)S(1)} %slice_bitcast_fusion.refs_4_), channel_id=1, source_target_pairs={{0,4},{2,6},{4,0},{6,2},{8,12},{10,14},{12,8},{14,10},{16,20},{18,... | collective-permute-start | bytes 1572872 | tf_op jit(solution)/shard_map/ppermute | solution.py:383
  87.3 10.5 %collective-permute-done.8.refs_5_ = bf16[1024,256]{1,0:T(8,128)(2,1)S(1)} collective-permute-done((bf16[1024,256]{1,0:T(8,128)(2,1)S(1)}, bf16[1024,256]{1,0:T(8,128)(2,1)S(1)}, u32[]{:S(2)}, u32[]{:S(2)}) %collective-permute-start.8) | collective-permute-done | bytes 524320 | tf_op jit(solution)/shard_map/ppermute | solution.py:383
  97.8 2.0 %collective-permute-start.20 = (bf16[512,256]{1,0:T(8,128)(2,1)S(1)}, bf16[512,256]{1,0:T(8,128)(2,1)S(1)}, u32[]{:S(2)}, u32[]{:S(2)}) collective-permute-start(bf16[512,256]{1,0:T(8,128)(2,1)S(1)} %collective-permute-done.19.refs_6_), channel_id=1, source_target_pairs={{0,4},{2,6},{4,0},{6,2},{8,12},{10,14},{12,8},{14,10},{16,20},{18,... | collective-permute-start | bytes 786440 | tf_op jit(solution)/shard_map/ppermute | solution.py:383
  100.9 2.0 %collective-permute-start.23 = (bf16[512,256]{1,0:T(8,128)(2,1)S(1)}, bf16[512,256]{1,0:T(8,128)(2,1)S(1)}, u32[]{:S(2)}, u32[]{:S(2)}) collective-permute-start(bf16[512,256]{1,0:T(8,128)(2,1)S(1)} %collective-permute-done.22.refs_10_), channel_id=1, source_target_pairs={{0,4},{2,6},{4,0},{6,2},{8,12},{10,14},{12,8},{14,10},{16,20},{18,... | collective-permute-start | bytes 786440 | tf_op jit(solution)/shard_map/ppermute | solution.py:383
  102.9 6.1 %collective-permute-done.10.refs_7_ = bf16[1024,256]{1,0:T(8,128)(2,1)S(1)} collective-permute-done((bf16[1024,256]{1,0:T(8,128)(2,1)S(1)}, bf16[1024,256]{1,0:T(8,128)(2,1)S(1)}, u32[]{:S(2)}, u32[]{:S(2)}) %collective-permute-start.10) | collective-permute-done | bytes 524320 | tf_op jit(solution)/shard_map/ppermute | solution.py:383
  110.8 3.9 %collective-permute-done.20.refs_7_ = bf16[512,256]{1,0:T(8,128)(2,1)S(1)} collective-permute-done((bf16[512,256]{1,0:T(8,128)(2,1)S(1)}, bf16[512,256]{1,0:T(8,128)(2,1)S(1)}, u32[]{:S(2)}, u32[]{:S(2)}) %collective-permute-start.20) | collective-permute-done | bytes 262176 | tf_op jit(solution)/shard_map/ppermute | solution.py:383
  114.6 5.6 %collective-permute-done.21.refs_9_ = bf16[512,256]{1,0:T(8,128)(2,1)S(1)} collective-permute-done((bf16[512,256]{1,0:T(8,128)(2,1)S(1)}, bf16[512,256]{1,0:T(8,128)(2,1)S(1)}, u32[]{:S(2)}, u32[]{:S(2)}) %collective-permute-start.21) | collective-permute-done | bytes 262176 | tf_op jit(solution)/shard_map/ppermute | solution.py:383
  120.3 5.4 %collective-permute-done.23.refs_11_ = bf16[512,256]{1,0:T(8,128)(2,1)S(1)} collective-permute-done((bf16[512,256]{1,0:T(8,128)(2,1)S(1)}, bf16[512,256]{1,0:T(8,128)(2,1)S(1)}, u32[]{:S(2)}, u32[]{:S(2)}) %collective-permute-start.23) | collective-permute-done | bytes 262176 | tf_op jit(solution)/shard_map/ppermute | solution.py:383
  125.6 3.4 %second.1 = (bf16[64,1024]{1,0:T(8,128)(2,1)S(1)}, bf16[64,1024]{1,0:T(8,128)(2,1)S(1)}, bf16[64,1024]{1,0:T(8,128)(2,1)S(1)}, bf16[64,1024]{1,0:T(8,128)(2,1)S(...) custom-call(f32[512,1024]{1,0:T(8,128)S(1)} %shard_map.157.sum_ref, ...), custom_call_target="tpu_custom_call" | custom-call | flops 1073741824 | bytes 6291456 | tf_op jit(solution)/shard_map/second/pallas_call | solution.py:678
  130.6 2.0 %collective-permute-start.26 = (bf16[64,1024]{1,0:T(8,128)(2,1)S(1)}, bf16[64,1024]{1,0:T(8,128)(2,1)S(1)}, u32[]{:S(2)}, u32[]{:S(2)}) collective-permute-start(bf16[64,1024]{1,0:T(8,128)(2,1)S(1)} %get-tuple-element.42), channel_id=1, source_target_pairs={{0,9},{1,8},{2,11},{3,10},{4,13},{5,12},{6,15},{7,14},{8,1},{9,0},... | collective-permute-start | bytes 393224 | tf_op jit(solution)/shard_map/ppermute | solution.py:392
  132.6 1.6 %collective-permute-start.28 = (bf16[64,1024]{1,0:T(8,128)(2,1)S(1)}, bf16[64,1024]{1,0:T(8,128)(2,1)S(1)}, u32[]{:S(2)}, u32[]{:S(2)}) collective-permute-start(bf16[64,1024]{1,0:T(8,128)(2,1)S(1)} %get-tuple-element.44), channel_id=1, source_target_pairs={{0,3},{1,2},{2,1},{3,0},{4,7},{5,6},{6,5},{7,4},{8,11},{9,10},{10,... | collective-permute-start | bytes 393224 | tf_op jit(solution)/shard_map/ppermute | solution.py:392
  134.6 2.4 %collective-permute-done.25.refs_2_ = bf16[64,1024]{1,0:T(8,128)(2,1)S(1)} collective-permute-done((bf16[64,1024]{1,0:T(8,128)(2,1)S(1)}, bf16[64,1024]{1,0:T(8,128)(2,1)S(1)}, u32[]{:S(2)}, u32[]{:S(2)}) %collective-permute-start.25) | collective-permute-done | bytes 131104 | tf_op jit(solution)/shard_map/ppermute | solution.py:383
  138.5 1.7 %collective-permute-done.28.refs_5_ = bf16[64,1024]{1,0:T(8,128)(2,1)S(1)} collective-permute-done((bf16[64,1024]{1,0:T(8,128)(2,1)S(1)}, bf16[64,1024]{1,0:T(8,128)(2,1)S(1)}, u32[]{:S(2)}, u32[]{:S(2)}) %collective-permute-start.28) | collective-permute-done | bytes 131104 | tf_op jit(solution)/shard_map/ppermute | solution.py:392
  140.4 3.6 %collective-permute-done.30.refs_7_ = bf16[64,1024]{1,0:T(8,128)(2,1)S(1)} collective-permute-done((bf16[64,1024]{1,0:T(8,128)(2,1)S(1)}, bf16[64,1024]{1,0:T(8,128)(2,1)S(1)}, u32[]{:S(2)}, u32[]{:S(2)}) %collective-permute-start.30) | collective-permute-done | bytes 131104 | tf_op jit(solution)/shard_map/ppermute | solution.py:392
  (101 shorter events, 27.3 us)
Async XLA Ops:
  14.8 13.1 %collective-permute-start.4 = (bf16[272,512]{1,0:T(8,128)(2,1)S(1)}, bf16[272,512]{1,0:T(8,128)(2,1)S(1)}, u32[]{:S(2)}, u32[]{:S(2)}) collective-permute-start(bf16[272,512]{1,0:T(8,128)(2,1)S(1)} %get-tuple-element.27), channel_id=1, source_target_pairs={{0,2},{2,0},{4,6},{6,4},{8,10},{10,8},{12,14},{14,12},{16,18},{18,... | collective-permute-start | bytes 835592 | tf_op jit(solution)/shard_map/ppermute | solution.py:383
  19.7 34.7 %collective-permute-start = (bf16[128,1024]{1,0:T(8,128)(2,1)}, bf16[128,1024]{1,0:T(8,128)(2,1)S(1)}, u32[]{:S(2)}, u32[]{:S(2)}) collective-permute-start(bf16[128,1024]{1,0:T(8,128)(2,1)} %constant_dynamic-update-slice_fusion), channel_id=1, source_target_pairs={{0,2},{2,0},{4,6},{6,4},{8,10},{10,8},{12,14},{14,12},{16,18},{18,... | collective-permute-start | bytes 786440 | tf_op jit(solution)/shard_map/ppermute | solution.py:383
  19.7 35.0 %collective-permute-start.1 = (bf16[128,1024]{1,0:T(8,128)(2,1)}, bf16[128,1024]{1,0:T(8,128)(2,1)S(1)}, u32[]{:S(2)}, u32[]{:S(2)}) collective-permute-start(bf16[128,1024]{1,0:T(8,128)(2,1)} %constant_dynamic-update-slice_fusion), channel_id=1, source_target_pairs={{2,4},{6,8},{10,12},{14,16},{18,20},{22,24},{26,28},{4,2},{8,6},{1... | collective-permute-start | bytes 786440 | tf_op jit(solution)/shard_map/ppermute | solution.py:388
  20.6 61.0 %collective-permute-start.19 = (bf16[512,256]{1,0:T(8,128)(2,1)S(1)}, bf16[512,256]{1,0:T(8,128)(2,1)S(1)}, u32[]{:S(2)}, u32[]{:S(2)}) collective-permute-start(bf16[512,256]{1,0:T(8,128)(2,1)S(1)} %slice_bitcast_fusion.2.refs_4_), channel_id=1, source_target_pairs={{0,16},{2,18},{4,20},{6,22},{8,24},{10,26},{12,28},{14,30},{16,0},... | collective-permute-start | bytes 786440 | tf_op jit(solution)/shard_map/ppermute | solution.py:383
  27.4 58.5 %collective-permute-start.18 = (bf16[512,256]{1,0:T(8,128)(2,1)S(1)}, bf16[512,256]{1,0:T(8,128)(2,1)S(1)}, u32[]{:S(2)}, u32[]{:S(2)}) collective-permute-start(bf16[512,256]{1,0:T(8,128)(2,1)S(1)} %slice_bitcast_fusion.2.refs_4_), channel_id=1, source_target_pairs={{0,4},{2,6},{4,0},{6,2},{8,12},{10,14},{12,8},{14,10},{16,20},{18,... | collective-permute-start | bytes 786440 | tf_op jit(solution)/shard_map/ppermute | solution.py:383
  28.1 13.9 %collective-permute-start.11 = (bf16[272,512]{1,0:T(8,128)(2,1)S(1)}, bf16[272,512]{1,0:T(8,128)(2,1)S(1)}, u32[]{:S(2)}, u32[]{:S(2)}) collective-permute-start(bf16[272,512]{1,0:T(8,128)(2,1)S(1)} %shard_map.155.refs_0_), channel_id=1, source_target_pairs={{0,4},{2,6},{4,0},{6,2},{8,12},{10,14},{12,8},{14,10},{16,20},{18,... | collective-permute-start | bytes 835592 | tf_op jit(solution)/shard_map/ppermute | solution.py:383
  42.2 9.3 %collective-permute-start.12 = (bf16[272,512]{1,0:T(8,128)(2,1)S(1)}, bf16[272,512]{1,0:T(8,128)(2,1)S(1)}, u32[]{:S(2)}, u32[]{:S(2)}) collective-permute-start(bf16[272,512]{1,0:T(8,128)(2,1)S(1)} %get-tuple-element.32.refs_0_), channel_id=1, source_target_pairs={{0,8},{2,10},{4,12},{6,14},{8,0},{10,2},{12,4},{14,6},{16,24},{18,... | collective-permute-start | bytes 835592 | tf_op jit(solution)/shard_map/ppermute | solution.py:383
  51.5 34.8 %collective-permute-start.9 = (bf16[1024,256]{1,0:T(8,128)(2,1)S(1)}, bf16[1024,256]{1,0:T(8,128)(2,1)S(1)}, u32[]{:S(2)}, u32[]{:S(2)}) collective-permute-start(bf16[1024,256]{1,0:T(8,128)(2,1)S(1)} %slice_bitcast_fusion.refs_4_), channel_id=1, source_target_pairs={{0,16},{2,18},{4,20},{6,22},{8,24},{10,26},{12,28},{14,30},{16,0},... | collective-permute-start | bytes 1572872 | tf_op jit(solution)/shard_map/ppermute | solution.py:383
  54.4 27.0 %collective-permute-start.13 = (bf16[128,512]{1,0:T(8,128)(2,1)S(1)}, bf16[128,512]{1,0:T(8,128)(2,1)S(1)}, u32[]{:S(2)}, u32[]{:S(2)}) collective-permute-start(bf16[128,512]{1,0:T(8,128)(2,1)S(1)} %get-tuple-element.34), channel_id=1, source_target_pairs={{0,16},{2,18},{4,20},{6,22},{8,24},{10,26},{12,28},{14,30},{16,0},... | collective-permute-start | bytes 393224 | tf_op jit(solution)/shard_map/ppermute | solution.py:383
  58.3 27.9 %collective-permute-start.5 = (bf16[128,1024]{1,0:T(8,128)(2,1)S(1)}, bf16[128,1024]{1,0:T(8,128)(2,1)S(1)}, u32[]{:S(2)}, u32[]{:S(2)}) collective-permute-start(bf16[128,1024]{1,0:T(8,128)(2,1)S(1)} %shard_map.156.refs_0_), channel_id=1, source_target_pairs={{0,8},{2,10},{4,12},{6,14},{8,0},{10,2},{12,4},{14,6},{16,24},{18,... | collective-permute-start | bytes 786440 | tf_op jit(solution)/shard_map/ppermute | solution.py:383
  81.7 16.1 %collective-permute-start.8 = (bf16[1024,256]{1,0:T(8,128)(2,1)S(1)}, bf16[1024,256]{1,0:T(8,128)(2,1)S(1)}, u32[]{:S(2)}, u32[]{:S(2)}) collective-permute-start(bf16[1024,256]{1,0:T(8,128)(2,1)S(1)} %slice_bitcast_fusion.refs_4_), channel_id=1, source_target_pairs={{0,4},{2,6},{4,0},{6,2},{8,12},{10,14},{12,8},{14,10},{16,20},{18,... | collective-permute-start | bytes 1572872 | tf_op jit(solution)/shard_map/ppermute | solution.py:383
  86.0 11.8 %collective-permute-start.6 = (bf16[128,1024]{1,0:T(8,128)(2,1)S(1)}, bf16[128,1024]{1,0:T(8,128)(2,1)S(1)}, u32[]{:S(2)}, u32[]{:S(2)}) collective-permute-start(bf16[128,1024]{1,0:T(8,128)(2,1)S(1)} %shard_map.156.refs_0_), channel_id=1, source_target_pairs={{0,2},{2,0},{4,6},{6,4},{8,10},{10,8},{12,14},{14,12},{16,18},{18,... | collective-permute-start | bytes 786440 | tf_op jit(solution)/shard_map/ppermute | solution.py:383
  86.2 14.7 %collective-permute-start.22 = (bf16[512,256]{1,0:T(8,128)(2,1)S(1)}, bf16[512,256]{1,0:T(8,128)(2,1)S(1)}, u32[]{:S(2)}, u32[]{:S(2)}) collective-permute-start(bf16[512,256]{1,0:T(8,128)(2,1)S(1)} %slice_bitcast_fusion.1.refs_8_), channel_id=1, source_target_pairs={{0,16},{2,18},{4,20},{6,22},{8,24},{10,26},{12,28},{14,30},{16,0},... | collective-permute-start | bytes 786440 | tf_op jit(solution)/shard_map/ppermute | solution.py:383
  86.2 22.8 %collective-permute-start.10 = (bf16[1024,256]{1,0:T(8,128)(2,1)S(1)}, bf16[1024,256]{1,0:T(8,128)(2,1)S(1)}, u32[]{:S(2)}, u32[]{:S(2)}) collective-permute-start(bf16[1024,256]{1,0:T(8,128)(2,1)S(1)} %collective-permute-done.9.refs_6_), channel_id=1, source_target_pairs={{0,4},{2,6},{4,0},{6,2},{8,12},{10,14},{12,8},{14,10},{16,20},{18,... | collective-permute-start | bytes 1572872 | tf_op jit(solution)/shard_map/ppermute | solution.py:383
  86.6 14.3 %collective-permute-start.7 = (bf16[128,1024]{1,0:T(8,128)(2,1)S(1)}, bf16[128,1024]{1,0:T(8,128)(2,1)S(1)}, u32[]{:S(2)}, u32[]{:S(2)}) collective-permute-start(bf16[128,1024]{1,0:T(8,128)(2,1)S(1)} %collective-permute-done.5.refs_1_), channel_id=1, source_target_pairs={{0,2},{2,0},{4,6},{6,4},{8,10},{10,8},{12,14},{14,12},{16,18},{18,... | collective-permute-start | bytes 786440 | tf_op jit(solution)/shard_map/ppermute | solution.py:383
  97.8 11.2 %collective-permute-start.15 = (bf16[128,1024]{1,0:T(8,128)(2,1)S(1)}, bf16[128,1024]{1,0:T(8,128)(2,1)S(1)}, u32[]{:S(2)}, u32[]{:S(2)}) collective-permute-start(bf16[128,1024]{1,0:T(8,128)(2,1)S(1)} %shard_map.161.refs_0_), channel_id=1, source_target_pairs={{0,8},{2,10},{4,12},{6,14},{8,0},{10,2},{12,4},{14,6},{16,24},{18,... | collective-permute-start | bytes 786440 | tf_op jit(solution)/shard_map/ppermute | solution.py:383
  97.8 16.8 %collective-permute-start.20 = (bf16[512,256]{1,0:T(8,128)(2,1)S(1)}, bf16[512,256]{1,0:T(8,128)(2,1)S(1)}, u32[]{:S(2)}, u32[]{:S(2)}) collective-permute-start(bf16[512,256]{1,0:T(8,128)(2,1)S(1)} %collective-permute-done.19.refs_6_), channel_id=1, source_target_pairs={{0,4},{2,6},{4,0},{6,2},{8,12},{10,14},{12,8},{14,10},{16,20},{18,... | collective-permute-start | bytes 786440 | tf_op jit(solution)/shard_map/ppermute | solution.py:383
  100.9 19.4 %collective-permute-start.21 = (bf16[512,256]{1,0:T(8,128)(2,1)S(1)}, bf16[512,256]{1,0:T(8,128)(2,1)S(1)}, u32[]{:S(2)}, u32[]{:S(2)}) collective-permute-start(bf16[512,256]{1,0:T(8,128)(2,1)S(1)} %slice_bitcast_fusion.1.refs_8_), channel_id=1, source_target_pairs={{0,4},{2,6},{4,0},{6,2},{8,12},{10,14},{12,8},{14,10},{16,20},{18,... | collective-permute-start | bytes 786440 | tf_op jit(solution)/shard_map/ppermute | solution.py:383
  100.9 24.7 %collective-permute-start.23 = (bf16[512,256]{1,0:T(8,128)(2,1)S(1)}, bf16[512,256]{1,0:T(8,128)(2,1)S(1)}, u32[]{:S(2)}, u32[]{:S(2)}) collective-permute-start(bf16[512,256]{1,0:T(8,128)(2,1)S(1)} %collective-permute-done.22.refs_10_), channel_id=1, source_target_pairs={{0,4},{2,6},{4,0},{6,2},{8,12},{10,14},{12,8},{14,10},{16,20},{18,... | collective-permute-start | bytes 786440 | tf_op jit(solution)/shard_map/ppermute | solution.py:383
  109.0 16.6 %collective-permute-start.16 = (bf16[128,1024]{1,0:T(8,128)(2,1)S(1)}, bf16[128,1024]{1,0:T(8,128)(2,1)S(1)}, u32[]{:S(2)}, u32[]{:S(2)}) collective-permute-start(bf16[128,1024]{1,0:T(8,128)(2,1)S(1)} %shard_map.161.refs_0_), channel_id=1, source_target_pairs={{0,2},{2,0},{4,6},{6,4},{8,10},{10,8},{12,14},{14,12},{16,18},{18,... | collective-permute-start | bytes 786440 | tf_op jit(solution)/shard_map/ppermute | solution.py:383
  109.0 16.6 %collective-permute-start.17 = (bf16[128,1024]{1,0:T(8,128)(2,1)S(1)}, bf16[128,1024]{1,0:T(8,128)(2,1)S(1)}, u32[]{:S(2)}, u32[]{:S(2)}) collective-permute-start(bf16[128,1024]{1,0:T(8,128)(2,1)S(1)} %collective-permute-done.15.refs_1_), channel_id=1, source_target_pairs={{0,2},{2,0},{4,6},{6,4},{8,10},{10,8},{12,14},{14,12},{16,18},{18,... | collective-permute-start | bytes 786440 | tf_op jit(solution)/shard_map/ppermute | solution.py:383
  130.6 7.8 %collective-permute-start.26 = (bf16[64,1024]{1,0:T(8,128)(2,1)S(1)}, bf16[64,1024]{1,0:T(8,128)(2,1)S(1)}, u32[]{:S(2)}, u32[]{:S(2)}) collective-permute-start(bf16[64,1024]{1,0:T(8,128)(2,1)S(1)} %get-tuple-element.42), channel_id=1, source_target_pairs={{0,9},{1,8},{2,11},{3,10},{4,13},{5,12},{6,15},{7,14},{8,1},{9,0},... | collective-permute-start | bytes 393224 | tf_op jit(solution)/shard_map/ppermute | solution.py:392
  132.6 7.5 %collective-permute-start.28 = (bf16[64,1024]{1,0:T(8,128)(2,1)S(1)}, bf16[64,1024]{1,0:T(8,128)(2,1)S(1)}, u32[]{:S(2)}, u32[]{:S(2)}) collective-permute-start(bf16[64,1024]{1,0:T(8,128)(2,1)S(1)} %get-tuple-element.44), channel_id=1, source_target_pairs={{0,3},{1,2},{2,1},{3,0},{4,7},{5,6},{6,5},{7,4},{8,11},{9,10},{10,... | collective-permute-start | bytes 393224 | tf_op jit(solution)/shard_map/ppermute | solution.py:392
  137.0 7.0 %collective-permute-start.30 = (bf16[64,1024]{1,0:T(8,128)(2,1)S(1)}, bf16[64,1024]{1,0:T(8,128)(2,1)S(1)}, u32[]{:S(2)}, u32[]{:S(2)}) collective-permute-start(bf16[64,1024]{1,0:T(8,128)(2,1)S(1)} %get-tuple-element.46), channel_id=1, source_target_pairs={{0,11},{1,10},{2,9},{3,8},{4,15},{5,14},{6,13},{7,12},{8,3},{9,2},... | collective-permute-start | bytes 393224 | tf_op jit(solution)/shard_map/ppermute | solution.py:392
  (27 other events, 280.8 us)
